TPU v7x, 32 devices: a whole 2x2x4 slice. The times are simulated.
32 devices in a mesh: sp: 8 (over z, x), tp: 4 (over y, core).
Axes of the slice: x: 2, y: 2, z: 4, core: 2. Of those that a mesh axis runs over, the one named last changes fastest.
Arguments:
- residual: bfloat16 [1024, 2048], P(('sp', 'tp')), may hold values from -6 to 6
- query_first: bfloat16 [1024, 1024], P('sp', 'tp'), may hold values from -200 to 200
- key_first: bfloat16 [1024, 1024], P('sp', 'tp'), may hold values from -200 to 200
- query_second: bfloat16 [1024, 1024], P('sp', 'tp'), may hold values from -200 to 200
- key_second: bfloat16 [1024, 1024], P('sp', 'tp'), may hold values from -200 to 200
- values: bfloat16 [1024, 2048], P('sp', 'tp'), may hold values from -6 to 6
- lambda_weight: float32 [16], P('tp'), may hold values from 0.3 to 0.8
- head_gain: float32 [128], replicated, may hold values from 0.1 to 1.9
- out_weight: bfloat16 [2048, 2048], P('sp', 'tp'), may hold values from -0.125 to 0.125
- norm_gain: float32 [2048], replicated, may hold values from 0.1 to 1.9
- gate_weight: bfloat16 [2048, 5632], P(None, 'tp'), may hold values from -0.125 to 0.125
- up_weight: bfloat16 [2048, 5632], P(None, 'tp'), may hold values from -0.125 to 0.125
- down_weight: bfloat16 [2048, 5632], P('sp', 'tp'), may hold values from -0.078125 to 0.078125
Outputs:
- layer_out: bfloat16 [1024, 2048], P(('sp', 'tp'))
All inputs are finite; a program needn't handle non-finite values.
Results may differ from a plain program's by a relative error of at most 0.017.
Values may be sent and summed in bfloat16 or wider, within the bound.
No kernel may reach another device: no remote copies, remote signals or barrier semaphores. Data moves between devices by JAX's collectives and lax.ppermute only.
A program may use at most 128 MiB of HBM per device.

v0:
```python
import math

import jax
import jax.numpy as jnp
from jax import lax
from jax.sharding import PartitionSpec as P

epsilon = 1e-06


def map_update(state_in, queries, key_rows, value_block, score_scale):
    maxima, totals, accumulated = state_in
    scores = (
        jnp.einsum("thd,khd->htk", queries, key_rows, preferred_element_type=jnp.float32)
        * score_scale
    )
    newest = jnp.maximum(maxima, jnp.max(scores, axis=-1))
    factor = jnp.exp(maxima - newest)
    weights = jnp.exp(scores - newest[:, :, None])
    totals = totals * factor + jnp.sum(weights, axis=-1)
    product = jnp.einsum(
        "htk,khe->the",
        weights.astype(jnp.bfloat16),
        value_block,
        preferred_element_type=jnp.float32,
    )
    accumulated = accumulated * factor.T[:, :, None] + product
    return (newest, totals, accumulated)


def local(
    residual,
    query_first,
    key_first,
    query_second,
    key_second,
    values,
    lambda_weight,
    head_gain,
    out_weight,
    norm_gain,
    gate_weight,
    up_weight,
    down_weight,
):
    tokens_here = query_first.shape[0]
    head_count = lambda_weight.shape[0]
    head_size = query_first.shape[1] // head_count
    value_size = values.shape[1] // head_count
    score_scale = head_size ** (-0.5)
    queries_first = query_first.reshape(tokens_here, head_count, head_size)
    queries_second = query_second.reshape(tokens_here, head_count, head_size)
    empty_stats = (
        jnp.full((head_count, tokens_here), -jnp.inf, jnp.float32),
        jnp.zeros((head_count, tokens_here), jnp.float32),
        jnp.zeros((tokens_here, head_count, value_size), jnp.float32),
    )
    start_state = (empty_stats, empty_stats)
    keys_one = lax.all_gather(key_first, "sp", axis=0, tiled=True)
    row_count = keys_one.shape[0]
    block_rows = math.gcd(row_count, 1024)
    blocks = (
        keys_one.reshape(row_count // block_rows, block_rows, head_count, head_size),
        lax.all_gather(key_second, "sp", axis=0, tiled=True).reshape(
            row_count // block_rows, block_rows, head_count, head_size
        ),
        lax.all_gather(values, "sp", axis=0, tiled=True).reshape(
            row_count // block_rows, block_rows, head_count, value_size
        ),
    )

    def advance(current, block_keys):
        return (
            (
                map_update(current[0], queries_first, block_keys[0], block_keys[2], score_scale),
                map_update(current[1], queries_second, block_keys[1], block_keys[2], score_scale),
            ),
            None,
        )

    statistics = lax.scan(advance, start_state, blocks)[0]

    def finish(map_stats):
        return map_stats[2] / map_stats[1].T[:, :, None]

    difference = finish(statistics[0]) - lambda_weight[None, :, None] * finish(statistics[1])
    scaled = difference * lax.rsqrt(
        jnp.mean(difference * difference, axis=-1, keepdims=True) + epsilon
    )
    attended = (
        (scaled * head_gain).astype(jnp.bfloat16).reshape(tokens_here, head_count * value_size)
    )
    partial_value = lax.dot_general(
        attended,
        lax.all_gather(out_weight, "sp", axis=0, tiled=True),
        (((1,), (1,)), ((), ())),
        preferred_element_type=jnp.float32,
    )
    summed = lax.psum_scatter(
        partial_value.astype(jnp.bfloat16), "tp", scatter_dimension=0, tiled=True
    ).astype(jnp.float32)
    after_attention = (residual.astype(jnp.float32) + summed).astype(jnp.bfloat16)
    stream = after_attention.astype(jnp.float32)
    scaled_rows = stream * lax.rsqrt(jnp.mean(stream * stream, axis=-1, keepdims=True) + epsilon)
    shard_piece = lax.all_gather(
        (scaled_rows * norm_gain).astype(jnp.bfloat16), "tp", axis=0, tiled=True
    )
    gate_part = jnp.dot(shard_piece, gate_weight, preferred_element_type=jnp.float32)
    up_part = jnp.dot(shard_piece, up_weight, preferred_element_type=jnp.float32)
    hidden = (jax.nn.silu(gate_part) * up_part).astype(jnp.bfloat16)
    down_partial = lax.dot_general(
        hidden,
        lax.all_gather(down_weight, "sp", axis=0, tiled=True),
        (((1,), (1,)), ((), ())),
        preferred_element_type=jnp.float32,
    )
    feed_out = lax.psum_scatter(
        down_partial.astype(jnp.bfloat16), "tp", scatter_dimension=0, tiled=True
    ).astype(jnp.float32)
    return (after_attention.astype(jnp.float32) + feed_out).astype(jnp.bfloat16)


def solution(mesh):
    return jax.shard_map(
        local,
        mesh=mesh,
        in_specs=(
            P(("sp", "tp"), None),
            P("sp", "tp"),
            P("sp", "tp"),
            P("sp", "tp"),
            P("sp", "tp"),
            P("sp", "tp"),
            P("tp"),
            P(),
            P("sp", "tp"),
            P(),
            P(None, "tp"),
            P(None, "tp"),
            P("sp", "tp"),
        ),
        out_specs=P(("sp", "tp"), None),
        check_vma=False,
    )
```

profile of v0, /device:TPU:0, one launch (start us, length us, event | category | flops | bytes accessed | tf_op | source)
XLA Modules:
  0.0 259.6 jit_solution(6984431258322703495)
XLA Ops:
  6.5 0.0 copy-start.4
  6.5 0.0 copy-start.5
  6.5 0.0 all-gather.4.cloned.1.call-start
  6.5 0.7 all-gather.4.cloned.1.call-update
  7.3 0.0 all-gather.6.cloned.1.call-start
  7.3 0.7 all-gather.6.cloned.1.call-update
  8.0 0.0 reduce-scatter.3.cloned.1.call-start
  8.1 33.7 %all_gather.18 = bf16[1024,256]{1,0:T(8,128)(2,1)S(1)} all-gather(bf16[128,256]{1,0:T(8,128)(2,1)} %param.15), channel_id=1, replica_groups=mesh['sp'=8,'tp'=4] {'sp'}, dimensions={0}, use_global_device_ids=true | all-gather | bytes 589824 | tf_op jit(solution)/shard_map/all_gather | solution.py:59
  41.8 0.2 copy.20
  42.0 1.0 copy.19
  43.0 0.0 copy-done.4
  43.0 32.2 %all_gather.20 = bf16[1024,256]{1,0:T(8,128)(2,1)S(1)} all-gather(bf16[128,256]{1,0:T(8,128)(2,1)S(1)} %copy-done.4), channel_id=1, replica_groups=mesh['sp'=8,'tp'=4] {'sp'}, dimensions={0}, use_global_device_ids=true | all-gather | bytes 589824 | tf_op jit(solution)/shard_map/all_gather | solution.py:64
  75.1 0.2 copy.23
  75.4 0.0 copy-done.5
  75.4 0.1 copy.22
  75.5 0.6 multiply_reduce_fusion.1
  76.1 0.5 fusion.1
  76.5 0.6 multiply_reduce_fusion
  77.1 0.0 copy-start
  77.1 1.3 copy-done
  78.4 0.5 fusion.3
  79.0 0.0 all-gather.4.cloned.1.call-done
  79.0 1.5 copy.21
  80.5 0.0 copy-start.1
  80.5 0.0 copy-start.8
  80.5 0.7 fusion.10
  81.2 0.9 copy-done.1
  82.1 0.0 copy-done.8
  82.1 0.0 copy-start.7
  82.1 0.7 multiply_reduce_fusion.2
  82.8 0.0 copy-done.7
  82.8 0.1 multiply_convert_fusion
  82.9 0.0 copy-start.2
  82.9 22.5 %all-gather.6.cloned.1.call-done = bf16[2048,512]{1,0:T(8,128)(2,1)} async-done(((bf16[256,512]{1,0:T(8,128)(2,1)}), bf16[2048,512]{1,0:T(8,128)(2,1)}) %all-gather.6.cloned.1.call-update) | async-done | bytes 2097168 | tf_op jit(solution)/shard_map/all_gather | solution.py:95
  105.5 0.0 copy-start.6
  105.5 3.2 %convolution_convert_fusion = bf16[128,2048]{1,0:T(8,128)(2,1)} fusion(bf16[128,512]{0,1:T(8,128)(2,1)S(1)} %bitcast.51, bf16[2048,512]{1,0:T(8,128)(2,1)} %all-gather.6.cloned.1.call-done), kind=kOutput, calls=%fused_computation.2 | convolution fusion | flops 268697600 | bytes 2752512 | tf_op jit(solution)/shard_map/dot_general | solution.py:93
  108.7 0.0 reduce-scatter.3.cloned.1.call-update
  108.7 0.0 all-gather.8.cloned.1.call-start
  108.7 0.5 all-gather.8.cloned.1.call-update
  109.3 0.0 reduce-scatter.5.cloned.1.call-start
  109.3 19.8 %reduce-scatter.3.cloned.1.call-done = bf16[32,2048]{1,0:T(8,128)(2,1)} async-done(((bf16[128,2048]{1,0:T(8,128)(2,1)}), bf16[32,2048]{1,0:T(8,128)(2,1)}) %reduce-scatter.3.cloned.1.call-update) | async-done | bytes 131088 | tf_op jit(solution)/shard_map/reduce_scatter | solution.py:99
  129.1 0.0 copy-done.2
  129.1 1.1 fusion.18
  130.1 0.0 copy-done.6
  130.2 1.0 fusion.20
  131.2 6.6 %all_gather.22 = bf16[128,2048]{1,0:T(8,128)(2,1)S(1)} all-gather(bf16[32,2048]{1,0:T(8,128)(2,1)S(1)} %fusion.20), channel_id=1, replica_groups=mesh['sp'=8,'tp'=4] {'tp'}, dimensions={0}, use_global_device_ids=true | all-gather | bytes 655360 | tf_op jit(solution)/shard_map/all_gather | solution.py:105
  137.8 4.0 %fusion.25 = f32[128,1408]{1,0:T(8,128)S(1)} fusion(bf16[128,2048]{1,0:T(8,128)(2,1)S(1)} %all_gather.22, bf16[2048,1408]{1,0:T(8,128)(2,1)} %param.23), kind=kOutput, calls=%fused_computation.44 | convolution fusion | flops 738197504 | bytes 7012352 | tf_op jit(solution)/shard_map/dot_general | solution.py:108
  141.8 0.0 copy-start.3
  141.8 81.6 %all-gather.8.cloned.1.call-done = bf16[2048,1408]{1,0:T(8,128)(2,1)} async-done(((bf16[256,1408]{1,0:T(8,128)(2,1)}), bf16[2048,1408]{1,0:T(8,128)(2,1)}) %all-gather.8.cloned.1.call-update) | async-done | bytes 5767184 | tf_op jit(solution)/shard_map/all_gather | solution.py:113
  223.5 8.0 %convolution_convert_fusion.1 = bf16[128,2048]{1,0:T(8,128)(2,1)} fusion(bf16[2048,1408]{1,0:T(8,128)(2,1)} %all-gather.8.cloned.1.call-done, bf16[128,2048]{1,0:T(8,128)(2,1)S(1)} %all_gather.22, bf16[2048,1408]{1,0:T(8,128)(2,1)} %param.24, f32[128,1408]{1,0:T(8,128)S(1)} %fusion.25), kind=kOutput, calls=%fused_computation.3 | convolution fusion | flops 1477738496 | bytes 13303808 | tf_op jit(solution)/shard_map/dot_general | solution.py:111
  231.5 0.0 reduce-scatter.5.cloned.1.call-update
  231.5 20.0 %reduce-scatter.5.cloned.1.call-done = bf16[32,2048]{1,0:T(8,128)(2,1)} async-done(((bf16[128,2048]{1,0:T(8,128)(2,1)}), bf16[32,2048]{1,0:T(8,128)(2,1)}) %reduce-scatter.5.cloned.1.call-update) | async-done | bytes 131088 | tf_op jit(solution)/shard_map/reduce_scatter | solution.py:117
  251.5 0.0 copy-done.3
  251.5 1.6 fusion.21
  (6 shorter events, 0.0 us)
Async XLA Ops:
  6.5 36.4 %copy-start.4 = (bf16[128,256]{1,0:T(8,128)(2,1)S(1)}, bf16[128,256]{1,0:T(8,128)(2,1)}, u32[]{:S(2)}) copy-start(bf16[128,256]{1,0:T(8,128)(2,1)} %param.17) | copy-start | bytes 196612
  6.5 68.8 %copy-start.5 = (bf16[128,256]{1,0:T(8,128)(2,1)S(1)}, bf16[128,256]{1,0:T(8,128)(2,1)}, u32[]{:S(2)}) copy-start(bf16[128,256]{1,0:T(8,128)(2,1)} %param.16) | copy-start | bytes 196612
  6.5 72.5 %all-gather.4.cloned.1.call-start = ((), (), s32[]{:S(2)}) async-start(), calls=%async_computation.2 | async-start | bytes 1179648 | tf_op jit(solution)/shard_map/all_gather | solution.py:67
  7.3 98.2 %all-gather.6.cloned.1.call-start = ((), (), s32[]{:S(2)}) async-start(), calls=%async_computation.3 | async-start | bytes 2359296 | tf_op jit(solution)/shard_map/all_gather | solution.py:95
  8.0 121.1 %reduce-scatter.3.cloned.1.call-start = ((), (), s32[]{:S(2)}) async-start(), calls=%async_computation.4 | async-start | bytes 655360 | tf_op jit(solution)/shard_map/reduce_scatter | solution.py:99
  77.1 1.3 copy-start
  80.5 1.6 copy-start.1
  80.5 1.6 copy-start.8
  82.1 0.7 copy-start.7
  82.9 46.2 %copy-start.2 = (bf16[32,2048]{1,0:T(8,128)(2,1)S(1)}, bf16[32,2048]{1,0:T(8,128)(2,1)}, u32[]{:S(2)}) copy-start(bf16[32,2048]{1,0:T(8,128)(2,1)} %param.13) | copy-start | bytes 393220
  105.5 24.7 %copy-start.6 = (f32[2048]{0:T(1024)S(1)}, f32[2048]{0:T(1024)}, u32[]{:S(2)}) copy-start(f32[2048]{0:T(1024)} %param.22) | copy-start | bytes 24580
  108.7 114.8 %all-gather.8.cloned.1.call-start = ((), (), s32[]{:S(2)}) async-start(), calls=%async_computation.5 | async-start | bytes 6488064 | tf_op jit(solution)/shard_map/all_gather | solution.py:113
  109.3 142.2 %reduce-scatter.5.cloned.1.call-start = ((), (), s32[]{:S(2)}) async-start(), calls=%async_computation.6 | async-start | bytes 655360 | tf_op jit(solution)/shard_map/reduce_scatter | solution.py:117
  141.8 109.7 %copy-start.3 = (bf16[32,2048]{1,0:T(8,128)(2,1)S(1)}, bf16[32,2048]{1,0:T(8,128)(2,1)}, u32[]{:S(2)}) copy-start(bf16[32,2048]{1,0:T(8,128)(2,1)} %reduce-scatter.3.cloned.1.call-done) | copy-start | bytes 393220
Sparse Core Ops, SparseCore 0:
  9.5 44.3 all-gather.3
  55.9 49.4 all-gather.5
  108.8 20.2 reduce-scatter.2
  131.1 92.2 all-gather.7
  231.6 19.8 reduce-scatter.4
where the time goes:
time: 260 us
  waiting for transfers between devices  146 us (56%)
  blocking collectives  72.5 us (28%)
  matrix products  17.7 us (7%)
  between operations  13.3 us (5%)
  local copies, waits for them, and re-layouts  5.22 us (2%)
  other arithmetic  4.8 us (2%)
    all_gather x1, waiting for transfers between devices, local(): lax.all_gather(down_weight, 'sp', axis=0, tiled=True)  81.6 us
    all_gather x1, blocking collectives, local(): keys_one = lax.all_gather(key_first, 'sp', axis=0, tiled=True)  33.7 us
    all_gather x1, blocking collectives, local(): lax.all_gather(key_second, 'sp', axis=0, tiled=True)  32.2 us
    all_gather x1, waiting for transfers between devices, local(): lax.all_gather(out_weight, 'sp', axis=0, tiled=True)  22.5 us
    reduce_scatter x1, waiting for transfers between devices, local(): lax.psum_scatter(down_partial.astype(jnp.bfloat16), 'tp', scatter_dimensi...  20 us
    reduce_scatter x1, waiting for transfers between devices, local(): lax.psum_scatter(partial_value.astype(jnp.bfloat16), 'tp', scatter_dimens...  19.8 us
    dot_general x1, matrix products, local(): lax.dot_general(hidden, lax.all_gather(down_weight, 'sp', axis=0, tiled=T...  8 us
    all_gather x1, blocking collectives, local(): lax.all_gather((scaled_rows * norm_gain).astype(jnp.bfloat16), 'tp', axis...  6.59 us
  transfers between devices with their start and end apart: 5, of which 4 were waited for; matrix products, arithmetic and copies ran while one was open for 5% of the time, Pallas kernels for 0%

commit v1 on v0

--- a/solution.py
+++ b/solution.py
@@ -1,9 +1,13 @@
+import functools
 import math
 
 import jax
 import jax.numpy as jnp
 from jax import lax
+from jax.experimental import pallas as pl
+from jax.experimental.pallas import tpu as pltpu
 from jax.sharding import PartitionSpec as P
+
 
 epsilon = 1e-06
 
@@ -28,7 +32,7 @@
     return (newest, totals, accumulated)
 
 
-def local(
+def gathered_local(
     residual,
     query_first,
     key_first,
@@ -120,7 +124,351 @@
     return (after_attention.astype(jnp.float32) + feed_out).astype(jnp.bfloat16)
 
 
+def deal_body(*refs, sp_size, tp_size):
+    sources, out_ref, extra_ref, arrived, sems = refs[:7], refs[7], refs[8], refs[9:16], refs[16]
+    copies = [
+        pltpu.make_async_copy(source, to, sems.at[index])
+        for index, (source, to) in enumerate(zip(sources, arrived))
+    ]
+    for copy in copies:
+        copy.start()
+    for copy in copies:
+        copy.wait()
+    qf_ref, kf_ref, qs_ref, ks_ref, v_ref, gain_ref, lambda_ref = arrived
+    here = lax.axis_index("sp") // 2
+    member = lax.axis_index("tp")
+    heads = sp_size // 2
+    rows = qf_ref.shape[0] // tp_size
+    size = qf_ref.shape[1] // heads
+    value_size = v_ref.shape[1] // heads
+    extra_ref[0:1] = gain_ref[...]
+    extra_ref[1:2] = jnp.full((1, value_size), lambda_ref[here], jnp.float32)
+    for block in range(tp_size):
+        at = pl.ds(pl.multiple_of((member ^ block) * rows, rows), rows)
+        for head in range(heads):
+            columns = slice(head * size, (head + 1) * size)
+            narrow = [ref[at, columns] for ref in (qf_ref, qs_ref, kf_ref, ks_ref)]
+            out_ref[here ^ head, block * rows : (block + 1) * rows, :] = jnp.concatenate(
+                narrow + [v_ref[at, head * value_size : (head + 1) * value_size]], axis=1
+            )
+
+
+def attention_body(
+    extra_ref, a_ref, b_ref, c_ref, d_ref, ab_ref, cd_ref, out_ref, k_ref, v_ref
+):
+    rows = a_ref.shape[0]
+    gain, weight = extra_ref[0:1], extra_ref[1:2]
+    lanes = a_ref.shape[1] - ab_ref.shape[1]
+    head_size = lanes // 2
+    scale = head_size ** (-0.5)
+    queries = (a_ref, b_ref, c_ref, d_ref)
+    for index, ref in enumerate(queries):
+        k_ref[index * rows : (index + 1) * rows] = ref[:, lanes : 2 * lanes]
+        v_ref[index * rows : (index + 1) * rows] = ref[:, 2 * lanes :]
+    for index, ref in enumerate((ab_ref, cd_ref)):
+        at = slice((4 + 2 * index) * rows, (6 + 2 * index) * rows)
+        k_ref[at] = ref[:, :lanes]
+        v_ref[at] = ref[:, lanes:]
+    lane = lax.broadcasted_iota(jnp.int32, (rows, lanes), 1)
+
+    def one_map(query, which):
+        wanted = (lane < head_size) if which == 0 else (lane >= head_size)
+        scores = (
+            lax.dot_general(
+                jnp.where(wanted, query, jnp.zeros_like(query)),
+                k_ref[...],
+                (((1,), (1,)), ((), ())),
+                preferred_element_type=jnp.float32,
+            )
+            * scale
+        )
+        shifted = jnp.exp(scores - scores.max(axis=-1, keepdims=True))
+        total = shifted.sum(axis=-1, keepdims=True)
+        product = jnp.dot(
+            shifted.astype(jnp.bfloat16), v_ref[...], preferred_element_type=jnp.float32
+        )
+        return product / total
+
+    for index, ref in enumerate(queries):
+        query = ref[:, :lanes]
+        difference = one_map(query, 0) - weight * one_map(query, 1)
+        scaled = difference * lax.rsqrt(
+            jnp.mean(difference * difference, axis=-1, keepdims=True) + epsilon
+        )
+        out_ref[index] = (scaled * gain).astype(out_ref.dtype)
+
+
+def project_body(
+    own_ref, other_ref, b_ref, c_ref, d_ref, source, kept_ref, sent_ref, a_ref, sem, *, tp_size
+):
+    copy = pltpu.make_async_copy(source, a_ref, sem)
+    copy.start()
+    rows = own_ref.shape[0] // tp_size
+    width = a_ref.shape[0]
+    for index, ref in ((1, b_ref), (2, c_ref), (3, d_ref), (0, a_ref)):
+        if index == 0:
+            copy.wait()
+        columns = slice(index * width, (index + 1) * width)
+        for side, left_ref in enumerate((own_ref, other_ref)):
+            product = lax.dot_general(
+                left_ref[...], ref[...], (((1,), (1,)), ((), ())), preferred_element_type=jnp.float32
+            )
+            for chip in range(tp_size // 2):
+                to = slice((side * 2 + chip) * rows, (side * 2 + chip + 1) * rows)
+                at = chip * 2 * rows
+                kept_ref[to, columns] = product[at : at + rows]
+                sent_ref[to, columns] = product[at + rows : at + 2 * rows].astype(sent_ref.dtype)
+
+
+def gate_body(here_ref, there_ref, gate_ref, up_ref, hidden_ref, both_ref, *rest, tile):
+    rows = here_ref.shape[0]
+    units = gate_ref.shape[1]
+    starts = range(0, units, tile)
+    buffers, sems = rest[:-1], rest[-1]
+    copies = []
+    for index, start in enumerate(starts):
+        columns = pl.ds(start, min(tile, units - start))
+        pair = [
+            pltpu.make_async_copy(
+                ref.at[:, columns], buffers[2 * index + which], sems.at[2 * index + which]
+            )
+            for which, ref in enumerate((gate_ref, up_ref))
+        ]
+        for copy in pair:
+            copy.start()
+        copies.append(pair)
+    both_ref[:rows] = here_ref[...]
+    both_ref[rows:] = there_ref[...]
+    for index, start in enumerate(starts):
+        for copy in copies[index]:
+            copy.wait()
+        gate, up = (
+            jnp.dot(
+                both_ref[...], buffers[2 * index + which][...], preferred_element_type=jnp.float32
+            )
+            for which in range(2)
+        )
+        hidden = gate / (1.0 + jnp.exp(-gate)) * up
+        hidden_ref[:, start : start + gate.shape[1]] = hidden.astype(hidden_ref.dtype)
+
+
+def down_body(
+    hidden_ref,
+    own_ref,
+    near_ref,
+    third_inner_ref,
+    third_outer_ref,
+    last_inner_ref,
+    last_outer_ref,
+    kept_ref,
+    sent_ref,
+    *,
+    sp_size,
+):
+    place = lax.axis_index("sp") // 2
+    inner = (place > 0) & (place < sp_size // 2 - 1)
+    rows = kept_ref.shape[0]
+    width = own_ref.shape[0]
+    pieces = (
+        own_ref[...],
+        near_ref[...],
+        jnp.where(inner, third_inner_ref[...], third_outer_ref[...]),
+        jnp.where(inner, last_inner_ref[...], last_outer_ref[...]),
+    )
+    for index, piece in enumerate(pieces):
+        product = lax.dot_general(
+            hidden_ref[...], piece, (((1,), (1,)), ((), ())), preferred_element_type=jnp.float32
+        )
+        columns = slice(index * width, (index + 1) * width)
+        kept_ref[:, columns] = product[:rows]
+        sent_ref[:, columns] = product[rows:].astype(sent_ref.dtype)
+
+
+def kernel(body, out_shape, near, away=(), scratch=(), limit=16):
+    vmem = pl.BlockSpec(memory_space=pltpu.VMEM)
+    many = isinstance(out_shape, tuple)
+    call = pl.pallas_call(
+        body,
+        out_shape=out_shape,
+        in_specs=[vmem] * len(near) + [pl.BlockSpec(memory_space=pltpu.HBM)] * len(away),
+        out_specs=(vmem,) * len(out_shape) if many else vmem,
+        scratch_shapes=list(scratch),
+        compiler_params=pltpu.CompilerParams(vmem_limit_bytes=limit * 2**20),
+    )
+    return call(*near, *(pltpu.with_memory_space_constraint(array, pltpu.HBM) for array in away))
+
+
+def moved_local(
+    sp_size,
+    tp_size,
+    residual,
+    query_first,
+    key_first,
+    query_second,
+    key_second,
+    values,
+    lambda_weight,
+    head_gain,
+    out_weight,
+    norm_gain,
+    gate_weight,
+    up_weight,
+    down_weight,
+):
+    side, near, across, far = 1, 2, sp_size // 2, sp_size - 2
+    planes = sp_size // 2
+    chip, core = tp_size // 2, 1
+    place = lax.axis_index("sp")
+    on_side = (place & 1) == 1
+    low = (place & 2) == 2
+    high = (place & 4) == 4
+    bf16, f32 = jnp.bfloat16, jnp.float32
+
+    def swap(array, axis, distance):
+        count = sp_size if axis == "sp" else tp_size
+        return lax.ppermute(array, axis, [(i, i ^ distance) for i in range(count)])
+
+    def swap_both(array, first, second):
+        pairs = [
+            (i * tp_size + j, (i ^ first) * tp_size + (j ^ second))
+            for i in range(sp_size)
+            for j in range(tp_size)
+        ]
+        return lax.ppermute(array, ("sp", "tp"), pairs)
+
+    inner = [i for i in range(sp_size) if 0 < i // 2 < planes - 1]
+    middle_pairs = [(i, i ^ far) for i in inner]
+    outward_pairs = [(i, i ^ near) for i in inner]
+
+    def three(first, second, third):
+        third = swap(third, "sp", far)
+        second = swap(second, "sp", across)
+        return swap(first, "sp", near), second, third
+
+    def along_line(weight):
+        near_one = swap(weight, "sp", near)
+        middle_one = lax.ppermute(weight, "sp", middle_pairs)
+        middle_two = lax.ppermute(near_one, "sp", middle_pairs)
+        outer_one = lax.ppermute(middle_one, "sp", outward_pairs)
+        outer_two = lax.ppermute(middle_two, "sp", outward_pairs)
+        return weight, near_one, middle_one, outer_one, middle_two, outer_two
+
+    def planes_by_distance(n):
+        n = [jnp.where(low, n[k ^ 1], n[k]) for k in range(4)]
+        return [jnp.where(high, n[k ^ 2], n[k]) for k in range(4)]
+
+    def planes_along_line(n):
+        first, second = jnp.where(low, n[1], n[0]), jnp.where(low, n[0], n[1])
+        return [
+            jnp.where(high, n[3], first),
+            jnp.where(high, n[2], second),
+            jnp.where(high, first, n[2]),
+            jnp.where(high, second, n[3]),
+        ]
+
+    def scatter_sum(ours, given_away, ordered):
+        ours = ours + swap(given_away, "tp", core).astype(f32)
+        rows = ours.shape[0] // 4
+        rounded = ours.astype(bf16)
+        from_both = swap_both(rounded[3 * rows :], side, chip)
+        from_side = swap(rounded[2 * rows : 3 * rows], "sp", side)
+        from_chip = swap(rounded[rows : 2 * rows], "tp", chip)
+        same = ours[:rows] + from_chip.astype(f32)
+        other = from_side.astype(f32) + from_both.astype(f32)
+        piece = same.shape[1] // planes
+        joined = []
+        for k in range(planes):
+            a, b = (array[:, k * piece : (k + 1) * piece] for array in (same, other))
+            joined.append(
+                jnp.concatenate([jnp.where(on_side, b, a), jnp.where(on_side, a, b)], axis=1)
+            )
+        return jnp.concatenate(ordered(joined), axis=1)
+
+    tokens = query_first.shape[0]
+    rows = tokens // tp_size
+    head_lanes = 2 * query_first.shape[1] // planes
+    value_size = head_gain.shape[0]
+
+    streams = (query_first, key_first, query_second, key_second, values)
+    dealt, extra = kernel(
+        functools.partial(deal_body, sp_size=sp_size, tp_size=tp_size),
+        (
+            jax.ShapeDtypeStruct((planes, tokens, 2 * head_lanes + value_size), bf16),
+            jax.ShapeDtypeStruct((2, value_size), f32),
+        ),
+        (),
+        (*streams, head_gain.reshape(1, -1), lambda_weight),
+        [pltpu.VMEM(array.shape, bf16) for array in streams]
+        + [
+            pltpu.VMEM((1, value_size), f32),
+            pltpu.SMEM(lambda_weight.shape, f32),
+            pltpu.SemaphoreType.DMA((7,)),
+        ],
+    )
+    first, second, third = three(dealt[1], dealt[2], dealt[3])
+    early = swap(jnp.concatenate([dealt[0][:, head_lanes:], first[:, head_lanes:]], 0), "sp", side)
+    late = swap(jnp.concatenate([second[:, head_lanes:], third[:, head_lanes:]], 0), "sp", side)
+    attended = kernel(
+        attention_body,
+        jax.ShapeDtypeStruct((planes, tokens, value_size), bf16),
+        (extra, dealt[0], first, second, third, early, late),
+        scratch=[
+            pltpu.VMEM((2 * planes * tokens, head_lanes), bf16),
+            pltpu.VMEM((2 * planes * tokens, value_size), bf16),
+        ],
+    )
+    back = three(attended[1], attended[2], attended[3])
+    own_heads = jnp.concatenate(planes_by_distance([attended[0], *back]), axis=1)
+    other_heads = swap(own_heads, "sp", side)
+
+    half = (4 * rows, residual.shape[1] // 2)
+    halves = (jax.ShapeDtypeStruct(half, f32), jax.ShapeDtypeStruct(half, bf16))
+    projected = kernel(
+        functools.partial(project_body, tp_size=tp_size),
+        halves,
+        (own_heads, other_heads, *three(out_weight, out_weight, out_weight)),
+        (out_weight,),
+        [pltpu.VMEM(out_weight.shape, bf16), pltpu.SemaphoreType.DMA],
+    )
+    summed = scatter_sum(*projected, planes_by_distance)
+    after_attention = (residual.astype(f32) + summed).astype(bf16)
+    stream = after_attention.astype(f32)
+    scaled_rows = stream * lax.rsqrt(jnp.mean(stream * stream, axis=-1, keepdims=True) + epsilon)
+    normed = (scaled_rows * norm_gain).astype(bf16)
+
+    from_both = swap_both(normed, side, chip)
+    from_side = swap(normed, "sp", side)
+    from_chip = swap(normed, "tp", chip)
+    four = jnp.concatenate([normed, from_chip, from_side, from_both], axis=0)
+    units = gate_weight.shape[1]
+    tile = 256
+    sizes = [min(tile, units - start) for start in range(0, units, tile) for _ in range(2)]
+    hidden = kernel(
+        functools.partial(gate_body, tile=tile),
+        jax.ShapeDtypeStruct((8 * rows, units), bf16),
+        (four, swap(four, "tp", core)),
+        (gate_weight, up_weight),
+        [pltpu.VMEM((8 * rows, residual.shape[1]), bf16)]
+        + [pltpu.VMEM((residual.shape[1], size), bf16) for size in sizes]
+        + [pltpu.SemaphoreType.DMA((len(sizes),))],
+        limit=24,
+    )
+    fed = kernel(
+        functools.partial(down_body, sp_size=sp_size), halves, (hidden, *along_line(down_weight))
+    )
+    return (stream + scatter_sum(*fed, planes_along_line)).astype(bf16)
+
+
 def solution(mesh):
+    sp_size, tp_size = mesh.shape["sp"], mesh.shape["tp"]
+
+    def local(*arrays):
+        total_tokens = arrays[1].shape[0] * sp_size
+        short = total_tokens <= arrays[0].shape[1]
+        if short and (sp_size, tp_size) == (8, 4):
+            return moved_local(sp_size, tp_size, *arrays)
+        return gathered_local(*arrays)
+
     return jax.shard_map(
         local,
         mesh=mesh,

time: 260 us -> 125 us (0.48)
  waiting for transfers between devices: 146 us -> 70 us
  blocking collectives: 72.5 us -> 0 us
  starting transfers between devices: 0.16 us -> 40.2 us
  matrix products: 17.7 us -> 0 us
  between operations: 13.3 us -> 0.3 us
  Pallas kernels: 0 us -> 12.8 us
  local copies, waits for them, and re-layouts: 5.22 us -> 0.12 us
  other arithmetic: 4.8 us -> 1.38 us
    all_gather x3 -> x0, waiting for transfers between devices: 104 us -> none  [the longest x1 81.6 us: local(): lax.all_gather(down_weight, 'sp', axis=0, tiled=True)]
    all_gather x3 -> x0, blocking collectives: 72.5 us -> none  [the longest x1 33.7 us: local(): keys_one = lax.all_gather(key_first, 'sp', axis=0, tiled=True)]
    ppermute x0 -> x29, waiting for transfers between devices: none -> 70 us  [the longest x22 42.6 us: swap(): return lax.ppermute(array, axis, [(i, i ^ distance) for i in range(count)])]
    ppermute x0 -> x29, starting transfers between devices: none -> 40.2 us  [the longest x22 32.7 us: swap(): return lax.ppermute(array, axis, [(i, i ^ distance) for i in range(count)])]
    reduce_scatter x2 -> x0, waiting for transfers between devices: 39.8 us -> none  [the longest x1 20 us: local(): lax.psum_scatter(down_partial.astype(jnp.bfloat16), 'tp', scatter_dimensi...]
    dot_general x7 -> x0, matrix products: 17.7 us -> none  [the longest x1 8 us: local(): lax.dot_general(hidden, lax.all_gather(down_weight, 'sp', axis=0, tiled=T...]
    pallas_call x0 -> x5, Pallas kernels: none -> 12.8 us  [kernel(): call(*near, *(pltpu.with_memory_space_constraint(array, pltpu.HBM) for ar...]
    unnamed x20 -> x6, local copies, waits for them, and re-layouts: 3.32 us -> 0.01 us
  transfers between devices with their start and end apart: 5 -> 29, of which waited for: 4 -> 20; matrix products, arithmetic and copies ran while one was open for 5% -> 0% of each run, Pallas kernels for 0% -> 5%
where the time goes in v1:
time: 125 us
  waiting for transfers between devices  70 us (56%)
  starting transfers between devices  40.2 us (32%)
  Pallas kernels  12.8 us (10%)
  other arithmetic  1.38 us (1%)
    ppermute x22, waiting for transfers between devices, swap(): return lax.ppermute(array, axis, [(i, i ^ distance) for i in range(count)])  42.6 us
    ppermute x22, starting transfers between devices, swap(): return lax.ppermute(array, axis, [(i, i ^ distance) for i in range(count)])  32.7 us
    pallas_call x5, Pallas kernels, kernel(): call(*near, *(pltpu.with_memory_space_constraint(array, pltpu.HBM) for ar...  12.8 us
    ppermute x1, waiting for transfers between devices, along_line(): outer_two = lax.ppermute(middle_two, 'sp', outward_pairs)  12.6 us
    ppermute x1, waiting for transfers between devices, along_line(): outer_one = lax.ppermute(middle_one, 'sp', outward_pairs)  9.51 us
    ppermute x3, waiting for transfers between devices, swap_both(): return lax.ppermute(array, ('sp', 'tp'), pairs)  5.22 us
    ppermute x3, starting transfers between devices, swap_both(): return lax.ppermute(array, ('sp', 'tp'), pairs)  3.46 us
  transfers between devices with their start and end apart: 29, of which 20 were waited for; matrix products, arithmetic and copies ran while one was open for 0% of the time, Pallas kernels for 5%

profile of v1, /device:TPU:0, one launch (start us, length us, event | category | flops | bytes accessed | tf_op | source)
XLA Modules:
  0.0 124.8 jit_solution(17804417611946083482)
XLA Ops:
  0.0 1.3 %shard_map.127 = (bf16[4,128,384]{2,1,0:T(8,128)(2,1)S(1)}, f32[2,128]{1,0:T(2,128)S(1)}) custom-call(bf16[128,256]{1,0:T(8,128)(2,1)} %refs_0_.1, bf16[128,256]{1,0:T(8,128)(2,1)} %refs_1_.1, bf16[128,256]{1,0:T(8,128)(2,1)} %refs_2_.1, bf16[128,256]{1,0:T(8,128)(2,1)} %refs_3_.1, bf16[128,512]{1,0:T(8,128)(2,1)} %refs_4_.1, f32[1,128]{1,0:T(1,128)} %bitcast.29, ...), custom_call_target="tpu_custom_call" | custom-call | tf_op jit(solution)/shard_map/pallas_call | solution.py:298
  1.4 3.1 %collective-permute-start = (bf16[128,384]{1,0:T(8,128)(2,1)S(1)}, bf16[128,384]{1,0:T(8,128)(2,1)S(1)}, u32[]{:S(2)}, u32[]{:S(2)}) collective-permute-start(bf16[128,384]{1,0:T(8,128)(2,1)S(1)} %get-tuple-element.25), channel_id=1, source_target_pairs={{0,8},{4,12},{8,0},{12,4},{16,24},{20,28},{24,16},{28,20},{1,9},{5... | collective-permute-start | bytes 294920 | tf_op jit(solution)/shard_map/ppermute | solution.py:329
  4.5 2.5 %collective-permute-start.2 = (bf16[128,384]{1,0:T(8,128)(2,1)S(1)}, bf16[128,384]{1,0:T(8,128)(2,1)S(1)}, u32[]{:S(2)}, u32[]{:S(2)}) collective-permute-start(bf16[128,384]{1,0:T(8,128)(2,1)S(1)} %get-tuple-element.23), channel_id=1, source_target_pairs={{0,24},{4,28},{8,16},{12,20},{16,8},{20,12},{24,0},{28,4},{1,25},{... | collective-permute-start | bytes 294920 | tf_op jit(solution)/shard_map/ppermute | solution.py:329
  7.0 0.1 collective-permute-start.1
  7.1 0.2 collective-permute-done.b_ref
  7.3 1.8 %collective-permute-start.3 = (bf16[256,256]{1,0:T(8,128)(2,1)S(1)}, bf16[256,256]{1,0:T(8,128)(2,1)S(1)}, u32[]{:S(2)}, u32[]{:S(2)}) collective-permute-start(bf16[256,256]{1,0:T(8,128)(2,1)S(1)} %pad_maximum_fusion.1), channel_id=1, source_target_pairs={{0,4},{4,0},{8,12},{12,8},{16,20},{20,16},{24,28},{28,24},{1,5},{5... | collective-permute-start | bytes 393224 | tf_op jit(solution)/shard_map/ppermute | solution.py:329
  9.1 3.5 %collective-permute-done.2.d_ref = bf16[128,384]{1,0:T(8,128)(2,1)S(1)} collective-permute-done((bf16[128,384]{1,0:T(8,128)(2,1)S(1)}, bf16[128,384]{1,0:T(8,128)(2,1)S(1)}, u32[]{:S(2)}, u32[]{:S(2)}) %collective-permute-start.2) | collective-permute-done | bytes 98336 | tf_op jit(solution)/shard_map/ppermute | solution.py:329
  12.7 3.3 %collective-permute-done.1.c_ref = bf16[128,384]{1,0:T(8,128)(2,1)S(1)} collective-permute-done((bf16[128,384]{1,0:T(8,128)(2,1)S(1)}, bf16[128,384]{1,0:T(8,128)(2,1)S(1)}, u32[]{:S(2)}, u32[]{:S(2)}) %collective-permute-start.1) | collective-permute-done | bytes 98336 | tf_op jit(solution)/shard_map/ppermute | solution.py:329
  15.9 1.6 %collective-permute-start.4 = (bf16[256,256]{1,0:T(8,128)(2,1)S(1)}, bf16[256,256]{1,0:T(8,128)(2,1)S(1)}, u32[]{:S(2)}, u32[]{:S(2)}) collective-permute-start(bf16[256,256]{1,0:T(8,128)(2,1)S(1)} %pad_maximum_fusion.2), channel_id=1, source_target_pairs={{0,4},{4,0},{8,12},{12,8},{16,20},{20,16},{24,28},{28,24},{1,5},{5... | collective-permute-start | bytes 393224 | tf_op jit(solution)/shard_map/ppermute | solution.py:329
  17.5 0.0 collective-permute-done.3.ab_ref
  17.5 3.5 %collective-permute-done.4.cd_ref = bf16[256,256]{1,0:T(8,128)(2,1)S(1)} collective-permute-done((bf16[256,256]{1,0:T(8,128)(2,1)S(1)}, bf16[256,256]{1,0:T(8,128)(2,1)S(1)}, u32[]{:S(2)}, u32[]{:S(2)}) %collective-permute-start.4) | collective-permute-done | bytes 131104 | tf_op jit(solution)/shard_map/ppermute | solution.py:329
  21.0 3.2 %shard_map.128 = bf16[4,128,128]{2,1,0:T(8,128)(2,1)S(1)} custom-call(f32[2,128]{1,0:T(2,128)S(1)} %get-tuple-element.11.extra_ref, bf16[128,384]{1,0:T(8,128)(2,1)S(1)} %get-tuple-element.26.a_ref, bf16[128,384]{1,0:T(8,128)(2,1)S(1)} %collective-permute-done.b_ref, bf16[128,384]{1,0:T(8,128)(2,1)S(1)} %collective-permute-done.1.c_ref, ...), custom_call_target="tpu_custom_call" | custom-call | tf_op jit(solution)/shard_map/pallas_call | solution.py:298
  24.2 0.1 collective-permute-start.7
  24.3 3.2 %collective-permute-start.6 = (bf16[128,128]{1,0:T(8,128)(2,1)S(1)}, bf16[128,128]{1,0:T(8,128)(2,1)S(1)}, u32[]{:S(2)}, u32[]{:S(2)}) collective-permute-start(bf16[128,128]{1,0:T(8,128)(2,1)S(1)} %get-tuple-element.62), channel_id=1, source_target_pairs={{0,16},{4,20},{8,24},{12,28},{16,0},{20,4},{24,8},{28,12},{1,17},{... | collective-permute-start | bytes 98312 | tf_op jit(solution)/shard_map/ppermute | solution.py:329
  27.5 1.2 collective-permute-start.5
  28.7 0.4 collective-permute-start.10
  29.0 2.8 %collective-permute-start.9 = (bf16[256,512]{1,0:T(8,128)(2,1)}, bf16[256,512]{1,0:T(8,128)(2,1)S(1)}, u32[]{:S(2)}, u32[]{:S(2)}) collective-permute-start(bf16[256,512]{1,0:T(8,128)(2,1)} %source.1), channel_id=1, source_target_pairs={{0,8},{4,12},{8,0},{12,4},{16,24},{20,28},{24,16},{28,20},{1,9},{5... | collective-permute-start | bytes 786440 | tf_op jit(solution)/shard_map/ppermute | solution.py:329
  31.9 1.2 collective-permute-start.11
  33.1 0.5 collective-permute-done.5
  33.6 1.6 %collective-permute-start.8 = (bf16[128,512]{1,0:T(8,128)(2,1)S(1)}, bf16[128,512]{1,0:T(8,128)(2,1)S(1)}, u32[]{:S(2)}, u32[]{:S(2)}) collective-permute-start(bf16[128,512]{1,0:T(8,128)(2,1)S(1)} %pad_maximum_fusion.3.own_ref), channel_id=1, source_target_pairs={{0,4},{4,0},{8,12},{12,8},{16,20},{20,16},{24,28},{28,24},{1,5},{5... | collective-permute-start | bytes 393224 | tf_op jit(solution)/shard_map/ppermute | solution.py:329
  35.1 12.9 %collective-permute-done.10.c_ref = bf16[256,512]{1,0:T(8,128)(2,1)S(1)} collective-permute-done((bf16[256,512]{1,0:T(8,128)(2,1)}, bf16[256,512]{1,0:T(8,128)(2,1)S(1)}, u32[]{:S(2)}, u32[]{:S(2)}) %collective-permute-start.10) | collective-permute-done | bytes 262176 | tf_op jit(solution)/shard_map/ppermute | solution.py:329
  48.0 0.0 collective-permute-done.11.d_ref
  48.0 0.0 collective-permute-done.8.other_ref
  48.0 1.3 %shard_map.129 = (f32[128,1024]{1,0:T(8,128)S(1)}, bf16[128,1024]{1,0:T(8,128)(2,1)S(1)}) custom-call(bf16[128,512]{1,0:T(8,128)(2,1)S(1)} %pad_maximum_fusion.3.own_ref, bf16[128,512]{1,0:T(8,128)(2,1)S(1)} %collective-permute-done.8.other_ref, bf16[256,512]{1,0:T(8,128)(2,1)S(1)} %collective-permute-done.9.b_ref, ...), custom_call_target="tpu_custom_call" | custom-call | tf_op jit(solution)/shard_map/pallas_call | solution.py:298
  49.3 0.1 collective-permute-start.12
  49.4 1.5 %collective-permute-done.12 = bf16[128,1024]{1,0:T(8,128)(2,1)S(1)} collective-permute-done((bf16[128,1024]{1,0:T(8,128)(2,1)S(1)}, bf16[128,1024]{1,0:T(8,128)(2,1)S(1)}, u32[]{:S(2)}, u32[]{:S(2)}) %collective-permute-start.12) | collective-permute-done | bytes 262176 | tf_op jit(solution)/shard_map/ppermute | solution.py:329
  50.9 0.1 fusion.17
  51.0 1.6 %collective-permute-start.15 = (bf16[32,1024]{1,0:T(8,128)(2,1)S(1)}, bf16[32,1024]{1,0:T(8,128)(2,1)S(1)}, u32[]{:S(2)}, u32[]{:S(2)}) collective-permute-start(bf16[32,1024]{1,0:T(8,128)(2,1)S(1)} %get-tuple-element.51), channel_id=1, source_target_pairs={{0,2},{1,3},{2,0},{3,1},{4,6},{5,7},{6,4},{7,5},{8,10},{9,11},{10,... | collective-permute-start | bytes 196616 | tf_op jit(solution)/shard_map/ppermute | solution.py:329
  52.6 5.8 %collective-permute-start.20 = (bf16[256,1408]{1,0:T(8,128)(2,1)S(1)}, bf16[256,1408]{1,0:T(8,128)(2,1)S(1)}, u32[]{:S(2)}, u32[]{:S(2)}) collective-permute-start(bf16[256,1408]{1,0:T(8,128)(2,1)S(1)} %copy-done), channel_id=1, source_target_pairs={{0,8},{4,12},{8,0},{12,4},{16,24},{20,28},{24,16},{28,20},{1,9},{5... | collective-permute-start | bytes 2162696 | tf_op jit(solution)/shard_map/ppermute | solution.py:329
  58.4 0.7 collective-permute-start.21
  59.1 1.6 %collective-permute-start.13 = (bf16[32,1024]{1,0:T(8,128)(2,1)S(1)}, bf16[32,1024]{1,0:T(8,128)(2,1)S(1)}, u32[]{:S(2)}, u32[]{:S(2)}) collective-permute-start(bf16[32,1024]{1,0:T(8,128)(2,1)S(1)} %get-tuple-element.50), channel_id=1, source_target_pairs={{0,4},{4,0},{8,12},{12,8},{16,20},{20,16},{24,28},{28,24},{1,5},{5... | collective-permute-start | bytes 196616 | tf_op jit(solution)/shard_map/ppermute | solution.py:329
  60.7 0.5 collective-permute-start.14
  61.1 0.0 collective-permute-done.15
  61.1 2.7 %collective-permute-done.13 = bf16[32,1024]{1,0:T(8,128)(2,1)S(1)} collective-permute-done((bf16[32,1024]{1,0:T(8,128)(2,1)S(1)}, bf16[32,1024]{1,0:T(8,128)(2,1)S(1)}, u32[]{:S(2)}, u32[]{:S(2)}) %collective-permute-start.13) | collective-permute-done | bytes 65568 | tf_op jit(solution)/shard_map/ppermute | solution.py:329
  63.9 1.9 %collective-permute-done.14 = bf16[32,1024]{1,0:T(8,128)(2,1)S(1)} collective-permute-done((bf16[32,1024]{1,0:T(8,128)(2,1)S(1)}, bf16[32,1024]{1,0:T(8,128)(2,1)S(1)}, u32[]{:S(2)}, u32[]{:S(2)}) %collective-permute-start.14) | collective-permute-done | bytes 65568 | tf_op jit(solution)/shard_map/ppermute | solution.py:337
  65.9 0.2 fusion
  66.1 8.5 %collective-permute-done.20.near_ref = bf16[256,1408]{1,0:T(8,128)(2,1)S(1)} collective-permute-done((bf16[256,1408]{1,0:T(8,128)(2,1)S(1)}, bf16[256,1408]{1,0:T(8,128)(2,1)S(1)}, u32[]{:S(2)}, u32[]{:S(2)}) %collective-permute-start.20) | collective-permute-done | bytes 720928 | tf_op jit(solution)/shard_map/ppermute | solution.py:329
  74.6 0.7 collective-permute-start.23
  75.3 0.1 fusion.2
  75.4 1.5 %collective-permute-start.18 = (bf16[32,2048]{1,0:T(8,128)(2,1)S(1)}, bf16[32,2048]{1,0:T(8,128)(2,1)S(1)}, u32[]{:S(2)}, u32[]{:S(2)}) collective-permute-start(bf16[32,2048]{1,0:T(8,128)(2,1)S(1)} %fusion.2), channel_id=1, source_target_pairs={{0,6},{1,7},{2,4},{3,5},{4,2},{5,3},{6,0},{7,1},{8,14},{9,15},{10,... | collective-permute-start | bytes 393224 | tf_op jit(solution)/shard_map/ppermute | solution.py:337
  76.9 0.5 collective-permute-start.17
  77.4 1.5 %collective-permute-start.16 = (bf16[32,2048]{1,0:T(8,128)(2,1)S(1)}, bf16[32,2048]{1,0:T(8,128)(2,1)S(1)}, u32[]{:S(2)}, u32[]{:S(2)}) collective-permute-start(bf16[32,2048]{1,0:T(8,128)(2,1)S(1)} %fusion.2), channel_id=1, source_target_pairs={{0,2},{1,3},{2,0},{3,1},{4,6},{5,7},{6,4},{7,5},{8,10},{9,11},{10,... | collective-permute-start | bytes 393224 | tf_op jit(solution)/shard_map/ppermute | solution.py:329
  78.9 0.0 collective-permute-done.21.third_inner_ref
  78.9 1.3 %collective-permute-start.22 = (bf16[256,1408]{1,0:T(8,128)(2,1)S(1)}, bf16[256,1408]{1,0:T(8,128)(2,1)S(1)}, u32[]{:S(2)}, u32[]{:S(2)}) collective-permute-start(bf16[256,1408]{1,0:T(8,128)(2,1)S(1)} %collective-permute-done.21.third_inner_ref), channel_id=1, source_target_pairs={{8,0},{12,4},{16,24},{20,28},{9,1},{13,5},{17,25},{21,29},{10,2},{... | collective-permute-start | bytes 2162696 | tf_op jit(solution)/shard_map/ppermute | solution.py:352
  80.2 1.3 %collective-permute-start.24 = (bf16[256,1408]{1,0:T(8,128)(2,1)S(1)}, bf16[256,1408]{1,0:T(8,128)(2,1)S(1)}, u32[]{:S(2)}, u32[]{:S(2)}) collective-permute-start(bf16[256,1408]{1,0:T(8,128)(2,1)S(1)} %collective-permute-done.23.last_inner_ref), channel_id=1, source_target_pairs={{8,0},{12,4},{16,24},{20,28},{9,1},{13,5},{17,25},{21,29},{10,2},{... | collective-permute-start | bytes 2162696 | tf_op jit(solution)/shard_map/ppermute | solution.py:353
  81.5 0.9 collective-permute-done.18
  82.4 0.4 collective-permute-done.17
  82.9 1.0 collective-permute-done.16
  83.9 0.1 collective-permute-start.19
  84.0 1.9 %collective-permute-done.19.there_ref = bf16[128,2048]{1,0:T(8,128)(2,1)S(1)} collective-permute-done((bf16[128,2048]{1,0:T(8,128)(2,1)S(1)}, bf16[128,2048]{1,0:T(8,128)(2,1)S(1)}, u32[]{:S(2)}, u32[]{:S(2)}) %collective-permute-start.19) | collective-permute-done | bytes 524320 | tf_op jit(solution)/shard_map/ppermute | solution.py:329
  85.9 6.0 %shard_map.130.hidden_ref = bf16[256,1408]{1,0:T(8,128)(2,1)S(1)} custom-call(bf16[128,2048]{1,0:T(8,128)(2,1)S(1)} %pad_maximum_fusion.here_ref, bf16[128,2048]{1,0:T(8,128)(2,1)S(1)} %collective-permute-done.19.there_ref, bf16[2048,1408]{1,0:T(8,128)(2,1)} %gate_ref.1, bf16[2048,1408]{1,0:T(8,128)(2,1)} %up_ref.1), custom_call_target="tpu_custom_call" | custom-call | tf_op jit(solution)/shard_map/pallas_call | solution.py:298
  91.9 9.5 %collective-permute-done.22.third_outer_ref = bf16[256,1408]{1,0:T(8,128)(2,1)S(1)} collective-permute-done((bf16[256,1408]{1,0:T(8,128)(2,1)S(1)}, bf16[256,1408]{1,0:T(8,128)(2,1)S(1)}, u32[]{:S(2)}, u32[]{:S(2)}) %collective-permute-start.22) | collective-permute-done | bytes 720928 | tf_op jit(solution)/shard_map/ppermute | solution.py:352
  101.4 12.6 %collective-permute-done.24.last_outer_ref = bf16[256,1408]{1,0:T(8,128)(2,1)S(1)} collective-permute-done((bf16[256,1408]{1,0:T(8,128)(2,1)S(1)}, bf16[256,1408]{1,0:T(8,128)(2,1)S(1)}, u32[]{:S(2)}, u32[]{:S(2)}) %collective-permute-start.24) | collective-permute-done | bytes 720928 | tf_op jit(solution)/shard_map/ppermute | solution.py:353
  114.1 1.0 shard_map.131
  115.1 0.1 collective-permute-start.25
  115.1 1.5 %collective-permute-done.25 = bf16[128,1024]{1,0:T(8,128)(2,1)S(1)} collective-permute-done((bf16[128,1024]{1,0:T(8,128)(2,1)S(1)}, bf16[128,1024]{1,0:T(8,128)(2,1)S(1)}, u32[]{:S(2)}, u32[]{:S(2)}) %collective-permute-start.25) | collective-permute-done | bytes 262176 | tf_op jit(solution)/shard_map/ppermute | solution.py:329
  116.7 0.1 fusion.15
  116.8 0.6 collective-permute-start.28
  117.3 1.5 %collective-permute-start.26 = (bf16[32,1024]{1,0:T(8,128)(2,1)S(1)}, bf16[32,1024]{1,0:T(8,128)(2,1)S(1)}, u32[]{:S(2)}, u32[]{:S(2)}) collective-permute-start(bf16[32,1024]{1,0:T(8,128)(2,1)S(1)} %get-tuple-element.35), channel_id=1, source_target_pairs={{0,4},{4,0},{8,12},{12,8},{16,20},{20,16},{24,28},{28,24},{1,5},{5... | collective-permute-start | bytes 196616 | tf_op jit(solution)/shard_map/ppermute | solution.py:329
  118.8 1.5 %collective-permute-start.27 = (bf16[32,1024]{1,0:T(8,128)(2,1)S(1)}, bf16[32,1024]{1,0:T(8,128)(2,1)S(1)}, u32[]{:S(2)}, u32[]{:S(2)}) collective-permute-start(bf16[32,1024]{1,0:T(8,128)(2,1)S(1)} %get-tuple-element.37), channel_id=1, source_target_pairs={{0,6},{1,7},{2,4},{3,5},{4,2},{5,3},{6,0},{7,1},{8,14},{9,15},{10,... | collective-permute-start | bytes 196616 | tf_op jit(solution)/shard_map/ppermute | solution.py:337
  120.3 0.8 collective-permute-done.28
  121.1 0.5 collective-permute-done.26
  121.6 2.4 %collective-permute-done.27 = bf16[32,1024]{1,0:T(8,128)(2,1)S(1)} collective-permute-done((bf16[32,1024]{1,0:T(8,128)(2,1)S(1)}, bf16[32,1024]{1,0:T(8,128)(2,1)S(1)}, u32[]{:S(2)}, u32[]{:S(2)}) %collective-permute-start.27) | collective-permute-done | bytes 65568 | tf_op jit(solution)/shard_map/ppermute | solution.py:337
  124.1 0.7 fusion.3
  (34 shorter events, 0.4 us)
Async XLA Ops:
  0.0 52.6 %copy-start = (bf16[256,1408]{1,0:T(8,128)(2,1)S(1)}, bf16[256,1408]{1,0:T(8,128)(2,1)}, u32[]{:S(2)}) copy-start(bf16[256,1408]{1,0:T(8,128)(2,1)} %own_ref.1) | copy-start | bytes 2162692
  0.0 65.9 %copy-start.1 = (bf16[32,2048]{1,0:T(8,128)(2,1)S(1)}, bf16[32,2048]{1,0:T(8,128)(2,1)}, u32[]{:S(2)}) copy-start(bf16[32,2048]{1,0:T(8,128)(2,1)} %param.13) | copy-start | bytes 393220
  0.0 75.3 %copy-start.2 = (f32[2048]{0:T(1024)S(1)}, f32[2048]{0:T(1024)}, u32[]{:S(2)}) copy-start(f32[2048]{0:T(1024)} %param.22) | copy-start | bytes 24580
  1.4 5.9 %collective-permute-start = (bf16[128,384]{1,0:T(8,128)(2,1)S(1)}, bf16[128,384]{1,0:T(8,128)(2,1)S(1)}, u32[]{:S(2)}, u32[]{:S(2)}) collective-permute-start(bf16[128,384]{1,0:T(8,128)(2,1)S(1)} %get-tuple-element.25), channel_id=1, source_target_pairs={{0,8},{4,12},{8,0},{12,4},{16,24},{20,28},{24,16},{28,20},{1,9},{5... | collective-permute-start | bytes 294920 | tf_op jit(solution)/shard_map/ppermute | solution.py:329
  4.5 8.2 %collective-permute-start.2 = (bf16[128,384]{1,0:T(8,128)(2,1)S(1)}, bf16[128,384]{1,0:T(8,128)(2,1)S(1)}, u32[]{:S(2)}, u32[]{:S(2)}) collective-permute-start(bf16[128,384]{1,0:T(8,128)(2,1)S(1)} %get-tuple-element.23), channel_id=1, source_target_pairs={{0,24},{4,28},{8,16},{12,20},{16,8},{20,12},{24,0},{28,4},{1,25},{... | collective-permute-start | bytes 294920 | tf_op jit(solution)/shard_map/ppermute | solution.py:329
  7.0 8.9 %collective-permute-start.1 = (bf16[128,384]{1,0:T(8,128)(2,1)S(1)}, bf16[128,384]{1,0:T(8,128)(2,1)S(1)}, u32[]{:S(2)}, u32[]{:S(2)}) collective-permute-start(bf16[128,384]{1,0:T(8,128)(2,1)S(1)} %get-tuple-element.24), channel_id=1, source_target_pairs={{0,16},{4,20},{8,24},{12,28},{16,0},{20,4},{24,8},{28,12},{1,17},{... | collective-permute-start | bytes 294920 | tf_op jit(solution)/shard_map/ppermute | solution.py:329
  7.3 10.2 %collective-permute-start.3 = (bf16[256,256]{1,0:T(8,128)(2,1)S(1)}, bf16[256,256]{1,0:T(8,128)(2,1)S(1)}, u32[]{:S(2)}, u32[]{:S(2)}) collective-permute-start(bf16[256,256]{1,0:T(8,128)(2,1)S(1)} %pad_maximum_fusion.1), channel_id=1, source_target_pairs={{0,4},{4,0},{8,12},{12,8},{16,20},{20,16},{24,28},{28,24},{1,5},{5... | collective-permute-start | bytes 393224 | tf_op jit(solution)/shard_map/ppermute | solution.py:329
  15.9 5.0 %collective-permute-start.4 = (bf16[256,256]{1,0:T(8,128)(2,1)S(1)}, bf16[256,256]{1,0:T(8,128)(2,1)S(1)}, u32[]{:S(2)}, u32[]{:S(2)}) collective-permute-start(bf16[256,256]{1,0:T(8,128)(2,1)S(1)} %pad_maximum_fusion.2), channel_id=1, source_target_pairs={{0,4},{4,0},{8,12},{12,8},{16,20},{20,16},{24,28},{28,24},{1,5},{5... | collective-permute-start | bytes 393224 | tf_op jit(solution)/shard_map/ppermute | solution.py:329
  24.2 7.7 %collective-permute-start.7 = (bf16[128,128]{1,0:T(8,128)(2,1)S(1)}, bf16[128,128]{1,0:T(8,128)(2,1)S(1)}, u32[]{:S(2)}, u32[]{:S(2)}) collective-permute-start(bf16[128,128]{1,0:T(8,128)(2,1)S(1)} %get-tuple-element.61), channel_id=1, source_target_pairs={{0,8},{4,12},{8,0},{12,4},{16,24},{20,28},{24,16},{28,20},{1,9},{5... | collective-permute-start | bytes 98312 | tf_op jit(solution)/shard_map/ppermute | solution.py:329
  24.3 8.8 %collective-permute-start.6 = (bf16[128,128]{1,0:T(8,128)(2,1)S(1)}, bf16[128,128]{1,0:T(8,128)(2,1)S(1)}, u32[]{:S(2)}, u32[]{:S(2)}) collective-permute-start(bf16[128,128]{1,0:T(8,128)(2,1)S(1)} %get-tuple-element.62), channel_id=1, source_target_pairs={{0,16},{4,20},{8,24},{12,28},{16,0},{20,4},{24,8},{28,12},{1,17},{... | collective-permute-start | bytes 98312 | tf_op jit(solution)/shard_map/ppermute | solution.py:329
  27.5 6.1 %collective-permute-start.5 = (bf16[128,128]{1,0:T(8,128)(2,1)S(1)}, bf16[128,128]{1,0:T(8,128)(2,1)S(1)}, u32[]{:S(2)}, u32[]{:S(2)}) collective-permute-start(bf16[128,128]{1,0:T(8,128)(2,1)S(1)} %get-tuple-element.63), channel_id=1, source_target_pairs={{0,24},{4,28},{8,16},{12,20},{16,8},{20,12},{24,0},{28,4},{1,25},{... | collective-permute-start | bytes 98312 | tf_op jit(solution)/shard_map/ppermute | solution.py:329
  28.7 19.4 %collective-permute-start.10 = (bf16[256,512]{1,0:T(8,128)(2,1)}, bf16[256,512]{1,0:T(8,128)(2,1)S(1)}, u32[]{:S(2)}, u32[]{:S(2)}) collective-permute-start(bf16[256,512]{1,0:T(8,128)(2,1)} %source.1), channel_id=1, source_target_pairs={{0,16},{4,20},{8,24},{12,28},{16,0},{20,4},{24,8},{28,12},{1,17},{... | collective-permute-start | bytes 786440 | tf_op jit(solution)/shard_map/ppermute | solution.py:329
  29.0 19.0 %collective-permute-start.9 = (bf16[256,512]{1,0:T(8,128)(2,1)}, bf16[256,512]{1,0:T(8,128)(2,1)S(1)}, u32[]{:S(2)}, u32[]{:S(2)}) collective-permute-start(bf16[256,512]{1,0:T(8,128)(2,1)} %source.1), channel_id=1, source_target_pairs={{0,8},{4,12},{8,0},{12,4},{16,24},{20,28},{24,16},{28,20},{1,9},{5... | collective-permute-start | bytes 786440 | tf_op jit(solution)/shard_map/ppermute | solution.py:329
  31.9 16.1 %collective-permute-start.11 = (bf16[256,512]{1,0:T(8,128)(2,1)}, bf16[256,512]{1,0:T(8,128)(2,1)S(1)}, u32[]{:S(2)}, u32[]{:S(2)}) collective-permute-start(bf16[256,512]{1,0:T(8,128)(2,1)} %source.1), channel_id=1, source_target_pairs={{0,24},{4,28},{8,16},{12,20},{16,8},{20,12},{24,0},{28,4},{1,25},{... | collective-permute-start | bytes 786440 | tf_op jit(solution)/shard_map/ppermute | solution.py:329
  33.6 14.4 %collective-permute-start.8 = (bf16[128,512]{1,0:T(8,128)(2,1)S(1)}, bf16[128,512]{1,0:T(8,128)(2,1)S(1)}, u32[]{:S(2)}, u32[]{:S(2)}) collective-permute-start(bf16[128,512]{1,0:T(8,128)(2,1)S(1)} %pad_maximum_fusion.3.own_ref), channel_id=1, source_target_pairs={{0,4},{4,0},{8,12},{12,8},{16,20},{20,16},{24,28},{28,24},{1,5},{5... | collective-permute-start | bytes 393224 | tf_op jit(solution)/shard_map/ppermute | solution.py:329
  49.3 1.6 %collective-permute-start.12 = (bf16[128,1024]{1,0:T(8,128)(2,1)S(1)}, bf16[128,1024]{1,0:T(8,128)(2,1)S(1)}, u32[]{:S(2)}, u32[]{:S(2)}) collective-permute-start(bf16[128,1024]{1,0:T(8,128)(2,1)S(1)} %get-tuple-element.14), channel_id=1, source_target_pairs={{0,1},{1,0},{2,3},{3,2},{4,5},{5,4},{6,7},{7,6},{8,9},{9,8},{10,11... | collective-permute-start | bytes 786440 | tf_op jit(solution)/shard_map/ppermute | solution.py:329
  51.0 10.1 %collective-permute-start.15 = (bf16[32,1024]{1,0:T(8,128)(2,1)S(1)}, bf16[32,1024]{1,0:T(8,128)(2,1)S(1)}, u32[]{:S(2)}, u32[]{:S(2)}) collective-permute-start(bf16[32,1024]{1,0:T(8,128)(2,1)S(1)} %get-tuple-element.51), channel_id=1, source_target_pairs={{0,2},{1,3},{2,0},{3,1},{4,6},{5,7},{6,4},{7,5},{8,10},{9,11},{10,... | collective-permute-start | bytes 196616 | tf_op jit(solution)/shard_map/ppermute | solution.py:329
  52.6 22.0 %collective-permute-start.20 = (bf16[256,1408]{1,0:T(8,128)(2,1)S(1)}, bf16[256,1408]{1,0:T(8,128)(2,1)S(1)}, u32[]{:S(2)}, u32[]{:S(2)}) collective-permute-start(bf16[256,1408]{1,0:T(8,128)(2,1)S(1)} %copy-done), channel_id=1, source_target_pairs={{0,8},{4,12},{8,0},{12,4},{16,24},{20,28},{24,16},{28,20},{1,9},{5... | collective-permute-start | bytes 2162696 | tf_op jit(solution)/shard_map/ppermute | solution.py:329
  58.4 20.5 %collective-permute-start.21 = (bf16[256,1408]{1,0:T(8,128)(2,1)S(1)}, bf16[256,1408]{1,0:T(8,128)(2,1)S(1)}, u32[]{:S(2)}, u32[]{:S(2)}) collective-permute-start(bf16[256,1408]{1,0:T(8,128)(2,1)S(1)} %copy-done), channel_id=1, source_target_pairs={{8,16},{12,20},{16,8},{20,12},{9,17},{13,21},{17,9},{21,13},{10,18... | collective-permute-start | bytes 2162696 | tf_op jit(solution)/shard_map/ppermute | solution.py:350
  59.1 4.8 %collective-permute-start.13 = (bf16[32,1024]{1,0:T(8,128)(2,1)S(1)}, bf16[32,1024]{1,0:T(8,128)(2,1)S(1)}, u32[]{:S(2)}, u32[]{:S(2)}) collective-permute-start(bf16[32,1024]{1,0:T(8,128)(2,1)S(1)} %get-tuple-element.50), channel_id=1, source_target_pairs={{0,4},{4,0},{8,12},{12,8},{16,20},{20,16},{24,28},{28,24},{1,5},{5... | collective-permute-start | bytes 196616 | tf_op jit(solution)/shard_map/ppermute | solution.py:329
  60.7 5.2 %collective-permute-start.14 = (bf16[32,1024]{1,0:T(8,128)(2,1)S(1)}, bf16[32,1024]{1,0:T(8,128)(2,1)S(1)}, u32[]{:S(2)}, u32[]{:S(2)}) collective-permute-start(bf16[32,1024]{1,0:T(8,128)(2,1)S(1)} %get-tuple-element.52), channel_id=1, source_target_pairs={{0,6},{1,7},{2,4},{3,5},{4,2},{5,3},{6,0},{7,1},{8,14},{9,15},{10,... | collective-permute-start | bytes 196616 | tf_op jit(solution)/shard_map/ppermute | solution.py:337
  74.6 5.7 %collective-permute-start.23 = (bf16[256,1408]{1,0:T(8,128)(2,1)S(1)}, bf16[256,1408]{1,0:T(8,128)(2,1)S(1)}, u32[]{:S(2)}, u32[]{:S(2)}) collective-permute-start(bf16[256,1408]{1,0:T(8,128)(2,1)S(1)} %collective-permute-done.20.near_ref), channel_id=1, source_target_pairs={{8,16},{12,20},{16,8},{20,12},{9,17},{13,21},{17,9},{21,13},{10,18... | collective-permute-start | bytes 2162696 | tf_op jit(solution)/shard_map/ppermute | solution.py:351
  75.4 7.1 %collective-permute-start.18 = (bf16[32,2048]{1,0:T(8,128)(2,1)S(1)}, bf16[32,2048]{1,0:T(8,128)(2,1)S(1)}, u32[]{:S(2)}, u32[]{:S(2)}) collective-permute-start(bf16[32,2048]{1,0:T(8,128)(2,1)S(1)} %fusion.2), channel_id=1, source_target_pairs={{0,6},{1,7},{2,4},{3,5},{4,2},{5,3},{6,0},{7,1},{8,14},{9,15},{10,... | collective-permute-start | bytes 393224 | tf_op jit(solution)/shard_map/ppermute | solution.py:337
  76.9 6.0 %collective-permute-start.17 = (bf16[32,2048]{1,0:T(8,128)(2,1)S(1)}, bf16[32,2048]{1,0:T(8,128)(2,1)S(1)}, u32[]{:S(2)}, u32[]{:S(2)}) collective-permute-start(bf16[32,2048]{1,0:T(8,128)(2,1)S(1)} %fusion.2), channel_id=1, source_target_pairs={{0,4},{4,0},{8,12},{12,8},{16,20},{20,16},{24,28},{28,24},{1,5},{5... | collective-permute-start | bytes 393224 | tf_op jit(solution)/shard_map/ppermute | solution.py:329
  77.4 6.4 %collective-permute-start.16 = (bf16[32,2048]{1,0:T(8,128)(2,1)S(1)}, bf16[32,2048]{1,0:T(8,128)(2,1)S(1)}, u32[]{:S(2)}, u32[]{:S(2)}) collective-permute-start(bf16[32,2048]{1,0:T(8,128)(2,1)S(1)} %fusion.2), channel_id=1, source_target_pairs={{0,2},{1,3},{2,0},{3,1},{4,6},{5,7},{6,4},{7,5},{8,10},{9,11},{10,... | collective-permute-start | bytes 393224 | tf_op jit(solution)/shard_map/ppermute | solution.py:329
  78.9 22.5 %collective-permute-start.22 = (bf16[256,1408]{1,0:T(8,128)(2,1)S(1)}, bf16[256,1408]{1,0:T(8,128)(2,1)S(1)}, u32[]{:S(2)}, u32[]{:S(2)}) collective-permute-start(bf16[256,1408]{1,0:T(8,128)(2,1)S(1)} %collective-permute-done.21.third_inner_ref), channel_id=1, source_target_pairs={{8,0},{12,4},{16,24},{20,28},{9,1},{13,5},{17,25},{21,29},{10,2},{... | collective-permute-start | bytes 2162696 | tf_op jit(solution)/shard_map/ppermute | solution.py:352
  80.2 33.8 %collective-permute-start.24 = (bf16[256,1408]{1,0:T(8,128)(2,1)S(1)}, bf16[256,1408]{1,0:T(8,128)(2,1)S(1)}, u32[]{:S(2)}, u32[]{:S(2)}) collective-permute-start(bf16[256,1408]{1,0:T(8,128)(2,1)S(1)} %collective-permute-done.23.last_inner_ref), channel_id=1, source_target_pairs={{8,0},{12,4},{16,24},{20,28},{9,1},{13,5},{17,25},{21,29},{10,2},{... | collective-permute-start | bytes 2162696 | tf_op jit(solution)/shard_map/ppermute | solution.py:353
  83.9 2.0 %collective-permute-start.19 = (bf16[128,2048]{1,0:T(8,128)(2,1)S(1)}, bf16[128,2048]{1,0:T(8,128)(2,1)S(1)}, u32[]{:S(2)}, u32[]{:S(2)}) collective-permute-start(bf16[128,2048]{1,0:T(8,128)(2,1)S(1)} %pad_maximum_fusion.here_ref), channel_id=1, source_target_pairs={{0,1},{1,0},{2,3},{3,2},{4,5},{5,4},{6,7},{7,6},{8,9},{9,8},{10,11... | collective-permute-start | bytes 1572872 | tf_op jit(solution)/shard_map/ppermute | solution.py:329
  115.1 1.6 %collective-permute-start.25 = (bf16[128,1024]{1,0:T(8,128)(2,1)S(1)}, bf16[128,1024]{1,0:T(8,128)(2,1)S(1)}, u32[]{:S(2)}, u32[]{:S(2)}) collective-permute-start(bf16[128,1024]{1,0:T(8,128)(2,1)S(1)} %get-tuple-element.16), channel_id=1, source_target_pairs={{0,1},{1,0},{2,3},{3,2},{4,5},{5,4},{6,7},{7,6},{8,9},{9,8},{10,11... | collective-permute-start | bytes 786440 | tf_op jit(solution)/shard_map/ppermute | solution.py:329
  116.8 4.3 %collective-permute-start.28 = (bf16[32,1024]{1,0:T(8,128)(2,1)S(1)}, bf16[32,1024]{1,0:T(8,128)(2,1)S(1)}, u32[]{:S(2)}, u32[]{:S(2)}) collective-permute-start(bf16[32,1024]{1,0:T(8,128)(2,1)S(1)} %get-tuple-element.36), channel_id=1, source_target_pairs={{0,2},{1,3},{2,0},{3,1},{4,6},{5,7},{6,4},{7,5},{8,10},{9,11},{10,... | collective-permute-start | bytes 196616 | tf_op jit(solution)/shard_map/ppermute | solution.py:329
  117.3 4.3 %collective-permute-start.26 = (bf16[32,1024]{1,0:T(8,128)(2,1)S(1)}, bf16[32,1024]{1,0:T(8,128)(2,1)S(1)}, u32[]{:S(2)}, u32[]{:S(2)}) collective-permute-start(bf16[32,1024]{1,0:T(8,128)(2,1)S(1)} %get-tuple-element.35), channel_id=1, source_target_pairs={{0,4},{4,0},{8,12},{12,8},{16,20},{20,16},{24,28},{28,24},{1,5},{5... | collective-permute-start | bytes 196616 | tf_op jit(solution)/shard_map/ppermute | solution.py:329
  118.8 5.2 %collective-permute-start.27 = (bf16[32,1024]{1,0:T(8,128)(2,1)S(1)}, bf16[32,1024]{1,0:T(8,128)(2,1)S(1)}, u32[]{:S(2)}, u32[]{:S(2)}) collective-permute-start(bf16[32,1024]{1,0:T(8,128)(2,1)S(1)} %get-tuple-element.37), channel_id=1, source_target_pairs={{0,6},{1,7},{2,4},{3,5},{4,2},{5,3},{6,0},{7,1},{8,14},{9,15},{10,... | collective-permute-start | bytes 196616 | tf_op jit(solution)/shard_map/ppermute | solution.py:337

commit v2 on v1

--- a/solution.py
+++ b/solution.py
@@ -199,23 +199,29 @@
 
 
 def project_body(
-    own_ref, other_ref, b_ref, c_ref, d_ref, source, kept_ref, sent_ref, a_ref, sem, *, tp_size
+    a_ref, b_ref, c_ref, d_ref, other_ref, source, kept_ref, sent_ref, own_ref, heads_ref, sem, *, tp_size
 ):
-    copy = pltpu.make_async_copy(source, a_ref, sem)
+    copy = pltpu.make_async_copy(source, own_ref, sem)
     copy.start()
-    rows = own_ref.shape[0] // tp_size
-    width = a_ref.shape[0]
-    for index, ref in ((1, b_ref), (2, c_ref), (3, d_ref), (0, a_ref)):
+    here = lax.axis_index("sp") // 2
+    planes, tokens, size = a_ref.shape
+    for distance, ref in enumerate((a_ref, b_ref, c_ref, d_ref)):
+        columns = pl.ds(pl.multiple_of((here ^ distance) * size, size), size)
+        for block in range(planes):
+            heads_ref[block * tokens : (block + 1) * tokens, columns] = ref[distance ^ block]
+    rows = tokens // tp_size
+    width = own_ref.shape[0]
+    for index, ref in ((1, other_ref), (0, own_ref)):
         if index == 0:
             copy.wait()
         columns = slice(index * width, (index + 1) * width)
-        for side, left_ref in enumerate((own_ref, other_ref)):
-            product = lax.dot_general(
-                left_ref[...], ref[...], (((1,), (1,)), ((), ())), preferred_element_type=jnp.float32
-            )
+        product = lax.dot_general(
+            heads_ref[...], ref[...], (((1,), (1,)), ((), ())), preferred_element_type=jnp.float32
+        )
+        for block in range(planes):
             for chip in range(tp_size // 2):
-                to = slice((side * 2 + chip) * rows, (side * 2 + chip + 1) * rows)
-                at = chip * 2 * rows
+                to = slice((chip * planes + block) * rows, (chip * planes + block + 1) * rows)
+                at = block * tokens + chip * 2 * rows
                 kept_ref[to, columns] = product[at : at + rows]
                 sent_ref[to, columns] = product[at + rows : at + 2 * rows].astype(sent_ref.dtype)
 
@@ -252,32 +258,29 @@
         hidden_ref[:, start : start + gate.shape[1]] = hidden.astype(hidden_ref.dtype)
 
 
-def down_body(
-    hidden_ref,
-    own_ref,
-    near_ref,
-    third_inner_ref,
-    third_outer_ref,
-    last_inner_ref,
-    last_outer_ref,
-    kept_ref,
-    sent_ref,
-    *,
-    sp_size,
-):
+def down_body(hidden_ref, own_ref, *refs, sp_size):
+    parts, (kept_ref, sent_ref) = refs[:-2], refs[-2:]
+    parts = [parts[start : start + 5] for start in range(0, len(parts), 5)]
     place = lax.axis_index("sp") // 2
     inner = (place > 0) & (place < sp_size // 2 - 1)
     rows = kept_ref.shape[0]
     width = own_ref.shape[0]
+
+    def third(part):
+        return jnp.where(inner, part[1][...], part[2][...])
+
+    def last(part):
+        return jnp.where(inner, part[3][...], part[4][...])
+
     pieces = (
-        own_ref[...],
-        near_ref[...],
-        jnp.where(inner, third_inner_ref[...], third_outer_ref[...]),
-        jnp.where(inner, last_inner_ref[...], last_outer_ref[...]),
+        lambda: own_ref[...],
+        lambda: jnp.concatenate([part[0][...] for part in parts], axis=0),
+        lambda: jnp.concatenate([third(part) for part in parts], axis=0),
+        lambda: jnp.concatenate([last(part) for part in parts], axis=0),
     )
     for index, piece in enumerate(pieces):
         product = lax.dot_general(
-            hidden_ref[...], piece, (((1,), (1,)), ((), ())), preferred_element_type=jnp.float32
+            hidden_ref[...], piece(), (((1,), (1,)), ((), ())), preferred_element_type=jnp.float32
         )
         columns = slice(index * width, (index + 1) * width)
         kept_ref[:, columns] = product[:rows]
@@ -351,7 +354,7 @@
         middle_two = lax.ppermute(near_one, "sp", middle_pairs)
         outer_one = lax.ppermute(middle_one, "sp", outward_pairs)
         outer_two = lax.ppermute(middle_two, "sp", outward_pairs)
-        return weight, near_one, middle_one, outer_one, middle_two, outer_two
+        return near_one, middle_one, outer_one, middle_two, outer_two
 
     def planes_by_distance(n):
         n = [jnp.where(low, n[k ^ 1], n[k]) for k in range(4)]
@@ -365,6 +368,24 @@
             jnp.where(high, first, n[2]),
             jnp.where(high, second, n[3]),
         ]
+
+    def side_by_side(same, other):
+        return jnp.concatenate(
+            [jnp.where(on_side, other, same), jnp.where(on_side, same, other)], axis=1
+        )
+
+    def plane_sum(ours, given_away):
+        ours = ours + swap(given_away, "tp", core).astype(f32)
+        half_rows = ours.shape[0] // 2
+        from_chip = swap(ours[half_rows:].astype(bf16), "tp", chip)
+        ours = ours[:half_rows] + from_chip.astype(f32)
+        rows = half_rows // planes
+        blocks = [ours[k * rows : (k + 1) * rows] for k in range(planes)]
+        others = three(*(block.astype(bf16) for block in blocks[1:]))
+        blocks = [blocks[0], *(block.astype(f32) for block in others)]
+        middle = ours.shape[1] // 2
+        blocks = [side_by_side(block[:, :middle], block[:, middle:]) for block in blocks]
+        return jnp.concatenate(planes_by_distance(blocks), axis=1)
 
     def scatter_sum(ours, given_away, ordered):
         ours = ours + swap(given_away, "tp", core).astype(f32)
@@ -379,9 +400,7 @@
         joined = []
         for k in range(planes):
             a, b = (array[:, k * piece : (k + 1) * piece] for array in (same, other))
-            joined.append(
-                jnp.concatenate([jnp.where(on_side, b, a), jnp.where(on_side, a, b)], axis=1)
-            )
+            joined.append(side_by_side(a, b))
         return jnp.concatenate(ordered(joined), axis=1)
 
     tokens = query_first.shape[0]
@@ -417,20 +436,20 @@
             pltpu.VMEM((2 * planes * tokens, value_size), bf16),
         ],
     )
-    back = three(attended[1], attended[2], attended[3])
-    own_heads = jnp.concatenate(planes_by_distance([attended[0], *back]), axis=1)
-    other_heads = swap(own_heads, "sp", side)
-
-    half = (4 * rows, residual.shape[1] // 2)
-    halves = (jax.ShapeDtypeStruct(half, f32), jax.ShapeDtypeStruct(half, bf16))
+    width = residual.shape[1]
+    part = (planes * tokens // 2, width // planes)
     projected = kernel(
         functools.partial(project_body, tp_size=tp_size),
-        halves,
-        (own_heads, other_heads, *three(out_weight, out_weight, out_weight)),
+        (jax.ShapeDtypeStruct(part, f32), jax.ShapeDtypeStruct(part, bf16)),
+        (attended, *three(attended, attended, attended), swap(out_weight, "sp", side)),
         (out_weight,),
-        [pltpu.VMEM(out_weight.shape, bf16), pltpu.SemaphoreType.DMA],
-    )
-    summed = scatter_sum(*projected, planes_by_distance)
+        [
+            pltpu.VMEM(out_weight.shape, bf16),
+            pltpu.VMEM((planes * tokens, out_weight.shape[1]), bf16),
+            pltpu.SemaphoreType.DMA,
+        ],
+    )
+    summed = plane_sum(*projected)
     after_attention = (residual.astype(f32) + summed).astype(bf16)
     stream = after_attention.astype(f32)
     scaled_rows = stream * lax.rsqrt(jnp.mean(stream * stream, axis=-1, keepdims=True) + epsilon)
@@ -453,8 +472,13 @@
         + [pltpu.SemaphoreType.DMA((len(sizes),))],
         limit=24,
     )
+    half = (4 * rows, width // 2)
+    halves = (jax.ShapeDtypeStruct(half, f32), jax.ShapeDtypeStruct(half, bf16))
+    middle = down_weight.shape[0] // 2
     fed = kernel(
-        functools.partial(down_body, sp_size=sp_size), halves, (hidden, *along_line(down_weight))
+        functools.partial(down_body, sp_size=sp_size),
+        halves,
+        (hidden, down_weight, *along_line(down_weight[:middle]), *along_line(down_weight[middle:])),
     )
     return (stream + scatter_sum(*fed, planes_along_line)).astype(bf16)
 

time: 125 us -> 123 us (0.984)
  starting transfers between devices: 40.2 us -> 37.4 us
    ppermute x22, starting transfers between devices: 32.7 us -> 26.5 us  [swap(): return lax.ppermute(array, axis, [(i, i ^ distance) for i in range(count)])]
    ppermute x22, waiting for transfers between devices: 42.6 us -> 36.5 us  [swap(): return lax.ppermute(array, axis, [(i, i ^ distance) for i in range(count)])]
    ppermute x1 -> x2, waiting for transfers between devices: 9.51 us -> 15.6 us  [along_line(): outer_one = lax.ppermute(middle_one, 'sp', outward_pairs)]
    ppermute x1 -> x2, waiting for transfers between devices: 12.6 us -> 14 us  [along_line(): outer_two = lax.ppermute(middle_two, 'sp', outward_pairs)]
    ppermute x1 -> x2, starting transfers between devices: 1.28 us -> 2.58 us  [along_line(): outer_one = lax.ppermute(middle_one, 'sp', outward_pairs)]
    ppermute x1 -> x2, starting transfers between devices: 1.29 us -> 2.58 us  [along_line(): outer_two = lax.ppermute(middle_two, 'sp', outward_pairs)]
    ppermute x3 -> x2, waiting for transfers between devices: 5.22 us -> 4.32 us  [swap_both(): return lax.ppermute(array, ('sp', 'tp'), pairs)]
    ppermute x3 -> x2, starting transfers between devices: 3.46 us -> 2.99 us  [swap_both(): return lax.ppermute(array, ('sp', 'tp'), pairs)]
  transfers between devices with their start and end apart: 29 -> 32, of which waited for: 20 -> 19; matrix products, arithmetic and copies ran while one was open for 0% -> 0% of each run, Pallas kernels for 5% -> 8%
where the time goes in v2:
time: 123 us
  waiting for transfers between devices  70.3 us (57%)
  starting transfers between devices  37.4 us (30%)
  Pallas kernels  13.1 us (11%)
  other arithmetic  1.36 us (1%)
    ppermute x22, waiting for transfers between devices, swap(): return lax.ppermute(array, axis, [(i, i ^ distance) for i in range(count)])  36.5 us
    ppermute x22, starting transfers between devices, swap(): return lax.ppermute(array, axis, [(i, i ^ distance) for i in range(count)])  26.5 us
    ppermute x2, waiting for transfers between devices, along_line(): outer_one = lax.ppermute(middle_one, 'sp', outward_pairs)  15.6 us
    ppermute x2, waiting for transfers between devices, along_line(): outer_two = lax.ppermute(middle_two, 'sp', outward_pairs)  14 us
    pallas_call x5, Pallas kernels, kernel(): call(*near, *(pltpu.with_memory_space_constraint(array, pltpu.HBM) for ar...  13.1 us
    ppermute x2, waiting for transfers between devices, swap_both(): return lax.ppermute(array, ('sp', 'tp'), pairs)  4.32 us
    ppermute x2, starting transfers between devices, swap_both(): return lax.ppermute(array, ('sp', 'tp'), pairs)  2.99 us
    ppermute x2, starting transfers between devices, along_line(): outer_one = lax.ppermute(middle_one, 'sp', outward_pairs)  2.58 us
  transfers between devices with their start and end apart: 32, of which 19 were waited for; matrix products, arithmetic and copies ran while one was open for 0% of the time, Pallas kernels for 8%

profile of v2, /device:TPU:0, one launch (start us, length us, event | category | flops | bytes accessed | tf_op | source)
XLA Modules:
  0.0 122.7 jit_solution(12621863218426040565)
XLA Ops:
  0.0 1.3 %shard_map.127 = (bf16[4,128,384]{2,1,0:T(8,128)(2,1)S(1)}, f32[2,128]{1,0:T(2,128)S(1)}) custom-call(bf16[128,256]{1,0:T(8,128)(2,1)} %refs_0_.1, bf16[128,256]{1,0:T(8,128)(2,1)} %refs_1_.1, bf16[128,256]{1,0:T(8,128)(2,1)} %refs_2_.1, bf16[128,256]{1,0:T(8,128)(2,1)} %refs_3_.1, bf16[128,512]{1,0:T(8,128)(2,1)} %refs_4_.1, f32[1,128]{1,0:T(1,128)} %bitcast.9, ...), custom_call_target="tpu_custom_call" | custom-call | tf_op jit(solution)/shard_map/pallas_call | solution.py:301
  1.4 3.1 %collective-permute-start = (bf16[128,384]{1,0:T(8,128)(2,1)S(1)}, bf16[128,384]{1,0:T(8,128)(2,1)S(1)}, u32[]{:S(2)}, u32[]{:S(2)}) collective-permute-start(bf16[128,384]{1,0:T(8,128)(2,1)S(1)} %get-tuple-element.27), channel_id=1, source_target_pairs={{0,8},{4,12},{8,0},{12,4},{16,24},{20,28},{24,16},{28,20},{1,9},{5... | collective-permute-start | bytes 294920 | tf_op jit(solution)/shard_map/ppermute | solution.py:332
  4.5 2.5 %collective-permute-start.2 = (bf16[128,384]{1,0:T(8,128)(2,1)S(1)}, bf16[128,384]{1,0:T(8,128)(2,1)S(1)}, u32[]{:S(2)}, u32[]{:S(2)}) collective-permute-start(bf16[128,384]{1,0:T(8,128)(2,1)S(1)} %get-tuple-element.25), channel_id=1, source_target_pairs={{0,24},{4,28},{8,16},{12,20},{16,8},{20,12},{24,0},{28,4},{1,25},{... | collective-permute-start | bytes 294920 | tf_op jit(solution)/shard_map/ppermute | solution.py:332
  7.0 0.1 collective-permute-start.1
  7.1 0.2 collective-permute-done.b_ref
  7.3 1.8 %collective-permute-start.3 = (bf16[256,256]{1,0:T(8,128)(2,1)S(1)}, bf16[256,256]{1,0:T(8,128)(2,1)S(1)}, u32[]{:S(2)}, u32[]{:S(2)}) collective-permute-start(bf16[256,256]{1,0:T(8,128)(2,1)S(1)} %pad_maximum_fusion.1), channel_id=1, source_target_pairs={{0,4},{4,0},{8,12},{12,8},{16,20},{20,16},{24,28},{28,24},{1,5},{5... | collective-permute-start | bytes 393224 | tf_op jit(solution)/shard_map/ppermute | solution.py:332
  9.1 3.5 %collective-permute-done.2.d_ref = bf16[128,384]{1,0:T(8,128)(2,1)S(1)} collective-permute-done((bf16[128,384]{1,0:T(8,128)(2,1)S(1)}, bf16[128,384]{1,0:T(8,128)(2,1)S(1)}, u32[]{:S(2)}, u32[]{:S(2)}) %collective-permute-start.2) | collective-permute-done | bytes 98336 | tf_op jit(solution)/shard_map/ppermute | solution.py:332
  12.7 3.3 %collective-permute-done.1.c_ref = bf16[128,384]{1,0:T(8,128)(2,1)S(1)} collective-permute-done((bf16[128,384]{1,0:T(8,128)(2,1)S(1)}, bf16[128,384]{1,0:T(8,128)(2,1)S(1)}, u32[]{:S(2)}, u32[]{:S(2)}) %collective-permute-start.1) | collective-permute-done | bytes 98336 | tf_op jit(solution)/shard_map/ppermute | solution.py:332
  15.9 1.6 %collective-permute-start.4 = (bf16[256,256]{1,0:T(8,128)(2,1)S(1)}, bf16[256,256]{1,0:T(8,128)(2,1)S(1)}, u32[]{:S(2)}, u32[]{:S(2)}) collective-permute-start(bf16[256,256]{1,0:T(8,128)(2,1)S(1)} %pad_maximum_fusion.2), channel_id=1, source_target_pairs={{0,4},{4,0},{8,12},{12,8},{16,20},{20,16},{24,28},{28,24},{1,5},{5... | collective-permute-start | bytes 393224 | tf_op jit(solution)/shard_map/ppermute | solution.py:332
  17.5 0.5 collective-permute-start.8
  18.0 0.0 collective-permute-done.3.ab_ref
  18.0 4.3 %collective-permute-done.4.cd_ref = bf16[256,256]{1,0:T(8,128)(2,1)S(1)} collective-permute-done((bf16[256,256]{1,0:T(8,128)(2,1)S(1)}, bf16[256,256]{1,0:T(8,128)(2,1)S(1)}, u32[]{:S(2)}, u32[]{:S(2)}) %collective-permute-start.4) | collective-permute-done | bytes 131104 | tf_op jit(solution)/shard_map/ppermute | solution.py:332
  22.4 3.2 %shard_map.128.a_ref = bf16[4,128,128]{2,1,0:T(8,128)(2,1)S(1)} custom-call(f32[2,128]{1,0:T(2,128)S(1)} %get-tuple-element.11.extra_ref, bf16[128,384]{1,0:T(8,128)(2,1)S(1)} %get-tuple-element.28.a_ref, bf16[128,384]{1,0:T(8,128)(2,1)S(1)} %collective-permute-done.b_ref, bf16[128,384]{1,0:T(8,128)(2,1)S(1)} %collective-permute-done.1.c_ref, ...), custom_call_target="tpu_custom_call" | custom-call | tf_op jit(solution)/shard_map/pallas_call | solution.py:301
  25.6 2.7 %collective-permute-start.7 = (bf16[4,128,128]{2,1,0:T(8,128)(2,1)S(1)}, bf16[4,128,128]{2,1,0:T(8,128)(2,1)S(1)}, u32[]{:S(2)}, u32[]{:S(2)}) collective-permute-start(bf16[4,128,128]{2,1,0:T(8,128)(2,1)S(1)} %shard_map.128.a_ref), channel_id=1, source_target_pairs={{0,24},{4,28},{8,16},{12,20},{16,8},{20,12},{24,0},{28,4},{1,25},{... | collective-permute-start | bytes 393224 | tf_op jit(solution)/shard_map/ppermute | solution.py:332
  28.3 0.0 collective-permute-start.6
  28.3 1.7 %collective-permute-start.5 = (bf16[4,128,128]{2,1,0:T(8,128)(2,1)S(1)}, bf16[4,128,128]{2,1,0:T(8,128)(2,1)S(1)}, u32[]{:S(2)}, u32[]{:S(2)}) collective-permute-start(bf16[4,128,128]{2,1,0:T(8,128)(2,1)S(1)} %shard_map.128.a_ref), channel_id=1, source_target_pairs={{0,8},{4,12},{8,0},{12,4},{16,24},{20,28},{24,16},{28,20},{1,9},{5... | collective-permute-start | bytes 393224 | tf_op jit(solution)/shard_map/ppermute | solution.py:332
  30.0 0.0 collective-permute-done.8.other_ref
  30.0 3.1 %collective-permute-done.7.d_ref = bf16[4,128,128]{2,1,0:T(8,128)(2,1)S(1)} collective-permute-done((bf16[4,128,128]{2,1,0:T(8,128)(2,1)S(1)}, bf16[4,128,128]{2,1,0:T(8,128)(2,1)S(1)}, u32[]{:S(2)}, u32[]{:S(2)}) %collective-permute-start.7) | collective-permute-done | bytes 131104 | tf_op jit(solution)/shard_map/ppermute | solution.py:332
  33.1 4.1 %collective-permute-done.6.c_ref = bf16[4,128,128]{2,1,0:T(8,128)(2,1)S(1)} collective-permute-done((bf16[4,128,128]{2,1,0:T(8,128)(2,1)S(1)}, bf16[4,128,128]{2,1,0:T(8,128)(2,1)S(1)}, u32[]{:S(2)}, u32[]{:S(2)}) %collective-permute-start.6) | collective-permute-done | bytes 131104 | tf_op jit(solution)/shard_map/ppermute | solution.py:332
  37.2 1.5 %shard_map.129 = (f32[256,512]{1,0:T(8,128)S(1)}, bf16[256,512]{1,0:T(8,128)(2,1)S(1)}) custom-call(bf16[4,128,128]{2,1,0:T(8,128)(2,1)S(1)} %shard_map.128.a_ref, bf16[4,128,128]{2,1,0:T(8,128)(2,1)S(1)} %collective-permute-done.5.b_ref, bf16[4,128,128]{2,1,0:T(8,128)(2,1)S(1)} %collective-permute-done.6.c_ref, ...), custom_call_target="tpu_custom_call" | custom-call | tf_op jit(solution)/shard_map/pallas_call | solution.py:301
  38.7 0.1 collective-permute-start.9
  38.8 1.5 %collective-permute-done.9 = bf16[256,512]{1,0:T(8,128)(2,1)S(1)} collective-permute-done((bf16[256,512]{1,0:T(8,128)(2,1)S(1)}, bf16[256,512]{1,0:T(8,128)(2,1)S(1)}, u32[]{:S(2)}, u32[]{:S(2)}) %collective-permute-start.9) | collective-permute-done | bytes 262176 | tf_op jit(solution)/shard_map/ppermute | solution.py:332
  40.3 0.1 convert_add_fusion.1
  40.4 1.6 %collective-permute-start.10 = (bf16[128,512]{1,0:T(8,128)(2,1)S(1)}, bf16[128,512]{1,0:T(8,128)(2,1)S(1)}, u32[]{:S(2)}, u32[]{:S(2)}) collective-permute-start(bf16[128,512]{1,0:T(8,128)(2,1)S(1)} %slice.216), channel_id=1, source_target_pairs={{0,2},{1,3},{2,0},{3,1},{4,6},{5,7},{6,4},{7,5},{8,10},{9,11},{10,... | collective-permute-start | bytes 393224 | tf_op jit(solution)/shard_map/ppermute | solution.py:332
  42.0 0.1 fusion.18
  42.1 0.1 collective-permute-start.23
  42.2 2.0 %collective-permute-start.18 = (bf16[128,1408]{1,0:T(8,128)(2,1)S(1)}, bf16[128,1408]{1,0:T(8,128)(2,1)S(1)}, u32[]{:S(2)}, u32[]{:S(2)}) collective-permute-start(bf16[128,1408]{1,0:T(8,128)(2,1)S(1)} %get-tuple-element.24), channel_id=1, source_target_pairs={{0,8},{4,12},{8,0},{12,4},{16,24},{20,28},{24,16},{28,20},{1,9},{5... | collective-permute-start | bytes 1081352 | tf_op jit(solution)/shard_map/ppermute | solution.py:332
  44.2 1.9 %collective-permute-done.10 = bf16[128,512]{1,0:T(8,128)(2,1)S(1)} collective-permute-done((bf16[128,512]{1,0:T(8,128)(2,1)S(1)}, bf16[128,512]{1,0:T(8,128)(2,1)S(1)}, u32[]{:S(2)}, u32[]{:S(2)}) %collective-permute-start.10) | collective-permute-done | bytes 131104 | tf_op jit(solution)/shard_map/ppermute | solution.py:332
  46.1 0.1 collective-permute-start.13
  46.2 2.5 %collective-permute-start.12 = (bf16[32,512]{1,0:T(8,128)(2,1)S(1)}, bf16[32,512]{1,0:T(8,128)(2,1)S(1)}, u32[]{:S(2)}, u32[]{:S(2)}) collective-permute-start(bf16[32,512]{1,0:T(8,128)(2,1)S(1)} %get-tuple-element.51), channel_id=1, source_target_pairs={{0,16},{4,20},{8,24},{12,28},{16,0},{20,4},{24,8},{28,12},{1,17},{... | collective-permute-start | bytes 98312 | tf_op jit(solution)/shard_map/ppermute | solution.py:332
  48.7 1.8 %collective-permute-start.11 = (bf16[32,512]{1,0:T(8,128)(2,1)S(1)}, bf16[32,512]{1,0:T(8,128)(2,1)S(1)}, u32[]{:S(2)}, u32[]{:S(2)}) collective-permute-start(bf16[32,512]{1,0:T(8,128)(2,1)S(1)} %get-tuple-element.52), channel_id=1, source_target_pairs={{0,24},{4,28},{8,16},{12,20},{16,8},{20,12},{24,0},{28,4},{1,25},{... | collective-permute-start | bytes 98312 | tf_op jit(solution)/shard_map/ppermute | solution.py:332
  50.5 11.3 %collective-permute-done.13 = bf16[32,512]{1,0:T(8,128)(2,1)S(1)} collective-permute-done((bf16[32,512]{1,0:T(8,128)(2,1)S(1)}, bf16[32,512]{1,0:T(8,128)(2,1)S(1)}, u32[]{:S(2)}, u32[]{:S(2)}) %collective-permute-start.13) | collective-permute-done | bytes 32800 | tf_op jit(solution)/shard_map/ppermute | solution.py:332
  61.9 0.5 collective-permute-done.11
  62.5 0.2 fusion
  62.7 0.1 fusion.2
  62.8 1.5 %collective-permute-start.16 = (bf16[32,2048]{1,0:T(8,128)(2,1)S(1)}, bf16[32,2048]{1,0:T(8,128)(2,1)S(1)}, u32[]{:S(2)}, u32[]{:S(2)}) collective-permute-start(bf16[32,2048]{1,0:T(8,128)(2,1)S(1)} %fusion.2), channel_id=1, source_target_pairs={{0,6},{1,7},{2,4},{3,5},{4,2},{5,3},{6,0},{7,1},{8,14},{9,15},{10,... | collective-permute-start | bytes 393224 | tf_op jit(solution)/shard_map/ppermute | solution.py:340
  64.3 0.5 collective-permute-start.15
  64.8 1.5 %collective-permute-start.14 = (bf16[32,2048]{1,0:T(8,128)(2,1)S(1)}, bf16[32,2048]{1,0:T(8,128)(2,1)S(1)}, u32[]{:S(2)}, u32[]{:S(2)}) collective-permute-start(bf16[32,2048]{1,0:T(8,128)(2,1)S(1)} %fusion.2), channel_id=1, source_target_pairs={{0,2},{1,3},{2,0},{3,1},{4,6},{5,7},{6,4},{7,5},{8,10},{9,11},{10,... | collective-permute-start | bytes 393224 | tf_op jit(solution)/shard_map/ppermute | solution.py:332
  66.3 0.7 collective-permute-start.24
  67.0 0.7 collective-permute-start.19
  67.7 1.9 %collective-permute-done.16 = bf16[32,2048]{1,0:T(8,128)(2,1)S(1)} collective-permute-done((bf16[32,2048]{1,0:T(8,128)(2,1)S(1)}, bf16[32,2048]{1,0:T(8,128)(2,1)S(1)}, u32[]{:S(2)}, u32[]{:S(2)}) %collective-permute-start.16) | collective-permute-done | bytes 131104 | tf_op jit(solution)/shard_map/ppermute | solution.py:340
  69.6 0.7 collective-permute-start.26
  70.3 0.7 collective-permute-start.21
  71.1 0.1 collective-permute-start.17
  71.1 1.3 %collective-permute-start.25 = (bf16[128,1408]{1,0:T(8,128)(2,1)S(1)}, bf16[128,1408]{1,0:T(8,128)(2,1)S(1)}, u32[]{:S(2)}, u32[]{:S(2)}) collective-permute-start(bf16[128,1408]{1,0:T(8,128)(2,1)S(1)} %collective-permute-done.24.refs_6_), channel_id=1, source_target_pairs={{8,0},{12,4},{16,24},{20,28},{9,1},{13,5},{17,25},{21,29},{10,2},{... | collective-permute-start | bytes 1081352 | tf_op jit(solution)/shard_map/ppermute | solution.py:355
  72.5 1.3 %collective-permute-start.20 = (bf16[128,1408]{1,0:T(8,128)(2,1)S(1)}, bf16[128,1408]{1,0:T(8,128)(2,1)S(1)}, u32[]{:S(2)}, u32[]{:S(2)}) collective-permute-start(bf16[128,1408]{1,0:T(8,128)(2,1)S(1)} %collective-permute-done.19.refs_1_), channel_id=1, source_target_pairs={{8,0},{12,4},{16,24},{20,28},{9,1},{13,5},{17,25},{21,29},{10,2},{... | collective-permute-start | bytes 1081352 | tf_op jit(solution)/shard_map/ppermute | solution.py:355
  73.8 1.3 %collective-permute-start.27 = (bf16[128,1408]{1,0:T(8,128)(2,1)S(1)}, bf16[128,1408]{1,0:T(8,128)(2,1)S(1)}, u32[]{:S(2)}, u32[]{:S(2)}) collective-permute-start(bf16[128,1408]{1,0:T(8,128)(2,1)S(1)} %collective-permute-done.26.refs_8_), channel_id=1, source_target_pairs={{8,0},{12,4},{16,24},{20,28},{9,1},{13,5},{17,25},{21,29},{10,2},{... | collective-permute-start | bytes 1081352 | tf_op jit(solution)/shard_map/ppermute | solution.py:356
  75.1 1.3 %collective-permute-start.22 = (bf16[128,1408]{1,0:T(8,128)(2,1)S(1)}, bf16[128,1408]{1,0:T(8,128)(2,1)S(1)}, u32[]{:S(2)}, u32[]{:S(2)}) collective-permute-start(bf16[128,1408]{1,0:T(8,128)(2,1)S(1)} %collective-permute-done.21.refs_3_), channel_id=1, source_target_pairs={{8,0},{12,4},{16,24},{20,28},{9,1},{13,5},{17,25},{21,29},{10,2},{... | collective-permute-start | bytes 1081352 | tf_op jit(solution)/shard_map/ppermute | solution.py:356
  76.4 6.0 %shard_map.130.hidden_ref = bf16[256,1408]{1,0:T(8,128)(2,1)S(1)} custom-call(bf16[128,2048]{1,0:T(8,128)(2,1)S(1)} %pad_maximum_fusion.here_ref, bf16[128,2048]{1,0:T(8,128)(2,1)S(1)} %collective-permute-done.17.there_ref, bf16[2048,1408]{1,0:T(8,128)(2,1)} %gate_ref.1, bf16[2048,1408]{1,0:T(8,128)(2,1)} %up_ref.1), custom_call_target="tpu_custom_call" | custom-call | tf_op jit(solution)/shard_map/pallas_call | solution.py:301
  82.4 7.8 %collective-permute-done.25.refs_7_ = bf16[128,1408]{1,0:T(8,128)(2,1)S(1)} collective-permute-done((bf16[128,1408]{1,0:T(8,128)(2,1)S(1)}, bf16[128,1408]{1,0:T(8,128)(2,1)S(1)}, u32[]{:S(2)}, u32[]{:S(2)}) %collective-permute-start.25) | collective-permute-done | bytes 360480 | tf_op jit(solution)/shard_map/ppermute | solution.py:355
  90.3 7.7 %collective-permute-done.20.refs_2_ = bf16[128,1408]{1,0:T(8,128)(2,1)S(1)} collective-permute-done((bf16[128,1408]{1,0:T(8,128)(2,1)S(1)}, bf16[128,1408]{1,0:T(8,128)(2,1)S(1)}, u32[]{:S(2)}, u32[]{:S(2)}) %collective-permute-start.20) | collective-permute-done | bytes 360480 | tf_op jit(solution)/shard_map/ppermute | solution.py:355
  98.0 7.7 %collective-permute-done.27.refs_9_ = bf16[128,1408]{1,0:T(8,128)(2,1)S(1)} collective-permute-done((bf16[128,1408]{1,0:T(8,128)(2,1)S(1)}, bf16[128,1408]{1,0:T(8,128)(2,1)S(1)}, u32[]{:S(2)}, u32[]{:S(2)}) %collective-permute-start.27) | collective-permute-done | bytes 360480 | tf_op jit(solution)/shard_map/ppermute | solution.py:356
  105.7 6.2 %collective-permute-done.22.refs_4_ = bf16[128,1408]{1,0:T(8,128)(2,1)S(1)} collective-permute-done((bf16[128,1408]{1,0:T(8,128)(2,1)S(1)}, bf16[128,1408]{1,0:T(8,128)(2,1)S(1)}, u32[]{:S(2)}, u32[]{:S(2)}) %collective-permute-start.22) | collective-permute-done | bytes 360480 | tf_op jit(solution)/shard_map/ppermute | solution.py:356
  112.0 1.0 shard_map.131
  113.0 0.1 collective-permute-start.28
  113.1 1.5 %collective-permute-done.28 = bf16[128,1024]{1,0:T(8,128)(2,1)S(1)} collective-permute-done((bf16[128,1024]{1,0:T(8,128)(2,1)S(1)}, bf16[128,1024]{1,0:T(8,128)(2,1)S(1)}, u32[]{:S(2)}, u32[]{:S(2)}) %collective-permute-start.28) | collective-permute-done | bytes 262176 | tf_op jit(solution)/shard_map/ppermute | solution.py:332
  114.6 0.1 fusion.15
  114.7 0.6 collective-permute-start.31
  115.2 1.5 %collective-permute-start.29 = (bf16[32,1024]{1,0:T(8,128)(2,1)S(1)}, bf16[32,1024]{1,0:T(8,128)(2,1)S(1)}, u32[]{:S(2)}, u32[]{:S(2)}) collective-permute-start(bf16[32,1024]{1,0:T(8,128)(2,1)S(1)} %get-tuple-element.37), channel_id=1, source_target_pairs={{0,4},{4,0},{8,12},{12,8},{16,20},{20,16},{24,28},{28,24},{1,5},{5... | collective-permute-start | bytes 196616 | tf_op jit(solution)/shard_map/ppermute | solution.py:332
  116.7 1.5 %collective-permute-start.30 = (bf16[32,1024]{1,0:T(8,128)(2,1)S(1)}, bf16[32,1024]{1,0:T(8,128)(2,1)S(1)}, u32[]{:S(2)}, u32[]{:S(2)}) collective-permute-start(bf16[32,1024]{1,0:T(8,128)(2,1)S(1)} %get-tuple-element.39), channel_id=1, source_target_pairs={{0,6},{1,7},{2,4},{3,5},{4,2},{5,3},{6,0},{7,1},{8,14},{9,15},{10,... | collective-permute-start | bytes 196616 | tf_op jit(solution)/shard_map/ppermute | solution.py:340
  118.2 0.8 collective-permute-done.31
  119.0 0.5 collective-permute-done.29
  119.5 2.4 %collective-permute-done.30 = bf16[32,1024]{1,0:T(8,128)(2,1)S(1)} collective-permute-done((bf16[32,1024]{1,0:T(8,128)(2,1)S(1)}, bf16[32,1024]{1,0:T(8,128)(2,1)S(1)}, u32[]{:S(2)}, u32[]{:S(2)}) %collective-permute-start.30) | collective-permute-done | bytes 65568 | tf_op jit(solution)/shard_map/ppermute | solution.py:340
  122.0 0.7 fusion.3
  (44 shorter events, 0.4 us)
Async XLA Ops:
  0.0 42.0 %copy-start = (bf16[256,1408]{1,0:T(8,128)(2,1)S(1)}, bf16[256,1408]{1,0:T(8,128)(2,1)}, u32[]{:S(2)}) copy-start(bf16[256,1408]{1,0:T(8,128)(2,1)} %own_ref.1) | copy-start | bytes 2162692
  0.0 62.5 %copy-start.1 = (bf16[32,2048]{1,0:T(8,128)(2,1)S(1)}, bf16[32,2048]{1,0:T(8,128)(2,1)}, u32[]{:S(2)}) copy-start(bf16[32,2048]{1,0:T(8,128)(2,1)} %param.13) | copy-start | bytes 393220
  0.0 62.6 %copy-start.2 = (f32[2048]{0:T(1024)S(1)}, f32[2048]{0:T(1024)}, u32[]{:S(2)}) copy-start(f32[2048]{0:T(1024)} %param.22) | copy-start | bytes 24580
  1.4 5.9 %collective-permute-start = (bf16[128,384]{1,0:T(8,128)(2,1)S(1)}, bf16[128,384]{1,0:T(8,128)(2,1)S(1)}, u32[]{:S(2)}, u32[]{:S(2)}) collective-permute-start(bf16[128,384]{1,0:T(8,128)(2,1)S(1)} %get-tuple-element.27), channel_id=1, source_target_pairs={{0,8},{4,12},{8,0},{12,4},{16,24},{20,28},{24,16},{28,20},{1,9},{5... | collective-permute-start | bytes 294920 | tf_op jit(solution)/shard_map/ppermute | solution.py:332
  4.5 8.2 %collective-permute-start.2 = (bf16[128,384]{1,0:T(8,128)(2,1)S(1)}, bf16[128,384]{1,0:T(8,128)(2,1)S(1)}, u32[]{:S(2)}, u32[]{:S(2)}) collective-permute-start(bf16[128,384]{1,0:T(8,128)(2,1)S(1)} %get-tuple-element.25), channel_id=1, source_target_pairs={{0,24},{4,28},{8,16},{12,20},{16,8},{20,12},{24,0},{28,4},{1,25},{... | collective-permute-start | bytes 294920 | tf_op jit(solution)/shard_map/ppermute | solution.py:332
  7.0 8.9 %collective-permute-start.1 = (bf16[128,384]{1,0:T(8,128)(2,1)S(1)}, bf16[128,384]{1,0:T(8,128)(2,1)S(1)}, u32[]{:S(2)}, u32[]{:S(2)}) collective-permute-start(bf16[128,384]{1,0:T(8,128)(2,1)S(1)} %get-tuple-element.26), channel_id=1, source_target_pairs={{0,16},{4,20},{8,24},{12,28},{16,0},{20,4},{24,8},{28,12},{1,17},{... | collective-permute-start | bytes 294920 | tf_op jit(solution)/shard_map/ppermute | solution.py:332
  7.3 10.7 %collective-permute-start.3 = (bf16[256,256]{1,0:T(8,128)(2,1)S(1)}, bf16[256,256]{1,0:T(8,128)(2,1)S(1)}, u32[]{:S(2)}, u32[]{:S(2)}) collective-permute-start(bf16[256,256]{1,0:T(8,128)(2,1)S(1)} %pad_maximum_fusion.1), channel_id=1, source_target_pairs={{0,4},{4,0},{8,12},{12,8},{16,20},{20,16},{24,28},{28,24},{1,5},{5... | collective-permute-start | bytes 393224 | tf_op jit(solution)/shard_map/ppermute | solution.py:332
  15.9 6.4 %collective-permute-start.4 = (bf16[256,256]{1,0:T(8,128)(2,1)S(1)}, bf16[256,256]{1,0:T(8,128)(2,1)S(1)}, u32[]{:S(2)}, u32[]{:S(2)}) collective-permute-start(bf16[256,256]{1,0:T(8,128)(2,1)S(1)} %pad_maximum_fusion.2), channel_id=1, source_target_pairs={{0,4},{4,0},{8,12},{12,8},{16,20},{20,16},{24,28},{28,24},{1,5},{5... | collective-permute-start | bytes 393224 | tf_op jit(solution)/shard_map/ppermute | solution.py:332
  17.5 12.5 %collective-permute-start.8 = (bf16[256,512]{1,0:T(8,128)(2,1)}, bf16[256,512]{1,0:T(8,128)(2,1)S(1)}, u32[]{:S(2)}, u32[]{:S(2)}) collective-permute-start(bf16[256,512]{1,0:T(8,128)(2,1)} %source.1), channel_id=1, source_target_pairs={{0,4},{4,0},{8,12},{12,8},{16,20},{20,16},{24,28},{28,24},{1,5},{5... | collective-permute-start | bytes 786440 | tf_op jit(solution)/shard_map/ppermute | solution.py:332
  25.6 7.5 %collective-permute-start.7 = (bf16[4,128,128]{2,1,0:T(8,128)(2,1)S(1)}, bf16[4,128,128]{2,1,0:T(8,128)(2,1)S(1)}, u32[]{:S(2)}, u32[]{:S(2)}) collective-permute-start(bf16[4,128,128]{2,1,0:T(8,128)(2,1)S(1)} %shard_map.128.a_ref), channel_id=1, source_target_pairs={{0,24},{4,28},{8,16},{12,20},{16,8},{20,12},{24,0},{28,4},{1,25},{... | collective-permute-start | bytes 393224 | tf_op jit(solution)/shard_map/ppermute | solution.py:332
  28.3 8.9 %collective-permute-start.6 = (bf16[4,128,128]{2,1,0:T(8,128)(2,1)S(1)}, bf16[4,128,128]{2,1,0:T(8,128)(2,1)S(1)}, u32[]{:S(2)}, u32[]{:S(2)}) collective-permute-start(bf16[4,128,128]{2,1,0:T(8,128)(2,1)S(1)} %shard_map.128.a_ref), channel_id=1, source_target_pairs={{0,16},{4,20},{8,24},{12,28},{16,0},{20,4},{24,8},{28,12},{1,17},{... | collective-permute-start | bytes 393224 | tf_op jit(solution)/shard_map/ppermute | solution.py:332
  28.3 8.9 %collective-permute-start.5 = (bf16[4,128,128]{2,1,0:T(8,128)(2,1)S(1)}, bf16[4,128,128]{2,1,0:T(8,128)(2,1)S(1)}, u32[]{:S(2)}, u32[]{:S(2)}) collective-permute-start(bf16[4,128,128]{2,1,0:T(8,128)(2,1)S(1)} %shard_map.128.a_ref), channel_id=1, source_target_pairs={{0,8},{4,12},{8,0},{12,4},{16,24},{20,28},{24,16},{28,20},{1,9},{5... | collective-permute-start | bytes 393224 | tf_op jit(solution)/shard_map/ppermute | solution.py:332
  38.7 1.6 %collective-permute-start.9 = (bf16[256,512]{1,0:T(8,128)(2,1)S(1)}, bf16[256,512]{1,0:T(8,128)(2,1)S(1)}, u32[]{:S(2)}, u32[]{:S(2)}) collective-permute-start(bf16[256,512]{1,0:T(8,128)(2,1)S(1)} %get-tuple-element.14), channel_id=1, source_target_pairs={{0,1},{1,0},{2,3},{3,2},{4,5},{5,4},{6,7},{7,6},{8,9},{9,8},{10,11... | collective-permute-start | bytes 786440 | tf_op jit(solution)/shard_map/ppermute | solution.py:332
  40.4 5.6 %collective-permute-start.10 = (bf16[128,512]{1,0:T(8,128)(2,1)S(1)}, bf16[128,512]{1,0:T(8,128)(2,1)S(1)}, u32[]{:S(2)}, u32[]{:S(2)}) collective-permute-start(bf16[128,512]{1,0:T(8,128)(2,1)S(1)} %slice.216), channel_id=1, source_target_pairs={{0,2},{1,3},{2,0},{3,1},{4,6},{5,7},{6,4},{7,5},{8,10},{9,11},{10,... | collective-permute-start | bytes 393224 | tf_op jit(solution)/shard_map/ppermute | solution.py:332
  42.1 24.2 %collective-permute-start.23 = (bf16[128,1408]{1,0:T(8,128)(2,1)S(1)}, bf16[128,1408]{1,0:T(8,128)(2,1)S(1)}, u32[]{:S(2)}, u32[]{:S(2)}) collective-permute-start(bf16[128,1408]{1,0:T(8,128)(2,1)S(1)} %get-tuple-element.23), channel_id=1, source_target_pairs={{0,8},{4,12},{8,0},{12,4},{16,24},{20,28},{24,16},{28,20},{1,9},{5... | collective-permute-start | bytes 1081352 | tf_op jit(solution)/shard_map/ppermute | solution.py:332
  42.2 24.9 %collective-permute-start.18 = (bf16[128,1408]{1,0:T(8,128)(2,1)S(1)}, bf16[128,1408]{1,0:T(8,128)(2,1)S(1)}, u32[]{:S(2)}, u32[]{:S(2)}) collective-permute-start(bf16[128,1408]{1,0:T(8,128)(2,1)S(1)} %get-tuple-element.24), channel_id=1, source_target_pairs={{0,8},{4,12},{8,0},{12,4},{16,24},{20,28},{24,16},{28,20},{1,9},{5... | collective-permute-start | bytes 1081352 | tf_op jit(solution)/shard_map/ppermute | solution.py:332
  46.1 15.7 %collective-permute-start.13 = (bf16[32,512]{1,0:T(8,128)(2,1)S(1)}, bf16[32,512]{1,0:T(8,128)(2,1)S(1)}, u32[]{:S(2)}, u32[]{:S(2)}) collective-permute-start(bf16[32,512]{1,0:T(8,128)(2,1)S(1)} %get-tuple-element.50), channel_id=1, source_target_pairs={{0,8},{4,12},{8,0},{12,4},{16,24},{20,28},{24,16},{28,20},{1,9},{5... | collective-permute-start | bytes 98312 | tf_op jit(solution)/shard_map/ppermute | solution.py:332
  46.2 15.7 %collective-permute-start.12 = (bf16[32,512]{1,0:T(8,128)(2,1)S(1)}, bf16[32,512]{1,0:T(8,128)(2,1)S(1)}, u32[]{:S(2)}, u32[]{:S(2)}) collective-permute-start(bf16[32,512]{1,0:T(8,128)(2,1)S(1)} %get-tuple-element.51), channel_id=1, source_target_pairs={{0,16},{4,20},{8,24},{12,28},{16,0},{20,4},{24,8},{28,12},{1,17},{... | collective-permute-start | bytes 98312 | tf_op jit(solution)/shard_map/ppermute | solution.py:332
  48.7 13.7 %collective-permute-start.11 = (bf16[32,512]{1,0:T(8,128)(2,1)S(1)}, bf16[32,512]{1,0:T(8,128)(2,1)S(1)}, u32[]{:S(2)}, u32[]{:S(2)}) collective-permute-start(bf16[32,512]{1,0:T(8,128)(2,1)S(1)} %get-tuple-element.52), channel_id=1, source_target_pairs={{0,24},{4,28},{8,16},{12,20},{16,8},{20,12},{24,0},{28,4},{1,25},{... | collective-permute-start | bytes 98312 | tf_op jit(solution)/shard_map/ppermute | solution.py:332
  62.8 6.9 %collective-permute-start.16 = (bf16[32,2048]{1,0:T(8,128)(2,1)S(1)}, bf16[32,2048]{1,0:T(8,128)(2,1)S(1)}, u32[]{:S(2)}, u32[]{:S(2)}) collective-permute-start(bf16[32,2048]{1,0:T(8,128)(2,1)S(1)} %fusion.2), channel_id=1, source_target_pairs={{0,6},{1,7},{2,4},{3,5},{4,2},{5,3},{6,0},{7,1},{8,14},{9,15},{10,... | collective-permute-start | bytes 393224 | tf_op jit(solution)/shard_map/ppermute | solution.py:340
  64.3 6.0 %collective-permute-start.15 = (bf16[32,2048]{1,0:T(8,128)(2,1)S(1)}, bf16[32,2048]{1,0:T(8,128)(2,1)S(1)}, u32[]{:S(2)}, u32[]{:S(2)}) collective-permute-start(bf16[32,2048]{1,0:T(8,128)(2,1)S(1)} %fusion.2), channel_id=1, source_target_pairs={{0,4},{4,0},{8,12},{12,8},{16,20},{20,16},{24,28},{28,24},{1,5},{5... | collective-permute-start | bytes 393224 | tf_op jit(solution)/shard_map/ppermute | solution.py:332
  64.8 6.2 %collective-permute-start.14 = (bf16[32,2048]{1,0:T(8,128)(2,1)S(1)}, bf16[32,2048]{1,0:T(8,128)(2,1)S(1)}, u32[]{:S(2)}, u32[]{:S(2)}) collective-permute-start(bf16[32,2048]{1,0:T(8,128)(2,1)S(1)} %fusion.2), channel_id=1, source_target_pairs={{0,2},{1,3},{2,0},{3,1},{4,6},{5,7},{6,4},{7,5},{8,10},{9,11},{10,... | collective-permute-start | bytes 393224 | tf_op jit(solution)/shard_map/ppermute | solution.py:332
  66.3 4.8 %collective-permute-start.24 = (bf16[128,1408]{1,0:T(8,128)(2,1)S(1)}, bf16[128,1408]{1,0:T(8,128)(2,1)S(1)}, u32[]{:S(2)}, u32[]{:S(2)}) collective-permute-start(bf16[128,1408]{1,0:T(8,128)(2,1)S(1)} %get-tuple-element.23), channel_id=1, source_target_pairs={{8,16},{12,20},{16,8},{20,12},{9,17},{13,21},{17,9},{21,13},{10,18... | collective-permute-start | bytes 1081352 | tf_op jit(solution)/shard_map/ppermute | solution.py:353
  67.0 5.4 %collective-permute-start.19 = (bf16[128,1408]{1,0:T(8,128)(2,1)S(1)}, bf16[128,1408]{1,0:T(8,128)(2,1)S(1)}, u32[]{:S(2)}, u32[]{:S(2)}) collective-permute-start(bf16[128,1408]{1,0:T(8,128)(2,1)S(1)} %get-tuple-element.24), channel_id=1, source_target_pairs={{8,16},{12,20},{16,8},{20,12},{9,17},{13,21},{17,9},{21,13},{10,18... | collective-permute-start | bytes 1081352 | tf_op jit(solution)/shard_map/ppermute | solution.py:353
  69.6 4.1 %collective-permute-start.26 = (bf16[128,1408]{1,0:T(8,128)(2,1)S(1)}, bf16[128,1408]{1,0:T(8,128)(2,1)S(1)}, u32[]{:S(2)}, u32[]{:S(2)}) collective-permute-start(bf16[128,1408]{1,0:T(8,128)(2,1)S(1)} %collective-permute-done.23.refs_5_), channel_id=1, source_target_pairs={{8,16},{12,20},{16,8},{20,12},{9,17},{13,21},{17,9},{21,13},{10,18... | collective-permute-start | bytes 1081352 | tf_op jit(solution)/shard_map/ppermute | solution.py:354
  70.3 4.8 %collective-permute-start.21 = (bf16[128,1408]{1,0:T(8,128)(2,1)S(1)}, bf16[128,1408]{1,0:T(8,128)(2,1)S(1)}, u32[]{:S(2)}, u32[]{:S(2)}) collective-permute-start(bf16[128,1408]{1,0:T(8,128)(2,1)S(1)} %collective-permute-done.18.refs_0_), channel_id=1, source_target_pairs={{8,16},{12,20},{16,8},{20,12},{9,17},{13,21},{17,9},{21,13},{10,18... | collective-permute-start | bytes 1081352 | tf_op jit(solution)/shard_map/ppermute | solution.py:354
  71.1 5.3 %collective-permute-start.17 = (bf16[128,2048]{1,0:T(8,128)(2,1)S(1)}, bf16[128,2048]{1,0:T(8,128)(2,1)S(1)}, u32[]{:S(2)}, u32[]{:S(2)}) collective-permute-start(bf16[128,2048]{1,0:T(8,128)(2,1)S(1)} %pad_maximum_fusion.here_ref), channel_id=1, source_target_pairs={{0,1},{1,0},{2,3},{3,2},{4,5},{5,4},{6,7},{7,6},{8,9},{9,8},{10,11... | collective-permute-start | bytes 1572872 | tf_op jit(solution)/shard_map/ppermute | solution.py:332
  71.1 19.1 %collective-permute-start.25 = (bf16[128,1408]{1,0:T(8,128)(2,1)S(1)}, bf16[128,1408]{1,0:T(8,128)(2,1)S(1)}, u32[]{:S(2)}, u32[]{:S(2)}) collective-permute-start(bf16[128,1408]{1,0:T(8,128)(2,1)S(1)} %collective-permute-done.24.refs_6_), channel_id=1, source_target_pairs={{8,0},{12,4},{16,24},{20,28},{9,1},{13,5},{17,25},{21,29},{10,2},{... | collective-permute-start | bytes 1081352 | tf_op jit(solution)/shard_map/ppermute | solution.py:355
  72.5 25.5 %collective-permute-start.20 = (bf16[128,1408]{1,0:T(8,128)(2,1)S(1)}, bf16[128,1408]{1,0:T(8,128)(2,1)S(1)}, u32[]{:S(2)}, u32[]{:S(2)}) collective-permute-start(bf16[128,1408]{1,0:T(8,128)(2,1)S(1)} %collective-permute-done.19.refs_1_), channel_id=1, source_target_pairs={{8,0},{12,4},{16,24},{20,28},{9,1},{13,5},{17,25},{21,29},{10,2},{... | collective-permute-start | bytes 1081352 | tf_op jit(solution)/shard_map/ppermute | solution.py:355
  73.8 31.9 %collective-permute-start.27 = (bf16[128,1408]{1,0:T(8,128)(2,1)S(1)}, bf16[128,1408]{1,0:T(8,128)(2,1)S(1)}, u32[]{:S(2)}, u32[]{:S(2)}) collective-permute-start(bf16[128,1408]{1,0:T(8,128)(2,1)S(1)} %collective-permute-done.26.refs_8_), channel_id=1, source_target_pairs={{8,0},{12,4},{16,24},{20,28},{9,1},{13,5},{17,25},{21,29},{10,2},{... | collective-permute-start | bytes 1081352 | tf_op jit(solution)/shard_map/ppermute | solution.py:356
  75.1 36.9 %collective-permute-start.22 = (bf16[128,1408]{1,0:T(8,128)(2,1)S(1)}, bf16[128,1408]{1,0:T(8,128)(2,1)S(1)}, u32[]{:S(2)}, u32[]{:S(2)}) collective-permute-start(bf16[128,1408]{1,0:T(8,128)(2,1)S(1)} %collective-permute-done.21.refs_3_), channel_id=1, source_target_pairs={{8,0},{12,4},{16,24},{20,28},{9,1},{13,5},{17,25},{21,29},{10,2},{... | collective-permute-start | bytes 1081352 | tf_op jit(solution)/shard_map/ppermute | solution.py:356
  113.0 1.6 %collective-permute-start.28 = (bf16[128,1024]{1,0:T(8,128)(2,1)S(1)}, bf16[128,1024]{1,0:T(8,128)(2,1)S(1)}, u32[]{:S(2)}, u32[]{:S(2)}) collective-permute-start(bf16[128,1024]{1,0:T(8,128)(2,1)S(1)} %get-tuple-element.16), channel_id=1, source_target_pairs={{0,1},{1,0},{2,3},{3,2},{4,5},{5,4},{6,7},{7,6},{8,9},{9,8},{10,11... | collective-permute-start | bytes 786440 | tf_op jit(solution)/shard_map/ppermute | solution.py:332
  114.7 4.3 %collective-permute-start.31 = (bf16[32,1024]{1,0:T(8,128)(2,1)S(1)}, bf16[32,1024]{1,0:T(8,128)(2,1)S(1)}, u32[]{:S(2)}, u32[]{:S(2)}) collective-permute-start(bf16[32,1024]{1,0:T(8,128)(2,1)S(1)} %get-tuple-element.38), channel_id=1, source_target_pairs={{0,2},{1,3},{2,0},{3,1},{4,6},{5,7},{6,4},{7,5},{8,10},{9,11},{10,... | collective-permute-start | bytes 196616 | tf_op jit(solution)/shard_map/ppermute | solution.py:332
  115.2 4.3 %collective-permute-start.29 = (bf16[32,1024]{1,0:T(8,128)(2,1)S(1)}, bf16[32,1024]{1,0:T(8,128)(2,1)S(1)}, u32[]{:S(2)}, u32[]{:S(2)}) collective-permute-start(bf16[32,1024]{1,0:T(8,128)(2,1)S(1)} %get-tuple-element.37), channel_id=1, source_target_pairs={{0,4},{4,0},{8,12},{12,8},{16,20},{20,16},{24,28},{28,24},{1,5},{5... | collective-permute-start | bytes 196616 | tf_op jit(solution)/shard_map/ppermute | solution.py:332
  116.7 5.2 %collective-permute-start.30 = (bf16[32,1024]{1,0:T(8,128)(2,1)S(1)}, bf16[32,1024]{1,0:T(8,128)(2,1)S(1)}, u32[]{:S(2)}, u32[]{:S(2)}) collective-permute-start(bf16[32,1024]{1,0:T(8,128)(2,1)S(1)} %get-tuple-element.39), channel_id=1, source_target_pairs={{0,6},{1,7},{2,4},{3,5},{4,2},{5,3},{6,0},{7,1},{8,14},{9,15},{10,... | collective-permute-start | bytes 196616 | tf_op jit(solution)/shard_map/ppermute | solution.py:340

commit v3 on v2

--- a/solution.py
+++ b/solution.py
@@ -161,6 +161,7 @@
     lanes = a_ref.shape[1] - ab_ref.shape[1]
     head_size = lanes // 2
     scale = head_size ** (-0.5)
+    exact = math.frexp(scale)[0] == 0.5
     queries = (a_ref, b_ref, c_ref, d_ref)
     for index, ref in enumerate(queries):
         k_ref[index * rows : (index + 1) * rows] = ref[:, lanes : 2 * lanes]
@@ -173,15 +174,14 @@
 
     def one_map(query, which):
         wanted = (lane < head_size) if which == 0 else (lane >= head_size)
-        scores = (
-            lax.dot_general(
-                jnp.where(wanted, query, jnp.zeros_like(query)),
-                k_ref[...],
-                (((1,), (1,)), ((), ())),
-                preferred_element_type=jnp.float32,
-            )
-            * scale
-        )
+        scores = lax.dot_general(
+            jnp.where(wanted, query, jnp.zeros_like(query)),
+            k_ref[...],
+            (((1,), (1,)), ((), ())),
+            preferred_element_type=jnp.float32,
+        )
+        if not exact:
+            scores = scores * scale
         shifted = jnp.exp(scores - scores.max(axis=-1, keepdims=True))
         total = shifted.sum(axis=-1, keepdims=True)
         product = jnp.dot(
@@ -191,6 +191,8 @@
 
     for index, ref in enumerate(queries):
         query = ref[:, :lanes]
+        if exact:
+            query = query * jnp.asarray(scale, query.dtype)
         difference = one_map(query, 0) - weight * one_map(query, 1)
         scaled = difference * lax.rsqrt(
             jnp.mean(difference * difference, axis=-1, keepdims=True) + epsilon
@@ -474,7 +476,7 @@
     )
     half = (4 * rows, width // 2)
     halves = (jax.ShapeDtypeStruct(half, f32), jax.ShapeDtypeStruct(half, bf16))
-    middle = down_weight.shape[0] // 2
+    middle = down_weight.shape[0] * 5 // 8
     fed = kernel(
         functools.partial(down_body, sp_size=sp_size),
         halves,

time: 123 us -> 131 us (1.065)
  starting transfers between devices: 37.4 us -> 45.4 us
    ppermute x22, starting transfers between devices: 26.5 us -> 35.6 us  [swap(): return lax.ppermute(array, axis, [(i, i ^ distance) for i in range(count)])]
    ppermute x2, waiting for transfers between devices: 14 us -> 5.59 us  [along_line(): outer_two = lax.ppermute(middle_two, 'sp', outward_pairs)]
    ppermute x2, waiting for transfers between devices: 15.6 us -> 20.3 us  [along_line(): outer_one = lax.ppermute(middle_one, 'sp', outward_pairs)]
    ppermute x22, waiting for transfers between devices: 36.5 us -> 40.4 us  [swap(): return lax.ppermute(array, axis, [(i, i ^ distance) for i in range(count)])]
  transfers between devices with their start and end apart: 32 -> 32, of which waited for: 19 -> 17; matrix products, arithmetic and copies ran while one was open for 0% -> 1% of each run, Pallas kernels for 8% -> 7%
where the time goes in v3:
time: 131 us
  waiting for transfers between devices  69.4 us (53%)
  starting transfers between devices  45.4 us (35%)
  Pallas kernels  13.1 us (10%)
  other arithmetic  1.37 us (1%)
    ppermute x22, waiting for transfers between devices, swap(): return lax.ppermute(array, axis, [(i, i ^ distance) for i in range(count)])  40.4 us
    ppermute x22, starting transfers between devices, swap(): return lax.ppermute(array, axis, [(i, i ^ distance) for i in range(count)])  35.6 us
    ppermute x2, waiting for transfers between devices, along_line(): outer_one = lax.ppermute(middle_one, 'sp', outward_pairs)  20.3 us
    pallas_call x5, Pallas kernels, kernel(): call(*near, *(pltpu.with_memory_space_constraint(array, pltpu.HBM) for ar...  13.1 us
    ppermute x2, waiting for transfers between devices, along_line(): outer_two = lax.ppermute(middle_two, 'sp', outward_pairs)  5.59 us
    ppermute x2, waiting for transfers between devices, swap_both(): return lax.ppermute(array, ('sp', 'tp'), pairs)  3.16 us
  transfers between devices with their start and end apart: 32, of which 17 were waited for; matrix products, arithmetic and copies ran while one was open for 1% of the time, Pallas kernels for 7%

profile of v3, /device:TPU:0, one launch (start us, length us, event | category | flops | bytes accessed | tf_op | source)
XLA Modules:
  0.0 130.9 jit_solution(18064693286606558820)
XLA Ops:
  0.0 1.3 %shard_map.127 = (bf16[4,128,384]{2,1,0:T(8,128)(2,1)S(1)}, f32[2,128]{1,0:T(2,128)S(1)}) custom-call(bf16[128,256]{1,0:T(8,128)(2,1)} %refs_0_.1, bf16[128,256]{1,0:T(8,128)(2,1)} %refs_1_.1, bf16[128,256]{1,0:T(8,128)(2,1)} %refs_2_.1, bf16[128,256]{1,0:T(8,128)(2,1)} %refs_3_.1, bf16[128,512]{1,0:T(8,128)(2,1)} %refs_4_.1, f32[1,128]{1,0:T(1,128)} %bitcast.9, ...), custom_call_target="tpu_custom_call" | custom-call | tf_op jit(solution)/shard_map/pallas_call | solution.py:303
  1.4 4.1 %collective-permute-start.1 = (bf16[128,384]{1,0:T(8,128)(2,1)S(1)}, bf16[128,384]{1,0:T(8,128)(2,1)S(1)}, u32[]{:S(2)}, u32[]{:S(2)}) collective-permute-start(bf16[128,384]{1,0:T(8,128)(2,1)S(1)} %get-tuple-element.24), channel_id=1, source_target_pairs={{0,16},{4,20},{8,24},{12,28},{16,0},{20,4},{24,8},{28,12},{1,17},{... | collective-permute-start | bytes 294920 | tf_op jit(solution)/shard_map/ppermute | solution.py:334
  5.5 1.3 %collective-permute-start.2 = (bf16[128,384]{1,0:T(8,128)(2,1)S(1)}, bf16[128,384]{1,0:T(8,128)(2,1)S(1)}, u32[]{:S(2)}, u32[]{:S(2)}) collective-permute-start(bf16[128,384]{1,0:T(8,128)(2,1)S(1)} %get-tuple-element.23), channel_id=1, source_target_pairs={{0,24},{4,28},{8,16},{12,20},{16,8},{20,12},{24,0},{28,4},{1,25},{... | collective-permute-start | bytes 294920 | tf_op jit(solution)/shard_map/ppermute | solution.py:334
  6.9 0.2 collective-permute-start
  7.1 6.3 %collective-permute-done.1.c_ref = bf16[128,384]{1,0:T(8,128)(2,1)S(1)} collective-permute-done((bf16[128,384]{1,0:T(8,128)(2,1)S(1)}, bf16[128,384]{1,0:T(8,128)(2,1)S(1)}, u32[]{:S(2)}, u32[]{:S(2)}) %collective-permute-start.1) | collective-permute-done | bytes 98336 | tf_op jit(solution)/shard_map/ppermute | solution.py:334
  13.4 0.0 collective-permute-done.2.d_ref
  13.5 1.7 %collective-permute-start.4 = (bf16[256,256]{1,0:T(8,128)(2,1)S(1)}, bf16[256,256]{1,0:T(8,128)(2,1)S(1)}, u32[]{:S(2)}, u32[]{:S(2)}) collective-permute-start(bf16[256,256]{1,0:T(8,128)(2,1)S(1)} %pad_maximum_fusion.2), channel_id=1, source_target_pairs={{0,4},{4,0},{8,12},{12,8},{16,20},{20,16},{24,28},{28,24},{1,5},{5... | collective-permute-start | bytes 393224 | tf_op jit(solution)/shard_map/ppermute | solution.py:334
  15.2 0.0 collective-permute-done.b_ref
  15.2 0.4 collective-permute-start.3
  15.7 1.7 %collective-permute-start.8 = (bf16[256,512]{1,0:T(8,128)(2,1)}, bf16[256,512]{1,0:T(8,128)(2,1)S(1)}, u32[]{:S(2)}, u32[]{:S(2)}) collective-permute-start(bf16[256,512]{1,0:T(8,128)(2,1)} %source.1), channel_id=1, source_target_pairs={{0,4},{4,0},{8,12},{12,8},{16,20},{20,16},{24,28},{28,24},{1,5},{5... | collective-permute-start | bytes 786440 | tf_op jit(solution)/shard_map/ppermute | solution.py:334
  17.3 2.6 %collective-permute-done.4.cd_ref = bf16[256,256]{1,0:T(8,128)(2,1)S(1)} collective-permute-done((bf16[256,256]{1,0:T(8,128)(2,1)S(1)}, bf16[256,256]{1,0:T(8,128)(2,1)S(1)}, u32[]{:S(2)}, u32[]{:S(2)}) %collective-permute-start.4) | collective-permute-done | bytes 131104 | tf_op jit(solution)/shard_map/ppermute | solution.py:334
  19.9 2.7 %collective-permute-done.3.ab_ref = bf16[256,256]{1,0:T(8,128)(2,1)S(1)} collective-permute-done((bf16[256,256]{1,0:T(8,128)(2,1)S(1)}, bf16[256,256]{1,0:T(8,128)(2,1)S(1)}, u32[]{:S(2)}, u32[]{:S(2)}) %collective-permute-start.3) | collective-permute-done | bytes 131104 | tf_op jit(solution)/shard_map/ppermute | solution.py:334
  22.6 3.2 %shard_map.128.a_ref = bf16[4,128,128]{2,1,0:T(8,128)(2,1)S(1)} custom-call(f32[2,128]{1,0:T(2,128)S(1)} %get-tuple-element.11.extra_ref, bf16[128,384]{1,0:T(8,128)(2,1)S(1)} %get-tuple-element.26.a_ref, bf16[128,384]{1,0:T(8,128)(2,1)S(1)} %collective-permute-done.b_ref, bf16[128,384]{1,0:T(8,128)(2,1)S(1)} %collective-permute-done.1.c_ref, ...), custom_call_target="tpu_custom_call" | custom-call | tf_op jit(solution)/shard_map/pallas_call | solution.py:303
  25.8 2.1 %collective-permute-start.5 = (bf16[4,128,128]{2,1,0:T(8,128)(2,1)S(1)}, bf16[4,128,128]{2,1,0:T(8,128)(2,1)S(1)}, u32[]{:S(2)}, u32[]{:S(2)}) collective-permute-start(bf16[4,128,128]{2,1,0:T(8,128)(2,1)S(1)} %shard_map.128.a_ref), channel_id=1, source_target_pairs={{0,8},{4,12},{8,0},{12,4},{16,24},{20,28},{24,16},{28,20},{1,9},{5... | collective-permute-start | bytes 393224 | tf_op jit(solution)/shard_map/ppermute | solution.py:334
  27.9 2.0 %collective-permute-start.6 = (bf16[4,128,128]{2,1,0:T(8,128)(2,1)S(1)}, bf16[4,128,128]{2,1,0:T(8,128)(2,1)S(1)}, u32[]{:S(2)}, u32[]{:S(2)}) collective-permute-start(bf16[4,128,128]{2,1,0:T(8,128)(2,1)S(1)} %shard_map.128.a_ref), channel_id=1, source_target_pairs={{0,16},{4,20},{8,24},{12,28},{16,0},{20,4},{24,8},{28,12},{1,17},{... | collective-permute-start | bytes 393224 | tf_op jit(solution)/shard_map/ppermute | solution.py:334
  29.9 1.4 %collective-permute-start.7 = (bf16[4,128,128]{2,1,0:T(8,128)(2,1)S(1)}, bf16[4,128,128]{2,1,0:T(8,128)(2,1)S(1)}, u32[]{:S(2)}, u32[]{:S(2)}) collective-permute-start(bf16[4,128,128]{2,1,0:T(8,128)(2,1)S(1)} %shard_map.128.a_ref), channel_id=1, source_target_pairs={{0,24},{4,28},{8,16},{12,20},{16,8},{20,12},{24,0},{28,4},{1,25},{... | collective-permute-start | bytes 393224 | tf_op jit(solution)/shard_map/ppermute | solution.py:334
  31.3 0.0 collective-permute-done.8.other_ref
  31.3 0.9 collective-permute-done.5.b_ref
  32.2 7.7 %collective-permute-done.6.c_ref = bf16[4,128,128]{2,1,0:T(8,128)(2,1)S(1)} collective-permute-done((bf16[4,128,128]{2,1,0:T(8,128)(2,1)S(1)}, bf16[4,128,128]{2,1,0:T(8,128)(2,1)S(1)}, u32[]{:S(2)}, u32[]{:S(2)}) %collective-permute-start.6) | collective-permute-done | bytes 131104 | tf_op jit(solution)/shard_map/ppermute | solution.py:334
  39.9 1.5 %shard_map.129 = (f32[256,512]{1,0:T(8,128)S(1)}, bf16[256,512]{1,0:T(8,128)(2,1)S(1)}) custom-call(bf16[4,128,128]{2,1,0:T(8,128)(2,1)S(1)} %shard_map.128.a_ref, bf16[4,128,128]{2,1,0:T(8,128)(2,1)S(1)} %collective-permute-done.5.b_ref, bf16[4,128,128]{2,1,0:T(8,128)(2,1)S(1)} %collective-permute-done.6.c_ref, ...), custom_call_target="tpu_custom_call" | custom-call | tf_op jit(solution)/shard_map/pallas_call | solution.py:303
  41.4 0.1 collective-permute-start.9
  41.5 1.1 slice.134
  42.6 2.0 %collective-permute-start.18 = (bf16[160,1408]{1,0:T(8,128)(2,1)S(1)}, bf16[160,1408]{1,0:T(8,128)(2,1)S(1)}, u32[]{:S(2)}, u32[]{:S(2)}) collective-permute-start(bf16[160,1408]{1,0:T(8,128)(2,1)S(1)} %slice.134), channel_id=1, source_target_pairs={{0,8},{4,12},{8,0},{12,4},{16,24},{20,28},{24,16},{28,20},{1,9},{5... | collective-permute-start | bytes 1351688 | tf_op jit(solution)/shard_map/ppermute | solution.py:334
  44.6 0.0 collective-permute-done.9
  44.6 0.1 convert_add_fusion.1
  44.7 1.6 %collective-permute-start.10 = (bf16[128,512]{1,0:T(8,128)(2,1)S(1)}, bf16[128,512]{1,0:T(8,128)(2,1)S(1)}, u32[]{:S(2)}, u32[]{:S(2)}) collective-permute-start(bf16[128,512]{1,0:T(8,128)(2,1)S(1)} %slice.216), channel_id=1, source_target_pairs={{0,2},{1,3},{2,0},{3,1},{4,6},{5,7},{6,4},{7,5},{8,10},{9,11},{10,... | collective-permute-start | bytes 393224 | tf_op jit(solution)/shard_map/ppermute | solution.py:334
  46.3 0.7 collective-permute-start.19
  47.0 3.3 %collective-permute-start.23 = (bf16[96,1408]{1,0:T(8,128)(2,1)S(1)}, bf16[96,1408]{1,0:T(8,128)(2,1)S(1)}, u32[]{:S(2)}, u32[]{:S(2)}) collective-permute-start(bf16[96,1408]{1,0:T(8,128)(2,1)S(1)} %slice.135), channel_id=1, source_target_pairs={{0,8},{4,12},{8,0},{12,4},{16,24},{20,28},{24,16},{28,20},{1,9},{5... | collective-permute-start | bytes 811016 | tf_op jit(solution)/shard_map/ppermute | solution.py:334
  50.3 5.6 %collective-permute-done.18.refs_0_ = bf16[160,1408]{1,0:T(8,128)(2,1)S(1)} collective-permute-done((bf16[160,1408]{1,0:T(8,128)(2,1)S(1)}, bf16[160,1408]{1,0:T(8,128)(2,1)S(1)}, u32[]{:S(2)}, u32[]{:S(2)}) %collective-permute-start.18) | collective-permute-done | bytes 450592 | tf_op jit(solution)/shard_map/ppermute | solution.py:334
  55.8 0.7 collective-permute-start.21
  56.6 4.8 %collective-permute-start.13 = (bf16[32,512]{1,0:T(8,128)(2,1)S(1)}, bf16[32,512]{1,0:T(8,128)(2,1)S(1)}, u32[]{:S(2)}, u32[]{:S(2)}) collective-permute-start(bf16[32,512]{1,0:T(8,128)(2,1)S(1)} %get-tuple-element.48), channel_id=1, source_target_pairs={{0,8},{4,12},{8,0},{12,4},{16,24},{20,28},{24,16},{28,20},{1,9},{5... | collective-permute-start | bytes 98312 | tf_op jit(solution)/shard_map/ppermute | solution.py:334
  61.4 1.3 %collective-permute-start.11 = (bf16[32,512]{1,0:T(8,128)(2,1)S(1)}, bf16[32,512]{1,0:T(8,128)(2,1)S(1)}, u32[]{:S(2)}, u32[]{:S(2)}) collective-permute-start(bf16[32,512]{1,0:T(8,128)(2,1)S(1)} %get-tuple-element.50), channel_id=1, source_target_pairs={{0,24},{4,28},{8,16},{12,20},{16,8},{20,12},{24,0},{28,4},{1,25},{... | collective-permute-start | bytes 98312 | tf_op jit(solution)/shard_map/ppermute | solution.py:334
  62.8 0.5 collective-permute-done.13
  63.3 2.1 %collective-permute-start.12 = (bf16[32,512]{1,0:T(8,128)(2,1)S(1)}, bf16[32,512]{1,0:T(8,128)(2,1)S(1)}, u32[]{:S(2)}, u32[]{:S(2)}) collective-permute-start(bf16[32,512]{1,0:T(8,128)(2,1)S(1)} %get-tuple-element.49), channel_id=1, source_target_pairs={{0,16},{4,20},{8,24},{12,28},{16,0},{20,4},{24,8},{28,12},{1,17},{... | collective-permute-start | bytes 98312 | tf_op jit(solution)/shard_map/ppermute | solution.py:334
  65.5 1.9 %collective-permute-done.11 = bf16[32,512]{1,0:T(8,128)(2,1)S(1)} collective-permute-done((bf16[32,512]{1,0:T(8,128)(2,1)S(1)}, bf16[32,512]{1,0:T(8,128)(2,1)S(1)}, u32[]{:S(2)}, u32[]{:S(2)}) %collective-permute-start.11) | collective-permute-done | bytes 32800 | tf_op jit(solution)/shard_map/ppermute | solution.py:334
  67.3 6.0 %collective-permute-done.12 = bf16[32,512]{1,0:T(8,128)(2,1)S(1)} collective-permute-done((bf16[32,512]{1,0:T(8,128)(2,1)S(1)}, bf16[32,512]{1,0:T(8,128)(2,1)S(1)}, u32[]{:S(2)}, u32[]{:S(2)}) %collective-permute-start.12) | collective-permute-done | bytes 32800 | tf_op jit(solution)/shard_map/ppermute | solution.py:334
  73.4 0.2 fusion
  73.6 0.1 fusion.2
  73.7 1.6 %collective-permute-start.14 = (bf16[32,2048]{1,0:T(8,128)(2,1)S(1)}, bf16[32,2048]{1,0:T(8,128)(2,1)S(1)}, u32[]{:S(2)}, u32[]{:S(2)}) collective-permute-start(bf16[32,2048]{1,0:T(8,128)(2,1)S(1)} %fusion.2), channel_id=1, source_target_pairs={{0,2},{1,3},{2,0},{3,1},{4,6},{5,7},{6,4},{7,5},{8,10},{9,11},{10,... | collective-permute-start | bytes 393224 | tf_op jit(solution)/shard_map/ppermute | solution.py:334
  75.3 1.5 %collective-permute-start.15 = (bf16[32,2048]{1,0:T(8,128)(2,1)S(1)}, bf16[32,2048]{1,0:T(8,128)(2,1)S(1)}, u32[]{:S(2)}, u32[]{:S(2)}) collective-permute-start(bf16[32,2048]{1,0:T(8,128)(2,1)S(1)} %fusion.2), channel_id=1, source_target_pairs={{0,4},{4,0},{8,12},{12,8},{16,20},{20,16},{24,28},{28,24},{1,5},{5... | collective-permute-start | bytes 393224 | tf_op jit(solution)/shard_map/ppermute | solution.py:334
  76.8 0.5 collective-permute-start.16
  77.3 2.9 %collective-permute-done.14 = bf16[32,2048]{1,0:T(8,128)(2,1)S(1)} collective-permute-done((bf16[32,2048]{1,0:T(8,128)(2,1)S(1)}, bf16[32,2048]{1,0:T(8,128)(2,1)S(1)}, u32[]{:S(2)}, u32[]{:S(2)}) %collective-permute-start.14) | collective-permute-done | bytes 131104 | tf_op jit(solution)/shard_map/ppermute | solution.py:334
  80.1 0.7 collective-permute-start.24
  80.8 0.7 collective-permute-start.26
  81.5 1.1 collective-permute-done.16
  82.7 0.1 collective-permute-start.17
  82.8 1.3 collective-permute-start.20
  84.1 1.3 collective-permute-start.22
  85.4 1.3 collective-permute-start.25
  86.7 1.3 collective-permute-start.27
  88.0 6.0 %shard_map.130.hidden_ref = bf16[256,1408]{1,0:T(8,128)(2,1)S(1)} custom-call(bf16[128,2048]{1,0:T(8,128)(2,1)S(1)} %pad_maximum_fusion.here_ref, bf16[128,2048]{1,0:T(8,128)(2,1)S(1)} %collective-permute-done.17.there_ref, bf16[2048,1408]{1,0:T(8,128)(2,1)} %gate_ref.1, bf16[2048,1408]{1,0:T(8,128)(2,1)} %up_ref.1), custom_call_target="tpu_custom_call" | custom-call | tf_op jit(solution)/shard_map/pallas_call | solution.py:303
  94.1 20.3 %collective-permute-done.25.refs_7_ = bf16[96,1408]{1,0:T(8,128)(2,1)S(1)} collective-permute-done((bf16[96,1408]{1,0:T(8,128)(2,1)S(1)}, bf16[96,1408]{1,0:T(8,128)(2,1)S(1)}, u32[]{:S(2)}, u32[]{:S(2)}) %collective-permute-start.25) | collective-permute-done | bytes 270368 | tf_op jit(solution)/shard_map/ppermute | solution.py:357
  114.3 5.6 %collective-permute-done.27.refs_9_ = bf16[96,1408]{1,0:T(8,128)(2,1)S(1)} collective-permute-done((bf16[96,1408]{1,0:T(8,128)(2,1)S(1)}, bf16[96,1408]{1,0:T(8,128)(2,1)S(1)}, u32[]{:S(2)}, u32[]{:S(2)}) %collective-permute-start.27) | collective-permute-done | bytes 270368 | tf_op jit(solution)/shard_map/ppermute | solution.py:358
  119.9 1.0 shard_map.131
  120.9 0.1 collective-permute-start.28
  121.0 1.5 %collective-permute-done.28 = bf16[128,1024]{1,0:T(8,128)(2,1)S(1)} collective-permute-done((bf16[128,1024]{1,0:T(8,128)(2,1)S(1)}, bf16[128,1024]{1,0:T(8,128)(2,1)S(1)}, u32[]{:S(2)}, u32[]{:S(2)}) %collective-permute-start.28) | collective-permute-done | bytes 262176 | tf_op jit(solution)/shard_map/ppermute | solution.py:334
  122.6 0.1 fusion.15
  122.7 1.1 collective-permute-start.29
  123.8 1.5 %collective-permute-start.30 = (bf16[32,1024]{1,0:T(8,128)(2,1)S(1)}, bf16[32,1024]{1,0:T(8,128)(2,1)S(1)}, u32[]{:S(2)}, u32[]{:S(2)}) collective-permute-start(bf16[32,1024]{1,0:T(8,128)(2,1)S(1)} %get-tuple-element.37), channel_id=1, source_target_pairs={{0,6},{1,7},{2,4},{3,5},{4,2},{5,3},{6,0},{7,1},{8,14},{9,15},{10,... | collective-permute-start | bytes 196616 | tf_op jit(solution)/shard_map/ppermute | solution.py:342
  125.3 0.9 collective-permute-start.31
  126.2 0.8 collective-permute-done.29
  127.0 2.0 %collective-permute-done.30 = bf16[32,1024]{1,0:T(8,128)(2,1)S(1)} collective-permute-done((bf16[32,1024]{1,0:T(8,128)(2,1)S(1)}, bf16[32,1024]{1,0:T(8,128)(2,1)S(1)}, u32[]{:S(2)}, u32[]{:S(2)}) %collective-permute-start.30) | collective-permute-done | bytes 65568 | tf_op jit(solution)/shard_map/ppermute | solution.py:342
  129.0 1.1 collective-permute-done.31
  130.2 0.7 fusion.3
  (45 shorter events, 0.5 us)
Async XLA Ops:
  0.0 47.0 %copy-start = (bf16[256,1408]{1,0:T(8,128)(2,1)S(1)}, bf16[256,1408]{1,0:T(8,128)(2,1)}, u32[]{:S(2)}) copy-start(bf16[256,1408]{1,0:T(8,128)(2,1)} %own_ref.1) | copy-start | bytes 2162692
  0.0 73.4 %copy-start.1 = (bf16[32,2048]{1,0:T(8,128)(2,1)S(1)}, bf16[32,2048]{1,0:T(8,128)(2,1)}, u32[]{:S(2)}) copy-start(bf16[32,2048]{1,0:T(8,128)(2,1)} %param.13) | copy-start | bytes 393220
  0.0 73.6 %copy-start.2 = (f32[2048]{0:T(1024)S(1)}, f32[2048]{0:T(1024)}, u32[]{:S(2)}) copy-start(f32[2048]{0:T(1024)} %param.22) | copy-start | bytes 24580
  1.4 12.0 %collective-permute-start.1 = (bf16[128,384]{1,0:T(8,128)(2,1)S(1)}, bf16[128,384]{1,0:T(8,128)(2,1)S(1)}, u32[]{:S(2)}, u32[]{:S(2)}) collective-permute-start(bf16[128,384]{1,0:T(8,128)(2,1)S(1)} %get-tuple-element.24), channel_id=1, source_target_pairs={{0,16},{4,20},{8,24},{12,28},{16,0},{20,4},{24,8},{28,12},{1,17},{... | collective-permute-start | bytes 294920 | tf_op jit(solution)/shard_map/ppermute | solution.py:334
  5.5 7.9 %collective-permute-start.2 = (bf16[128,384]{1,0:T(8,128)(2,1)S(1)}, bf16[128,384]{1,0:T(8,128)(2,1)S(1)}, u32[]{:S(2)}, u32[]{:S(2)}) collective-permute-start(bf16[128,384]{1,0:T(8,128)(2,1)S(1)} %get-tuple-element.23), channel_id=1, source_target_pairs={{0,24},{4,28},{8,16},{12,20},{16,8},{20,12},{24,0},{28,4},{1,25},{... | collective-permute-start | bytes 294920 | tf_op jit(solution)/shard_map/ppermute | solution.py:334
  6.9 8.3 %collective-permute-start = (bf16[128,384]{1,0:T(8,128)(2,1)S(1)}, bf16[128,384]{1,0:T(8,128)(2,1)S(1)}, u32[]{:S(2)}, u32[]{:S(2)}) collective-permute-start(bf16[128,384]{1,0:T(8,128)(2,1)S(1)} %get-tuple-element.25), channel_id=1, source_target_pairs={{0,8},{4,12},{8,0},{12,4},{16,24},{20,28},{24,16},{28,20},{1,9},{5... | collective-permute-start | bytes 294920 | tf_op jit(solution)/shard_map/ppermute | solution.py:334
  13.5 6.4 %collective-permute-start.4 = (bf16[256,256]{1,0:T(8,128)(2,1)S(1)}, bf16[256,256]{1,0:T(8,128)(2,1)S(1)}, u32[]{:S(2)}, u32[]{:S(2)}) collective-permute-start(bf16[256,256]{1,0:T(8,128)(2,1)S(1)} %pad_maximum_fusion.2), channel_id=1, source_target_pairs={{0,4},{4,0},{8,12},{12,8},{16,20},{20,16},{24,28},{28,24},{1,5},{5... | collective-permute-start | bytes 393224 | tf_op jit(solution)/shard_map/ppermute | solution.py:334
  15.2 7.3 %collective-permute-start.3 = (bf16[256,256]{1,0:T(8,128)(2,1)S(1)}, bf16[256,256]{1,0:T(8,128)(2,1)S(1)}, u32[]{:S(2)}, u32[]{:S(2)}) collective-permute-start(bf16[256,256]{1,0:T(8,128)(2,1)S(1)} %pad_maximum_fusion.1), channel_id=1, source_target_pairs={{0,4},{4,0},{8,12},{12,8},{16,20},{20,16},{24,28},{28,24},{1,5},{5... | collective-permute-start | bytes 393224 | tf_op jit(solution)/shard_map/ppermute | solution.py:334
  15.7 15.6 %collective-permute-start.8 = (bf16[256,512]{1,0:T(8,128)(2,1)}, bf16[256,512]{1,0:T(8,128)(2,1)S(1)}, u32[]{:S(2)}, u32[]{:S(2)}) collective-permute-start(bf16[256,512]{1,0:T(8,128)(2,1)} %source.1), channel_id=1, source_target_pairs={{0,4},{4,0},{8,12},{12,8},{16,20},{20,16},{24,28},{28,24},{1,5},{5... | collective-permute-start | bytes 786440 | tf_op jit(solution)/shard_map/ppermute | solution.py:334
  25.8 6.4 %collective-permute-start.5 = (bf16[4,128,128]{2,1,0:T(8,128)(2,1)S(1)}, bf16[4,128,128]{2,1,0:T(8,128)(2,1)S(1)}, u32[]{:S(2)}, u32[]{:S(2)}) collective-permute-start(bf16[4,128,128]{2,1,0:T(8,128)(2,1)S(1)} %shard_map.128.a_ref), channel_id=1, source_target_pairs={{0,8},{4,12},{8,0},{12,4},{16,24},{20,28},{24,16},{28,20},{1,9},{5... | collective-permute-start | bytes 393224 | tf_op jit(solution)/shard_map/ppermute | solution.py:334
  27.9 12.0 %collective-permute-start.6 = (bf16[4,128,128]{2,1,0:T(8,128)(2,1)S(1)}, bf16[4,128,128]{2,1,0:T(8,128)(2,1)S(1)}, u32[]{:S(2)}, u32[]{:S(2)}) collective-permute-start(bf16[4,128,128]{2,1,0:T(8,128)(2,1)S(1)} %shard_map.128.a_ref), channel_id=1, source_target_pairs={{0,16},{4,20},{8,24},{12,28},{16,0},{20,4},{24,8},{28,12},{1,17},{... | collective-permute-start | bytes 393224 | tf_op jit(solution)/shard_map/ppermute | solution.py:334
  29.9 10.0 %collective-permute-start.7 = (bf16[4,128,128]{2,1,0:T(8,128)(2,1)S(1)}, bf16[4,128,128]{2,1,0:T(8,128)(2,1)S(1)}, u32[]{:S(2)}, u32[]{:S(2)}) collective-permute-start(bf16[4,128,128]{2,1,0:T(8,128)(2,1)S(1)} %shard_map.128.a_ref), channel_id=1, source_target_pairs={{0,24},{4,28},{8,16},{12,20},{16,8},{20,12},{24,0},{28,4},{1,25},{... | collective-permute-start | bytes 393224 | tf_op jit(solution)/shard_map/ppermute | solution.py:334
  41.4 3.2 %collective-permute-start.9 = (bf16[256,512]{1,0:T(8,128)(2,1)S(1)}, bf16[256,512]{1,0:T(8,128)(2,1)S(1)}, u32[]{:S(2)}, u32[]{:S(2)}) collective-permute-start(bf16[256,512]{1,0:T(8,128)(2,1)S(1)} %get-tuple-element.14), channel_id=1, source_target_pairs={{0,1},{1,0},{2,3},{3,2},{4,5},{5,4},{6,7},{7,6},{8,9},{9,8},{10,11... | collective-permute-start | bytes 786440 | tf_op jit(solution)/shard_map/ppermute | solution.py:334
  42.6 13.3 %collective-permute-start.18 = (bf16[160,1408]{1,0:T(8,128)(2,1)S(1)}, bf16[160,1408]{1,0:T(8,128)(2,1)S(1)}, u32[]{:S(2)}, u32[]{:S(2)}) collective-permute-start(bf16[160,1408]{1,0:T(8,128)(2,1)S(1)} %slice.134), channel_id=1, source_target_pairs={{0,8},{4,12},{8,0},{12,4},{16,24},{20,28},{24,16},{28,20},{1,9},{5... | collective-permute-start | bytes 1351688 | tf_op jit(solution)/shard_map/ppermute | solution.py:334
  44.7 11.8 %collective-permute-start.10 = (bf16[128,512]{1,0:T(8,128)(2,1)S(1)}, bf16[128,512]{1,0:T(8,128)(2,1)S(1)}, u32[]{:S(2)}, u32[]{:S(2)}) collective-permute-start(bf16[128,512]{1,0:T(8,128)(2,1)S(1)} %slice.216), channel_id=1, source_target_pairs={{0,2},{1,3},{2,0},{3,1},{4,6},{5,7},{6,4},{7,5},{8,10},{9,11},{10,... | collective-permute-start | bytes 393224 | tf_op jit(solution)/shard_map/ppermute | solution.py:334
  46.3 36.5 %collective-permute-start.19 = (bf16[160,1408]{1,0:T(8,128)(2,1)S(1)}, bf16[160,1408]{1,0:T(8,128)(2,1)S(1)}, u32[]{:S(2)}, u32[]{:S(2)}) collective-permute-start(bf16[160,1408]{1,0:T(8,128)(2,1)S(1)} %slice.134), channel_id=1, source_target_pairs={{8,16},{12,20},{16,8},{20,12},{9,17},{13,21},{17,9},{21,13},{10,18... | collective-permute-start | bytes 1351688 | tf_op jit(solution)/shard_map/ppermute | solution.py:355
  47.0 29.8 %collective-permute-start.23 = (bf16[96,1408]{1,0:T(8,128)(2,1)S(1)}, bf16[96,1408]{1,0:T(8,128)(2,1)S(1)}, u32[]{:S(2)}, u32[]{:S(2)}) collective-permute-start(bf16[96,1408]{1,0:T(8,128)(2,1)S(1)} %slice.135), channel_id=1, source_target_pairs={{0,8},{4,12},{8,0},{12,4},{16,24},{20,28},{24,16},{28,20},{1,9},{5... | collective-permute-start | bytes 811016 | tf_op jit(solution)/shard_map/ppermute | solution.py:334
  55.8 28.3 %collective-permute-start.21 = (bf16[160,1408]{1,0:T(8,128)(2,1)S(1)}, bf16[160,1408]{1,0:T(8,128)(2,1)S(1)}, u32[]{:S(2)}, u32[]{:S(2)}) collective-permute-start(bf16[160,1408]{1,0:T(8,128)(2,1)S(1)} %collective-permute-done.18.refs_0_), channel_id=1, source_target_pairs={{8,16},{12,20},{16,8},{20,12},{9,17},{13,21},{17,9},{21,13},{10,18... | collective-permute-start | bytes 1351688 | tf_op jit(solution)/shard_map/ppermute | solution.py:356
  56.6 6.7 %collective-permute-start.13 = (bf16[32,512]{1,0:T(8,128)(2,1)S(1)}, bf16[32,512]{1,0:T(8,128)(2,1)S(1)}, u32[]{:S(2)}, u32[]{:S(2)}) collective-permute-start(bf16[32,512]{1,0:T(8,128)(2,1)S(1)} %get-tuple-element.48), channel_id=1, source_target_pairs={{0,8},{4,12},{8,0},{12,4},{16,24},{20,28},{24,16},{28,20},{1,9},{5... | collective-permute-start | bytes 98312 | tf_op jit(solution)/shard_map/ppermute | solution.py:334
  61.4 5.9 %collective-permute-start.11 = (bf16[32,512]{1,0:T(8,128)(2,1)S(1)}, bf16[32,512]{1,0:T(8,128)(2,1)S(1)}, u32[]{:S(2)}, u32[]{:S(2)}) collective-permute-start(bf16[32,512]{1,0:T(8,128)(2,1)S(1)} %get-tuple-element.50), channel_id=1, source_target_pairs={{0,24},{4,28},{8,16},{12,20},{16,8},{20,12},{24,0},{28,4},{1,25},{... | collective-permute-start | bytes 98312 | tf_op jit(solution)/shard_map/ppermute | solution.py:334
  63.3 10.0 %collective-permute-start.12 = (bf16[32,512]{1,0:T(8,128)(2,1)S(1)}, bf16[32,512]{1,0:T(8,128)(2,1)S(1)}, u32[]{:S(2)}, u32[]{:S(2)}) collective-permute-start(bf16[32,512]{1,0:T(8,128)(2,1)S(1)} %get-tuple-element.49), channel_id=1, source_target_pairs={{0,16},{4,20},{8,24},{12,28},{16,0},{20,4},{24,8},{28,12},{1,17},{... | collective-permute-start | bytes 98312 | tf_op jit(solution)/shard_map/ppermute | solution.py:334
  73.7 6.4 %collective-permute-start.14 = (bf16[32,2048]{1,0:T(8,128)(2,1)S(1)}, bf16[32,2048]{1,0:T(8,128)(2,1)S(1)}, u32[]{:S(2)}, u32[]{:S(2)}) collective-permute-start(bf16[32,2048]{1,0:T(8,128)(2,1)S(1)} %fusion.2), channel_id=1, source_target_pairs={{0,2},{1,3},{2,0},{3,1},{4,6},{5,7},{6,4},{7,5},{8,10},{9,11},{10,... | collective-permute-start | bytes 393224 | tf_op jit(solution)/shard_map/ppermute | solution.py:334
  75.3 5.5 %collective-permute-start.15 = (bf16[32,2048]{1,0:T(8,128)(2,1)S(1)}, bf16[32,2048]{1,0:T(8,128)(2,1)S(1)}, u32[]{:S(2)}, u32[]{:S(2)}) collective-permute-start(bf16[32,2048]{1,0:T(8,128)(2,1)S(1)} %fusion.2), channel_id=1, source_target_pairs={{0,4},{4,0},{8,12},{12,8},{16,20},{20,16},{24,28},{28,24},{1,5},{5... | collective-permute-start | bytes 393224 | tf_op jit(solution)/shard_map/ppermute | solution.py:334
  76.8 5.9 %collective-permute-start.16 = (bf16[32,2048]{1,0:T(8,128)(2,1)S(1)}, bf16[32,2048]{1,0:T(8,128)(2,1)S(1)}, u32[]{:S(2)}, u32[]{:S(2)}) collective-permute-start(bf16[32,2048]{1,0:T(8,128)(2,1)S(1)} %fusion.2), channel_id=1, source_target_pairs={{0,6},{1,7},{2,4},{3,5},{4,2},{5,3},{6,0},{7,1},{8,14},{9,15},{10,... | collective-permute-start | bytes 393224 | tf_op jit(solution)/shard_map/ppermute | solution.py:342
  80.1 5.3 %collective-permute-start.24 = (bf16[96,1408]{1,0:T(8,128)(2,1)S(1)}, bf16[96,1408]{1,0:T(8,128)(2,1)S(1)}, u32[]{:S(2)}, u32[]{:S(2)}) collective-permute-start(bf16[96,1408]{1,0:T(8,128)(2,1)S(1)} %slice.135), channel_id=1, source_target_pairs={{8,16},{12,20},{16,8},{20,12},{9,17},{13,21},{17,9},{21,13},{10,18... | collective-permute-start | bytes 811016 | tf_op jit(solution)/shard_map/ppermute | solution.py:355
  80.8 5.9 %collective-permute-start.26 = (bf16[96,1408]{1,0:T(8,128)(2,1)S(1)}, bf16[96,1408]{1,0:T(8,128)(2,1)S(1)}, u32[]{:S(2)}, u32[]{:S(2)}) collective-permute-start(bf16[96,1408]{1,0:T(8,128)(2,1)S(1)} %collective-permute-done.23.refs_5_), channel_id=1, source_target_pairs={{8,16},{12,20},{16,8},{20,12},{9,17},{13,21},{17,9},{21,13},{10,18... | collective-permute-start | bytes 811016 | tf_op jit(solution)/shard_map/ppermute | solution.py:356
  82.7 5.3 %collective-permute-start.17 = (bf16[128,2048]{1,0:T(8,128)(2,1)S(1)}, bf16[128,2048]{1,0:T(8,128)(2,1)S(1)}, u32[]{:S(2)}, u32[]{:S(2)}) collective-permute-start(bf16[128,2048]{1,0:T(8,128)(2,1)S(1)} %pad_maximum_fusion.here_ref), channel_id=1, source_target_pairs={{0,1},{1,0},{2,3},{3,2},{4,5},{5,4},{6,7},{7,6},{8,9},{9,8},{10,11... | collective-permute-start | bytes 1572872 | tf_op jit(solution)/shard_map/ppermute | solution.py:334
  82.8 37.1 %collective-permute-start.20 = (bf16[160,1408]{1,0:T(8,128)(2,1)S(1)}, bf16[160,1408]{1,0:T(8,128)(2,1)S(1)}, u32[]{:S(2)}, u32[]{:S(2)}) collective-permute-start(bf16[160,1408]{1,0:T(8,128)(2,1)S(1)} %collective-permute-done.19.refs_1_), channel_id=1, source_target_pairs={{8,0},{12,4},{16,24},{20,28},{9,1},{13,5},{17,25},{21,29},{10,2},{... | collective-permute-start | bytes 1351688 | tf_op jit(solution)/shard_map/ppermute | solution.py:357
  84.1 35.8 %collective-permute-start.22 = (bf16[160,1408]{1,0:T(8,128)(2,1)S(1)}, bf16[160,1408]{1,0:T(8,128)(2,1)S(1)}, u32[]{:S(2)}, u32[]{:S(2)}) collective-permute-start(bf16[160,1408]{1,0:T(8,128)(2,1)S(1)} %collective-permute-done.21.refs_3_), channel_id=1, source_target_pairs={{8,0},{12,4},{16,24},{20,28},{9,1},{13,5},{17,25},{21,29},{10,2},{... | collective-permute-start | bytes 1351688 | tf_op jit(solution)/shard_map/ppermute | solution.py:358
  85.4 28.9 %collective-permute-start.25 = (bf16[96,1408]{1,0:T(8,128)(2,1)S(1)}, bf16[96,1408]{1,0:T(8,128)(2,1)S(1)}, u32[]{:S(2)}, u32[]{:S(2)}) collective-permute-start(bf16[96,1408]{1,0:T(8,128)(2,1)S(1)} %collective-permute-done.24.refs_6_), channel_id=1, source_target_pairs={{8,0},{12,4},{16,24},{20,28},{9,1},{13,5},{17,25},{21,29},{10,2},{... | collective-permute-start | bytes 811016 | tf_op jit(solution)/shard_map/ppermute | solution.py:357
  86.7 33.2 %collective-permute-start.27 = (bf16[96,1408]{1,0:T(8,128)(2,1)S(1)}, bf16[96,1408]{1,0:T(8,128)(2,1)S(1)}, u32[]{:S(2)}, u32[]{:S(2)}) collective-permute-start(bf16[96,1408]{1,0:T(8,128)(2,1)S(1)} %collective-permute-done.26.refs_8_), channel_id=1, source_target_pairs={{8,0},{12,4},{16,24},{20,28},{9,1},{13,5},{17,25},{21,29},{10,2},{... | collective-permute-start | bytes 811016 | tf_op jit(solution)/shard_map/ppermute | solution.py:358
  120.9 1.6 %collective-permute-start.28 = (bf16[128,1024]{1,0:T(8,128)(2,1)S(1)}, bf16[128,1024]{1,0:T(8,128)(2,1)S(1)}, u32[]{:S(2)}, u32[]{:S(2)}) collective-permute-start(bf16[128,1024]{1,0:T(8,128)(2,1)S(1)} %get-tuple-element.16), channel_id=1, source_target_pairs={{0,1},{1,0},{2,3},{3,2},{4,5},{5,4},{6,7},{7,6},{8,9},{9,8},{10,11... | collective-permute-start | bytes 786440 | tf_op jit(solution)/shard_map/ppermute | solution.py:334
  122.7 4.3 %collective-permute-start.29 = (bf16[32,1024]{1,0:T(8,128)(2,1)S(1)}, bf16[32,1024]{1,0:T(8,128)(2,1)S(1)}, u32[]{:S(2)}, u32[]{:S(2)}) collective-permute-start(bf16[32,1024]{1,0:T(8,128)(2,1)S(1)} %get-tuple-element.35), channel_id=1, source_target_pairs={{0,4},{4,0},{8,12},{12,8},{16,20},{20,16},{24,28},{28,24},{1,5},{5... | collective-permute-start | bytes 196616 | tf_op jit(solution)/shard_map/ppermute | solution.py:334
  123.8 5.2 %collective-permute-start.30 = (bf16[32,1024]{1,0:T(8,128)(2,1)S(1)}, bf16[32,1024]{1,0:T(8,128)(2,1)S(1)}, u32[]{:S(2)}, u32[]{:S(2)}) collective-permute-start(bf16[32,1024]{1,0:T(8,128)(2,1)S(1)} %get-tuple-element.37), channel_id=1, source_target_pairs={{0,6},{1,7},{2,4},{3,5},{4,2},{5,3},{6,0},{7,1},{8,14},{9,15},{10,... | collective-permute-start | bytes 196616 | tf_op jit(solution)/shard_map/ppermute | solution.py:342
  125.3 4.8 %collective-permute-start.31 = (bf16[32,1024]{1,0:T(8,128)(2,1)S(1)}, bf16[32,1024]{1,0:T(8,128)(2,1)S(1)}, u32[]{:S(2)}, u32[]{:S(2)}) collective-permute-start(bf16[32,1024]{1,0:T(8,128)(2,1)S(1)} %get-tuple-element.36), channel_id=1, source_target_pairs={{0,2},{1,3},{2,0},{3,1},{4,6},{5,7},{6,4},{7,5},{8,10},{9,11},{10,... | collective-permute-start | bytes 196616 | tf_op jit(solution)/shard_map/ppermute | solution.py:334

commit v4 on v3

--- a/solution.py
+++ b/solution.py
@@ -260,33 +260,26 @@
         hidden_ref[:, start : start + gate.shape[1]] = hidden.astype(hidden_ref.dtype)
 
 
-def down_body(hidden_ref, own_ref, *refs, sp_size):
-    parts, (kept_ref, sent_ref) = refs[:-2], refs[-2:]
-    parts = [parts[start : start + 5] for start in range(0, len(parts), 5)]
+def down_body(hidden_ref, *refs, pieces, sp_size):
+    kept_ref, sent_ref = refs[-2:]
+    refs = list(refs[:-2])
     place = lax.axis_index("sp") // 2
     inner = (place > 0) & (place < sp_size // 2 - 1)
     rows = kept_ref.shape[0]
-    width = own_ref.shape[0]
-
-    def third(part):
-        return jnp.where(inner, part[1][...], part[2][...])
-
-    def last(part):
-        return jnp.where(inner, part[3][...], part[4][...])
-
-    pieces = (
-        lambda: own_ref[...],
-        lambda: jnp.concatenate([part[0][...] for part in parts], axis=0),
-        lambda: jnp.concatenate([third(part) for part in parts], axis=0),
-        lambda: jnp.concatenate([last(part) for part in parts], axis=0),
-    )
-    for index, piece in enumerate(pieces):
+    start = 0
+    for parts, choices in pieces:
+        values = []
+        for _ in range(parts):
+            part = [refs.pop(0)[...] for _ in range(choices)]
+            values.append(part[0] if choices == 1 else jnp.where(inner, *part))
+        piece = values[0] if parts == 1 else jnp.concatenate(values, axis=0)
         product = lax.dot_general(
-            hidden_ref[...], piece(), (((1,), (1,)), ((), ())), preferred_element_type=jnp.float32
-        )
-        columns = slice(index * width, (index + 1) * width)
+            hidden_ref[...], piece, (((1,), (1,)), ((), ())), preferred_element_type=jnp.float32
+        )
+        columns = slice(start, start + piece.shape[0])
         kept_ref[:, columns] = product[:rows]
         sent_ref[:, columns] = product[rows:].astype(sent_ref.dtype)
+        start += piece.shape[0]
 
 
 def kernel(body, out_shape, near, away=(), scratch=(), limit=16):
@@ -389,21 +382,17 @@
         blocks = [side_by_side(block[:, :middle], block[:, middle:]) for block in blocks]
         return jnp.concatenate(planes_by_distance(blocks), axis=1)
 
-    def scatter_sum(ours, given_away, ordered):
+    def side_parts(ours, given_away):
         ours = ours + swap(given_away, "tp", core).astype(f32)
         rows = ours.shape[0] // 4
         rounded = ours.astype(bf16)
         from_both = swap_both(rounded[3 * rows :], side, chip)
         from_side = swap(rounded[2 * rows : 3 * rows], "sp", side)
         from_chip = swap(rounded[rows : 2 * rows], "tp", chip)
-        same = ours[:rows] + from_chip.astype(f32)
-        other = from_side.astype(f32) + from_both.astype(f32)
-        piece = same.shape[1] // planes
-        joined = []
-        for k in range(planes):
-            a, b = (array[:, k * piece : (k + 1) * piece] for array in (same, other))
-            joined.append(side_by_side(a, b))
-        return jnp.concatenate(ordered(joined), axis=1)
+        return ours[:rows], from_chip, from_side, from_both
+
+    def side_sum(own, from_chip, from_side, from_both):
+        return own + from_chip.astype(f32), from_side.astype(f32) + from_both.astype(f32)
 
     tokens = query_first.shape[0]
     rows = tokens // tp_size
@@ -474,15 +463,31 @@
         + [pltpu.SemaphoreType.DMA((len(sizes),))],
         limit=24,
     )
-    half = (4 * rows, width // 2)
-    halves = (jax.ShapeDtypeStruct(half, f32), jax.ShapeDtypeStruct(half, bf16))
     middle = down_weight.shape[0] * 5 // 8
-    fed = kernel(
-        functools.partial(down_body, sp_size=sp_size),
-        halves,
-        (hidden, down_weight, *along_line(down_weight[:middle]), *along_line(down_weight[middle:])),
-    )
-    return (stream + scatter_sum(*fed, planes_along_line)).astype(bf16)
+    ways = [along_line(down_weight[:middle]), along_line(down_weight[middle:])]
+
+    def project_down(pieces, operands, columns):
+        shape = (4 * rows, columns)
+        parts = kernel(
+            functools.partial(down_body, pieces=pieces, sp_size=sp_size),
+            (jax.ShapeDtypeStruct(shape, f32), jax.ShapeDtypeStruct(shape, bf16)),
+            (hidden, *operands),
+        )
+        return side_parts(*parts)
+
+    piece = down_weight.shape[0]
+    early_refs = [down_weight, *(way[0] for way in ways)]
+    early_refs += [ref for way in ways for ref in way[1:3]]
+    first = project_down(((1, 1), (2, 1), (2, 2)), early_refs, 3 * piece)
+    last = project_down(((2, 2),), [ref for way in ways for ref in way[3:5]], piece)
+    first, last = lax.optimization_barrier((first, last))
+    first, last = side_sum(*first), side_sum(*last)
+    joined = [
+        side_by_side(*(array[:, k * piece : (k + 1) * piece] for array in first)) for k in range(3)
+    ]
+    joined.append(side_by_side(*last))
+    fed = jnp.concatenate(planes_along_line(joined), axis=1)
+    return (stream + fed).astype(bf16)
 
 
 def solution(mesh):

time: 131 us -> 132 us (level)
    ppermute x2, waiting for transfers between devices: 5.59 us -> 21.8 us  [along_line(): outer_two = lax.ppermute(middle_two, 'sp', outward_pairs)]
    ppermute x2, waiting for transfers between devices: 20.3 us -> 4.79 us  [along_line(): outer_one = lax.ppermute(middle_one, 'sp', outward_pairs)]
    ppermute x2 -> x3, starting transfers between devices: 1.97 us -> 5.43 us  [swap_both(): return lax.ppermute(array, ('sp', 'tp'), pairs)]
    ppermute x22 -> x25, starting transfers between devices: 35.6 us -> 32.7 us  [swap(): return lax.ppermute(array, axis, [(i, i ^ distance) for i in range(count)])]
    ppermute x22 -> x25, waiting for transfers between devices: 40.4 us -> 38.6 us  [swap(): return lax.ppermute(array, axis, [(i, i ^ distance) for i in range(count)])]
    ppermute x2 -> x3, waiting for transfers between devices: 3.16 us -> 3.87 us  [swap_both(): return lax.ppermute(array, ('sp', 'tp'), pairs)]
    pallas_call x5 -> x6, Pallas kernels: 13.1 us -> 13.3 us  [kernel(): call(*near, *(pltpu.with_memory_space_constraint(array, pltpu.HBM) for ar...]
  transfers between devices with their start and end apart: 32 -> 36, of which waited for: 17 -> 16; matrix products, arithmetic and copies ran while one was open for 1% -> 1% of each run, Pallas kernels for 7% -> 8%
where the time goes in v4:
time: 132 us; the launch traced here: 131 us
  waiting for transfers between devices  69.1 us (52%)
  starting transfers between devices  46 us (35%)
  Pallas kernels  13.3 us (10%)
  other arithmetic  1.37 us (1%)
    ppermute x25, waiting for transfers between devices, swap(): return lax.ppermute(array, axis, [(i, i ^ distance) for i in range(count)])  38.6 us
    ppermute x25, starting transfers between devices, swap(): return lax.ppermute(array, axis, [(i, i ^ distance) for i in range(count)])  32.7 us
    ppermute x2, waiting for transfers between devices, along_line(): outer_two = lax.ppermute(middle_two, 'sp', outward_pairs)  21.8 us
    pallas_call x6, Pallas kernels, kernel(): call(*near, *(pltpu.with_memory_space_constraint(array, pltpu.HBM) for ar...  13.3 us
    ppermute x3, starting transfers between devices, swap_both(): return lax.ppermute(array, ('sp', 'tp'), pairs)  5.43 us
    ppermute x2, waiting for transfers between devices, along_line(): outer_one = lax.ppermute(middle_one, 'sp', outward_pairs)  4.79 us
    ppermute x3, waiting for transfers between devices, swap_both(): return lax.ppermute(array, ('sp', 'tp'), pairs)  3.87 us
  transfers between devices with their start and end apart: 36, of which 16 were waited for; matrix products, arithmetic and copies ran while one was open for 1% of the time, Pallas kernels for 8%

profile of v4, /device:TPU:0, one launch (start us, length us, event | category | flops | bytes accessed | tf_op | source)
XLA Modules:
  0.0 131.4 jit_solution(15940841573498263394)
XLA Ops:
  0.0 1.3 %shard_map.127 = (bf16[4,128,384]{2,1,0:T(8,128)(2,1)S(1)}, f32[2,128]{1,0:T(2,128)S(1)}) custom-call(bf16[128,256]{1,0:T(8,128)(2,1)} %refs_0_.2, bf16[128,256]{1,0:T(8,128)(2,1)} %refs_1_.1, bf16[128,256]{1,0:T(8,128)(2,1)} %refs_2_.1, bf16[128,256]{1,0:T(8,128)(2,1)} %refs_3_.1, bf16[128,512]{1,0:T(8,128)(2,1)} %refs_4_.1, f32[1,128]{1,0:T(1,128)} %bitcast.9, ...), custom_call_target="tpu_custom_call" | custom-call | tf_op jit(solution)/shard_map/pallas_call | solution.py:296
  1.4 3.1 %collective-permute-start = (bf16[128,384]{1,0:T(8,128)(2,1)S(1)}, bf16[128,384]{1,0:T(8,128)(2,1)S(1)}, u32[]{:S(2)}, u32[]{:S(2)}) collective-permute-start(bf16[128,384]{1,0:T(8,128)(2,1)S(1)} %get-tuple-element.47), channel_id=1, source_target_pairs={{0,8},{4,12},{8,0},{12,4},{16,24},{20,28},{24,16},{28,20},{1,9},{5... | collective-permute-start | bytes 294920 | tf_op jit(solution)/shard_map/ppermute | solution.py:327
  4.5 2.6 %collective-permute-start.1 = (bf16[128,384]{1,0:T(8,128)(2,1)S(1)}, bf16[128,384]{1,0:T(8,128)(2,1)S(1)}, u32[]{:S(2)}, u32[]{:S(2)}) collective-permute-start(bf16[128,384]{1,0:T(8,128)(2,1)S(1)} %get-tuple-element.46), channel_id=1, source_target_pairs={{0,16},{4,20},{8,24},{12,28},{16,0},{20,4},{24,8},{28,12},{1,17},{... | collective-permute-start | bytes 294920 | tf_op jit(solution)/shard_map/ppermute | solution.py:327
  7.1 0.2 collective-permute-done.b_ref
  7.3 1.8 %collective-permute-start.3 = (bf16[256,256]{1,0:T(8,128)(2,1)S(1)}, bf16[256,256]{1,0:T(8,128)(2,1)S(1)}, u32[]{:S(2)}, u32[]{:S(2)}) collective-permute-start(bf16[256,256]{1,0:T(8,128)(2,1)S(1)} %pad_maximum_fusion.1), channel_id=1, source_target_pairs={{0,4},{4,0},{8,12},{12,8},{16,20},{20,16},{24,28},{28,24},{1,5},{5... | collective-permute-start | bytes 393224 | tf_op jit(solution)/shard_map/ppermute | solution.py:327
  9.1 4.6 %collective-permute-done.2.d_ref = bf16[128,384]{1,0:T(8,128)(2,1)S(1)} collective-permute-done((bf16[128,384]{1,0:T(8,128)(2,1)S(1)}, bf16[128,384]{1,0:T(8,128)(2,1)S(1)}, u32[]{:S(2)}, u32[]{:S(2)}) %collective-permute-start.2) | collective-permute-done | bytes 98336 | tf_op jit(solution)/shard_map/ppermute | solution.py:327
  13.7 1.2 collective-permute-done.1.c_ref
  14.9 1.6 %collective-permute-start.4 = (bf16[256,256]{1,0:T(8,128)(2,1)S(1)}, bf16[256,256]{1,0:T(8,128)(2,1)S(1)}, u32[]{:S(2)}, u32[]{:S(2)}) collective-permute-start(bf16[256,256]{1,0:T(8,128)(2,1)S(1)} %pad_maximum_fusion.2), channel_id=1, source_target_pairs={{0,4},{4,0},{8,12},{12,8},{16,20},{20,16},{24,28},{28,24},{1,5},{5... | collective-permute-start | bytes 393224 | tf_op jit(solution)/shard_map/ppermute | solution.py:327
  16.5 0.5 collective-permute-start.8
  17.0 0.0 collective-permute-done.3.ab_ref
  17.0 4.3 %collective-permute-done.4.cd_ref = bf16[256,256]{1,0:T(8,128)(2,1)S(1)} collective-permute-done((bf16[256,256]{1,0:T(8,128)(2,1)S(1)}, bf16[256,256]{1,0:T(8,128)(2,1)S(1)}, u32[]{:S(2)}, u32[]{:S(2)}) %collective-permute-start.4) | collective-permute-done | bytes 131104 | tf_op jit(solution)/shard_map/ppermute | solution.py:327
  21.3 3.2 %shard_map.128.a_ref = bf16[4,128,128]{2,1,0:T(8,128)(2,1)S(1)} custom-call(f32[2,128]{1,0:T(2,128)S(1)} %get-tuple-element.21.extra_ref, bf16[128,384]{1,0:T(8,128)(2,1)S(1)} %get-tuple-element.48.a_ref, bf16[128,384]{1,0:T(8,128)(2,1)S(1)} %collective-permute-done.b_ref, bf16[128,384]{1,0:T(8,128)(2,1)S(1)} %collective-permute-done.1.c_ref, ...), custom_call_target="tpu_custom_call" | custom-call | tf_op jit(solution)/shard_map/pallas_call | solution.py:296
  24.5 1.8 %collective-permute-start.5 = (bf16[4,128,128]{2,1,0:T(8,128)(2,1)S(1)}, bf16[4,128,128]{2,1,0:T(8,128)(2,1)S(1)}, u32[]{:S(2)}, u32[]{:S(2)}) collective-permute-start(bf16[4,128,128]{2,1,0:T(8,128)(2,1)S(1)} %shard_map.128.a_ref), channel_id=1, source_target_pairs={{0,8},{4,12},{8,0},{12,4},{16,24},{20,28},{24,16},{28,20},{1,9},{5... | collective-permute-start | bytes 393224 | tf_op jit(solution)/shard_map/ppermute | solution.py:327
  26.3 1.1 collective-permute-start.6
  27.4 1.6 %collective-permute-start.7 = (bf16[4,128,128]{2,1,0:T(8,128)(2,1)S(1)}, bf16[4,128,128]{2,1,0:T(8,128)(2,1)S(1)}, u32[]{:S(2)}, u32[]{:S(2)}) collective-permute-start(bf16[4,128,128]{2,1,0:T(8,128)(2,1)S(1)} %shard_map.128.a_ref), channel_id=1, source_target_pairs={{0,24},{4,28},{8,16},{12,20},{16,8},{20,12},{24,0},{28,4},{1,25},{... | collective-permute-start | bytes 393224 | tf_op jit(solution)/shard_map/ppermute | solution.py:327
  28.9 0.0 collective-permute-done.8.other_ref
  28.9 2.3 %collective-permute-done.5.b_ref = bf16[4,128,128]{2,1,0:T(8,128)(2,1)S(1)} collective-permute-done((bf16[4,128,128]{2,1,0:T(8,128)(2,1)S(1)}, bf16[4,128,128]{2,1,0:T(8,128)(2,1)S(1)}, u32[]{:S(2)}, u32[]{:S(2)}) %collective-permute-start.5) | collective-permute-done | bytes 131104 | tf_op jit(solution)/shard_map/ppermute | solution.py:327
  31.2 4.3 %collective-permute-done.6.c_ref = bf16[4,128,128]{2,1,0:T(8,128)(2,1)S(1)} collective-permute-done((bf16[4,128,128]{2,1,0:T(8,128)(2,1)S(1)}, bf16[4,128,128]{2,1,0:T(8,128)(2,1)S(1)}, u32[]{:S(2)}, u32[]{:S(2)}) %collective-permute-start.6) | collective-permute-done | bytes 131104 | tf_op jit(solution)/shard_map/ppermute | solution.py:327
  35.5 1.5 %shard_map.129 = (f32[256,512]{1,0:T(8,128)S(1)}, bf16[256,512]{1,0:T(8,128)(2,1)S(1)}) custom-call(bf16[4,128,128]{2,1,0:T(8,128)(2,1)S(1)} %shard_map.128.a_ref, bf16[4,128,128]{2,1,0:T(8,128)(2,1)S(1)} %collective-permute-done.5.b_ref, bf16[4,128,128]{2,1,0:T(8,128)(2,1)S(1)} %collective-permute-done.6.c_ref, ...), custom_call_target="tpu_custom_call" | custom-call | tf_op jit(solution)/shard_map/pallas_call | solution.py:296
  37.0 0.1 collective-permute-start.9
  37.1 1.1 slice.140
  38.2 2.0 %collective-permute-start.18 = (bf16[160,1408]{1,0:T(8,128)(2,1)S(1)}, bf16[160,1408]{1,0:T(8,128)(2,1)S(1)}, u32[]{:S(2)}, u32[]{:S(2)}) collective-permute-start(bf16[160,1408]{1,0:T(8,128)(2,1)S(1)} %slice.140), channel_id=1, source_target_pairs={{0,8},{4,12},{8,0},{12,4},{16,24},{20,28},{24,16},{28,20},{1,9},{5... | collective-permute-start | bytes 1351688 | tf_op jit(solution)/shard_map/ppermute | solution.py:327
  40.2 0.1 convert_add_fusion
  40.3 1.6 %collective-permute-start.10 = (bf16[128,512]{1,0:T(8,128)(2,1)S(1)}, bf16[128,512]{1,0:T(8,128)(2,1)S(1)}, u32[]{:S(2)}, u32[]{:S(2)}) collective-permute-start(bf16[128,512]{1,0:T(8,128)(2,1)S(1)} %slice.221), channel_id=1, source_target_pairs={{0,2},{1,3},{2,0},{3,1},{4,6},{5,7},{6,4},{7,5},{8,10},{9,11},{10,... | collective-permute-start | bytes 393224 | tf_op jit(solution)/shard_map/ppermute | solution.py:327
  41.9 0.5 collective-permute-start.19
  42.4 9.1 %collective-permute-done.18.refs_1_ = bf16[160,1408]{1,0:T(8,128)(2,1)S(1)} collective-permute-done((bf16[160,1408]{1,0:T(8,128)(2,1)S(1)}, bf16[160,1408]{1,0:T(8,128)(2,1)S(1)}, u32[]{:S(2)}, u32[]{:S(2)}) %collective-permute-start.18) | collective-permute-done | bytes 450592 | tf_op jit(solution)/shard_map/ppermute | solution.py:327
  51.5 0.7 collective-permute-start.28
  52.2 4.7 %collective-permute-start.12 = (bf16[32,512]{1,0:T(8,128)(2,1)S(1)}, bf16[32,512]{1,0:T(8,128)(2,1)S(1)}, u32[]{:S(2)}, u32[]{:S(2)}) collective-permute-start(bf16[32,512]{1,0:T(8,128)(2,1)S(1)} %get-tuple-element.69), channel_id=1, source_target_pairs={{0,16},{4,20},{8,24},{12,28},{16,0},{20,4},{24,8},{28,12},{1,17},{... | collective-permute-start | bytes 98312 | tf_op jit(solution)/shard_map/ppermute | solution.py:327
  56.9 2.5 %collective-permute-start.11 = (bf16[32,512]{1,0:T(8,128)(2,1)S(1)}, bf16[32,512]{1,0:T(8,128)(2,1)S(1)}, u32[]{:S(2)}, u32[]{:S(2)}) collective-permute-start(bf16[32,512]{1,0:T(8,128)(2,1)S(1)} %get-tuple-element.70), channel_id=1, source_target_pairs={{0,24},{4,28},{8,16},{12,20},{16,8},{20,12},{24,0},{28,4},{1,25},{... | collective-permute-start | bytes 98312 | tf_op jit(solution)/shard_map/ppermute | solution.py:327
  59.4 9.2 %collective-permute-done.12 = bf16[32,512]{1,0:T(8,128)(2,1)S(1)} collective-permute-done((bf16[32,512]{1,0:T(8,128)(2,1)S(1)}, bf16[32,512]{1,0:T(8,128)(2,1)S(1)}, u32[]{:S(2)}, u32[]{:S(2)}) %collective-permute-start.12) | collective-permute-done | bytes 32800 | tf_op jit(solution)/shard_map/ppermute | solution.py:327
  68.8 0.2 fusion
  69.0 0.1 fusion.2
  69.1 2.5 %collective-permute-start.16 = (bf16[32,2048]{1,0:T(8,128)(2,1)S(1)}, bf16[32,2048]{1,0:T(8,128)(2,1)S(1)}, u32[]{:S(2)}, u32[]{:S(2)}) collective-permute-start(bf16[32,2048]{1,0:T(8,128)(2,1)S(1)} %fusion.2), channel_id=1, source_target_pairs={{0,6},{1,7},{2,4},{3,5},{4,2},{5,3},{6,0},{7,1},{8,14},{9,15},{10,... | collective-permute-start | bytes 393224 | tf_op jit(solution)/shard_map/ppermute | solution.py:335
  71.6 0.5 collective-permute-start.15
  72.1 0.5 collective-permute-start.14
  72.6 0.7 collective-permute-start.20
  73.3 1.7 %collective-permute-done.16 = bf16[32,2048]{1,0:T(8,128)(2,1)S(1)} collective-permute-done((bf16[32,2048]{1,0:T(8,128)(2,1)S(1)}, bf16[32,2048]{1,0:T(8,128)(2,1)S(1)}, u32[]{:S(2)}, u32[]{:S(2)}) %collective-permute-start.16) | collective-permute-done | bytes 131104 | tf_op jit(solution)/shard_map/ppermute | solution.py:335
  75.0 0.7 collective-permute-start.30
  75.7 0.9 collective-permute-done.15
  76.5 0.5 collective-permute-done.14
  77.1 0.1 collective-permute-start.17
  77.2 0.7 collective-permute-start.22
  77.9 1.3 collective-permute-start.29
  79.2 1.3 collective-permute-start.21
  80.5 1.3 collective-permute-start.31
  81.8 1.3 collective-permute-start.23
  83.1 6.0 %shard_map.130.hidden_ref = bf16[256,1408]{1,0:T(8,128)(2,1)S(1)} custom-call(bf16[128,2048]{1,0:T(8,128)(2,1)S(1)} %pad_maximum_fusion.here_ref, bf16[128,2048]{1,0:T(8,128)(2,1)S(1)} %collective-permute-done.17.there_ref, bf16[2048,1408]{1,0:T(8,128)(2,1)} %gate_ref.1, bf16[2048,1408]{1,0:T(8,128)(2,1)} %up_ref.1), custom_call_target="tpu_custom_call" | custom-call | tf_op jit(solution)/shard_map/pallas_call | solution.py:296
  89.2 21.8 %collective-permute-done.31.refs_3_ = bf16[96,1408]{1,0:T(8,128)(2,1)S(1)} collective-permute-done((bf16[96,1408]{1,0:T(8,128)(2,1)S(1)}, bf16[96,1408]{1,0:T(8,128)(2,1)S(1)}, u32[]{:S(2)}, u32[]{:S(2)}) %collective-permute-start.31) | collective-permute-done | bytes 270368 | tf_op jit(solution)/shard_map/ppermute | solution.py:351
  110.9 0.4 shard_map.132
  111.4 0.1 collective-permute-start.32
  111.5 4.8 %collective-permute-done.23.refs_6_ = bf16[96,1408]{1,0:T(8,128)(2,1)S(1)} collective-permute-done((bf16[96,1408]{1,0:T(8,128)(2,1)S(1)}, bf16[96,1408]{1,0:T(8,128)(2,1)S(1)}, u32[]{:S(2)}, u32[]{:S(2)}) %collective-permute-start.23) | collective-permute-done | bytes 270368 | tf_op jit(solution)/shard_map/ppermute | solution.py:350
  116.2 0.8 shard_map.131
  117.1 0.1 collective-permute-start.24
  117.2 1.4 %collective-permute-done.24 = bf16[128,768]{1,0:T(8,128)(2,1)S(1)} collective-permute-done((bf16[128,768]{1,0:T(8,128)(2,1)S(1)}, bf16[128,768]{1,0:T(8,128)(2,1)S(1)}, u32[]{:S(2)}, u32[]{:S(2)}) %collective-permute-start.24) | collective-permute-done | bytes 196640 | tf_op jit(solution)/shard_map/ppermute | solution.py:327
  118.6 0.1 fusion.18
  118.7 1.6 %collective-permute-start.25 = (bf16[32,768]{1,0:T(8,128)(2,1)S(1)}, bf16[32,768]{1,0:T(8,128)(2,1)S(1)}, u32[]{:S(2)}, u32[]{:S(2)}) collective-permute-start(bf16[32,768]{1,0:T(8,128)(2,1)S(1)} %get-tuple-element.67), channel_id=1, source_target_pairs={{0,2},{1,3},{2,0},{3,1},{4,6},{5,7},{6,4},{7,5},{8,10},{9,11},{10,... | collective-permute-start | bytes 147464 | tf_op jit(solution)/shard_map/ppermute | solution.py:327
  120.2 1.5 %collective-permute-start.26 = (bf16[32,768]{1,0:T(8,128)(2,1)S(1)}, bf16[32,768]{1,0:T(8,128)(2,1)S(1)}, u32[]{:S(2)}, u32[]{:S(2)}) collective-permute-start(bf16[32,768]{1,0:T(8,128)(2,1)S(1)} %get-tuple-element.66), channel_id=1, source_target_pairs={{0,4},{4,0},{8,12},{12,8},{16,20},{20,16},{24,28},{28,24},{1,5},{5... | collective-permute-start | bytes 147464 | tf_op jit(solution)/shard_map/ppermute | solution.py:327
  121.7 0.5 collective-permute-start.27
  122.2 1.5 %collective-permute-start.33 = (bf16[32,256]{1,0:T(8,128)(2,1)S(1)}, bf16[32,256]{1,0:T(8,128)(2,1)S(1)}, u32[]{:S(2)}, u32[]{:S(2)}) collective-permute-start(bf16[32,256]{1,0:T(8,128)(2,1)S(1)} %get-tuple-element.75), channel_id=1, source_target_pairs={{0,2},{1,3},{2,0},{3,1},{4,6},{5,7},{6,4},{7,5},{8,10},{9,11},{10,... | collective-permute-start | bytes 49160 | tf_op jit(solution)/shard_map/ppermute | solution.py:327
  123.7 1.5 %collective-permute-start.34 = (bf16[32,256]{1,0:T(8,128)(2,1)S(1)}, bf16[32,256]{1,0:T(8,128)(2,1)S(1)}, u32[]{:S(2)}, u32[]{:S(2)}) collective-permute-start(bf16[32,256]{1,0:T(8,128)(2,1)S(1)} %get-tuple-element.74), channel_id=1, source_target_pairs={{0,4},{4,0},{8,12},{12,8},{16,20},{20,16},{24,28},{28,24},{1,5},{5... | collective-permute-start | bytes 49160 | tf_op jit(solution)/shard_map/ppermute | solution.py:327
  125.2 0.7 collective-permute-done.33
  126.0 2.4 %collective-permute-start.35 = (bf16[32,256]{1,0:T(8,128)(2,1)S(1)}, bf16[32,256]{1,0:T(8,128)(2,1)S(1)}, u32[]{:S(2)}, u32[]{:S(2)}) collective-permute-start(bf16[32,256]{1,0:T(8,128)(2,1)S(1)} %get-tuple-element.73), channel_id=1, source_target_pairs={{0,6},{1,7},{2,4},{3,5},{4,2},{5,3},{6,0},{7,1},{8,14},{9,15},{10,... | collective-permute-start | bytes 49160 | tf_op jit(solution)/shard_map/ppermute | solution.py:335
  128.4 2.2 %collective-permute-done.35 = bf16[32,256]{1,0:T(8,128)(2,1)S(1)} collective-permute-done((bf16[32,256]{1,0:T(8,128)(2,1)S(1)}, bf16[32,256]{1,0:T(8,128)(2,1)S(1)}, u32[]{:S(2)}, u32[]{:S(2)}) %collective-permute-start.35) | collective-permute-done | bytes 16416 | tf_op jit(solution)/shard_map/ppermute | solution.py:335
  130.7 0.7 fusion.3
  (58 shorter events, 0.5 us)
Async XLA Ops:
  0.0 41.9 %copy-start = (bf16[256,1408]{1,0:T(8,128)(2,1)S(1)}, bf16[256,1408]{1,0:T(8,128)(2,1)}, u32[]{:S(2)}) copy-start(bf16[256,1408]{1,0:T(8,128)(2,1)} %refs_0_.3) | copy-start | bytes 2162692
  0.0 68.8 %copy-start.1 = (bf16[32,2048]{1,0:T(8,128)(2,1)S(1)}, bf16[32,2048]{1,0:T(8,128)(2,1)}, u32[]{:S(2)}) copy-start(bf16[32,2048]{1,0:T(8,128)(2,1)} %param.13) | copy-start | bytes 393220
  0.0 68.9 %copy-start.2 = (f32[2048]{0:T(1024)S(1)}, f32[2048]{0:T(1024)}, u32[]{:S(2)}) copy-start(f32[2048]{0:T(1024)} %param.22) | copy-start | bytes 24580
  1.4 5.9 %collective-permute-start = (bf16[128,384]{1,0:T(8,128)(2,1)S(1)}, bf16[128,384]{1,0:T(8,128)(2,1)S(1)}, u32[]{:S(2)}, u32[]{:S(2)}) collective-permute-start(bf16[128,384]{1,0:T(8,128)(2,1)S(1)} %get-tuple-element.47), channel_id=1, source_target_pairs={{0,8},{4,12},{8,0},{12,4},{16,24},{20,28},{24,16},{28,20},{1,9},{5... | collective-permute-start | bytes 294920 | tf_op jit(solution)/shard_map/ppermute | solution.py:327
  4.5 10.4 %collective-permute-start.1 = (bf16[128,384]{1,0:T(8,128)(2,1)S(1)}, bf16[128,384]{1,0:T(8,128)(2,1)S(1)}, u32[]{:S(2)}, u32[]{:S(2)}) collective-permute-start(bf16[128,384]{1,0:T(8,128)(2,1)S(1)} %get-tuple-element.46), channel_id=1, source_target_pairs={{0,16},{4,20},{8,24},{12,28},{16,0},{20,4},{24,8},{28,12},{1,17},{... | collective-permute-start | bytes 294920 | tf_op jit(solution)/shard_map/ppermute | solution.py:327
  7.1 6.6 %collective-permute-start.2 = (bf16[128,384]{1,0:T(8,128)(2,1)S(1)}, bf16[128,384]{1,0:T(8,128)(2,1)S(1)}, u32[]{:S(2)}, u32[]{:S(2)}) collective-permute-start(bf16[128,384]{1,0:T(8,128)(2,1)S(1)} %get-tuple-element.45), channel_id=1, source_target_pairs={{0,24},{4,28},{8,16},{12,20},{16,8},{20,12},{24,0},{28,4},{1,25},{... | collective-permute-start | bytes 294920 | tf_op jit(solution)/shard_map/ppermute | solution.py:327
  7.3 9.7 %collective-permute-start.3 = (bf16[256,256]{1,0:T(8,128)(2,1)S(1)}, bf16[256,256]{1,0:T(8,128)(2,1)S(1)}, u32[]{:S(2)}, u32[]{:S(2)}) collective-permute-start(bf16[256,256]{1,0:T(8,128)(2,1)S(1)} %pad_maximum_fusion.1), channel_id=1, source_target_pairs={{0,4},{4,0},{8,12},{12,8},{16,20},{20,16},{24,28},{28,24},{1,5},{5... | collective-permute-start | bytes 393224 | tf_op jit(solution)/shard_map/ppermute | solution.py:327
  14.9 6.4 %collective-permute-start.4 = (bf16[256,256]{1,0:T(8,128)(2,1)S(1)}, bf16[256,256]{1,0:T(8,128)(2,1)S(1)}, u32[]{:S(2)}, u32[]{:S(2)}) collective-permute-start(bf16[256,256]{1,0:T(8,128)(2,1)S(1)} %pad_maximum_fusion.2), channel_id=1, source_target_pairs={{0,4},{4,0},{8,12},{12,8},{16,20},{20,16},{24,28},{28,24},{1,5},{5... | collective-permute-start | bytes 393224 | tf_op jit(solution)/shard_map/ppermute | solution.py:327
  16.5 12.4 %collective-permute-start.8 = (bf16[256,512]{1,0:T(8,128)(2,1)}, bf16[256,512]{1,0:T(8,128)(2,1)S(1)}, u32[]{:S(2)}, u32[]{:S(2)}) collective-permute-start(bf16[256,512]{1,0:T(8,128)(2,1)} %source.1), channel_id=1, source_target_pairs={{0,4},{4,0},{8,12},{12,8},{16,20},{20,16},{24,28},{28,24},{1,5},{5... | collective-permute-start | bytes 786440 | tf_op jit(solution)/shard_map/ppermute | solution.py:327
  24.5 6.7 %collective-permute-start.5 = (bf16[4,128,128]{2,1,0:T(8,128)(2,1)S(1)}, bf16[4,128,128]{2,1,0:T(8,128)(2,1)S(1)}, u32[]{:S(2)}, u32[]{:S(2)}) collective-permute-start(bf16[4,128,128]{2,1,0:T(8,128)(2,1)S(1)} %shard_map.128.a_ref), channel_id=1, source_target_pairs={{0,8},{4,12},{8,0},{12,4},{16,24},{20,28},{24,16},{28,20},{1,9},{5... | collective-permute-start | bytes 393224 | tf_op jit(solution)/shard_map/ppermute | solution.py:327
  26.3 9.2 %collective-permute-start.6 = (bf16[4,128,128]{2,1,0:T(8,128)(2,1)S(1)}, bf16[4,128,128]{2,1,0:T(8,128)(2,1)S(1)}, u32[]{:S(2)}, u32[]{:S(2)}) collective-permute-start(bf16[4,128,128]{2,1,0:T(8,128)(2,1)S(1)} %shard_map.128.a_ref), channel_id=1, source_target_pairs={{0,16},{4,20},{8,24},{12,28},{16,0},{20,4},{24,8},{28,12},{1,17},{... | collective-permute-start | bytes 393224 | tf_op jit(solution)/shard_map/ppermute | solution.py:327
  27.4 8.1 %collective-permute-start.7 = (bf16[4,128,128]{2,1,0:T(8,128)(2,1)S(1)}, bf16[4,128,128]{2,1,0:T(8,128)(2,1)S(1)}, u32[]{:S(2)}, u32[]{:S(2)}) collective-permute-start(bf16[4,128,128]{2,1,0:T(8,128)(2,1)S(1)} %shard_map.128.a_ref), channel_id=1, source_target_pairs={{0,24},{4,28},{8,16},{12,20},{16,8},{20,12},{24,0},{28,4},{1,25},{... | collective-permute-start | bytes 393224 | tf_op jit(solution)/shard_map/ppermute | solution.py:327
  37.0 3.2 %collective-permute-start.9 = (bf16[256,512]{1,0:T(8,128)(2,1)S(1)}, bf16[256,512]{1,0:T(8,128)(2,1)S(1)}, u32[]{:S(2)}, u32[]{:S(2)}) collective-permute-start(bf16[256,512]{1,0:T(8,128)(2,1)S(1)} %get-tuple-element.24), channel_id=1, source_target_pairs={{0,1},{1,0},{2,3},{3,2},{4,5},{5,4},{6,7},{7,6},{8,9},{9,8},{10,11... | collective-permute-start | bytes 786440 | tf_op jit(solution)/shard_map/ppermute | solution.py:327
  38.2 13.3 %collective-permute-start.18 = (bf16[160,1408]{1,0:T(8,128)(2,1)S(1)}, bf16[160,1408]{1,0:T(8,128)(2,1)S(1)}, u32[]{:S(2)}, u32[]{:S(2)}) collective-permute-start(bf16[160,1408]{1,0:T(8,128)(2,1)S(1)} %slice.140), channel_id=1, source_target_pairs={{0,8},{4,12},{8,0},{12,4},{16,24},{20,28},{24,16},{28,20},{1,9},{5... | collective-permute-start | bytes 1351688 | tf_op jit(solution)/shard_map/ppermute | solution.py:327
  40.3 11.8 %collective-permute-start.10 = (bf16[128,512]{1,0:T(8,128)(2,1)S(1)}, bf16[128,512]{1,0:T(8,128)(2,1)S(1)}, u32[]{:S(2)}, u32[]{:S(2)}) collective-permute-start(bf16[128,512]{1,0:T(8,128)(2,1)S(1)} %slice.221), channel_id=1, source_target_pairs={{0,2},{1,3},{2,0},{3,1},{4,6},{5,7},{6,4},{7,5},{8,10},{9,11},{10,... | collective-permute-start | bytes 393224 | tf_op jit(solution)/shard_map/ppermute | solution.py:327
  41.9 30.7 %collective-permute-start.19 = (bf16[96,1408]{1,0:T(8,128)(2,1)S(1)}, bf16[96,1408]{1,0:T(8,128)(2,1)S(1)}, u32[]{:S(2)}, u32[]{:S(2)}) collective-permute-start(bf16[96,1408]{1,0:T(8,128)(2,1)S(1)} %slice.141), channel_id=1, source_target_pairs={{0,8},{4,12},{8,0},{12,4},{16,24},{20,28},{24,16},{28,20},{1,9},{5... | collective-permute-start | bytes 811016 | tf_op jit(solution)/shard_map/ppermute | solution.py:327
  51.5 26.4 %collective-permute-start.28 = (bf16[160,1408]{1,0:T(8,128)(2,1)S(1)}, bf16[160,1408]{1,0:T(8,128)(2,1)S(1)}, u32[]{:S(2)}, u32[]{:S(2)}) collective-permute-start(bf16[160,1408]{1,0:T(8,128)(2,1)S(1)} %collective-permute-done.18.refs_1_), channel_id=1, source_target_pairs={{8,16},{12,20},{16,8},{20,12},{9,17},{13,21},{17,9},{21,13},{10,18... | collective-permute-start | bytes 1351688 | tf_op jit(solution)/shard_map/ppermute | solution.py:349
  52.2 16.4 %collective-permute-start.12 = (bf16[32,512]{1,0:T(8,128)(2,1)S(1)}, bf16[32,512]{1,0:T(8,128)(2,1)S(1)}, u32[]{:S(2)}, u32[]{:S(2)}) collective-permute-start(bf16[32,512]{1,0:T(8,128)(2,1)S(1)} %get-tuple-element.69), channel_id=1, source_target_pairs={{0,16},{4,20},{8,24},{12,28},{16,0},{20,4},{24,8},{28,12},{1,17},{... | collective-permute-start | bytes 98312 | tf_op jit(solution)/shard_map/ppermute | solution.py:327
  56.9 11.7 %collective-permute-start.11 = (bf16[32,512]{1,0:T(8,128)(2,1)S(1)}, bf16[32,512]{1,0:T(8,128)(2,1)S(1)}, u32[]{:S(2)}, u32[]{:S(2)}) collective-permute-start(bf16[32,512]{1,0:T(8,128)(2,1)S(1)} %get-tuple-element.70), channel_id=1, source_target_pairs={{0,24},{4,28},{8,16},{12,20},{16,8},{20,12},{24,0},{28,4},{1,25},{... | collective-permute-start | bytes 98312 | tf_op jit(solution)/shard_map/ppermute | solution.py:327
  59.4 9.3 %collective-permute-start.13 = (bf16[32,512]{1,0:T(8,128)(2,1)S(1)}, bf16[32,512]{1,0:T(8,128)(2,1)S(1)}, u32[]{:S(2)}, u32[]{:S(2)}) collective-permute-start(bf16[32,512]{1,0:T(8,128)(2,1)S(1)} %get-tuple-element.68), channel_id=1, source_target_pairs={{0,8},{4,12},{8,0},{12,4},{16,24},{20,28},{24,16},{28,20},{1,9},{5... | collective-permute-start | bytes 98312 | tf_op jit(solution)/shard_map/ppermute | solution.py:327
  69.1 5.9 %collective-permute-start.16 = (bf16[32,2048]{1,0:T(8,128)(2,1)S(1)}, bf16[32,2048]{1,0:T(8,128)(2,1)S(1)}, u32[]{:S(2)}, u32[]{:S(2)}) collective-permute-start(bf16[32,2048]{1,0:T(8,128)(2,1)S(1)} %fusion.2), channel_id=1, source_target_pairs={{0,6},{1,7},{2,4},{3,5},{4,2},{5,3},{6,0},{7,1},{8,14},{9,15},{10,... | collective-permute-start | bytes 393224 | tf_op jit(solution)/shard_map/ppermute | solution.py:335
  71.6 5.0 %collective-permute-start.15 = (bf16[32,2048]{1,0:T(8,128)(2,1)S(1)}, bf16[32,2048]{1,0:T(8,128)(2,1)S(1)}, u32[]{:S(2)}, u32[]{:S(2)}) collective-permute-start(bf16[32,2048]{1,0:T(8,128)(2,1)S(1)} %fusion.2), channel_id=1, source_target_pairs={{0,4},{4,0},{8,12},{12,8},{16,20},{20,16},{24,28},{28,24},{1,5},{5... | collective-permute-start | bytes 393224 | tf_op jit(solution)/shard_map/ppermute | solution.py:327
  72.1 5.0 %collective-permute-start.14 = (bf16[32,2048]{1,0:T(8,128)(2,1)S(1)}, bf16[32,2048]{1,0:T(8,128)(2,1)S(1)}, u32[]{:S(2)}, u32[]{:S(2)}) collective-permute-start(bf16[32,2048]{1,0:T(8,128)(2,1)S(1)} %fusion.2), channel_id=1, source_target_pairs={{0,2},{1,3},{2,0},{3,1},{4,6},{5,7},{6,4},{7,5},{8,10},{9,11},{10,... | collective-permute-start | bytes 393224 | tf_op jit(solution)/shard_map/ppermute | solution.py:327
  72.6 6.6 %collective-permute-start.20 = (bf16[160,1408]{1,0:T(8,128)(2,1)S(1)}, bf16[160,1408]{1,0:T(8,128)(2,1)S(1)}, u32[]{:S(2)}, u32[]{:S(2)}) collective-permute-start(bf16[160,1408]{1,0:T(8,128)(2,1)S(1)} %slice.140), channel_id=1, source_target_pairs={{8,16},{12,20},{16,8},{20,12},{9,17},{13,21},{17,9},{21,13},{10,18... | collective-permute-start | bytes 1351688 | tf_op jit(solution)/shard_map/ppermute | solution.py:348
  75.0 5.5 %collective-permute-start.30 = (bf16[96,1408]{1,0:T(8,128)(2,1)S(1)}, bf16[96,1408]{1,0:T(8,128)(2,1)S(1)}, u32[]{:S(2)}, u32[]{:S(2)}) collective-permute-start(bf16[96,1408]{1,0:T(8,128)(2,1)S(1)} %collective-permute-done.19.refs_2_), channel_id=1, source_target_pairs={{8,16},{12,20},{16,8},{20,12},{9,17},{13,21},{17,9},{21,13},{10,18... | collective-permute-start | bytes 811016 | tf_op jit(solution)/shard_map/ppermute | solution.py:349
  77.1 6.0 %collective-permute-start.17 = (bf16[128,2048]{1,0:T(8,128)(2,1)S(1)}, bf16[128,2048]{1,0:T(8,128)(2,1)S(1)}, u32[]{:S(2)}, u32[]{:S(2)}) collective-permute-start(bf16[128,2048]{1,0:T(8,128)(2,1)S(1)} %pad_maximum_fusion.here_ref), channel_id=1, source_target_pairs={{0,1},{1,0},{2,3},{3,2},{4,5},{5,4},{6,7},{7,6},{8,9},{9,8},{10,11... | collective-permute-start | bytes 1572872 | tf_op jit(solution)/shard_map/ppermute | solution.py:327
  77.2 4.6 %collective-permute-start.22 = (bf16[96,1408]{1,0:T(8,128)(2,1)S(1)}, bf16[96,1408]{1,0:T(8,128)(2,1)S(1)}, u32[]{:S(2)}, u32[]{:S(2)}) collective-permute-start(bf16[96,1408]{1,0:T(8,128)(2,1)S(1)} %slice.141), channel_id=1, source_target_pairs={{8,16},{12,20},{16,8},{20,12},{9,17},{13,21},{17,9},{21,13},{10,18... | collective-permute-start | bytes 811016 | tf_op jit(solution)/shard_map/ppermute | solution.py:348
  77.9 33.1 %collective-permute-start.29 = (bf16[160,1408]{1,0:T(8,128)(2,1)S(1)}, bf16[160,1408]{1,0:T(8,128)(2,1)S(1)}, u32[]{:S(2)}, u32[]{:S(2)}) collective-permute-start(bf16[160,1408]{1,0:T(8,128)(2,1)S(1)} %collective-permute-done.28.refs_0_), channel_id=1, source_target_pairs={{8,0},{12,4},{16,24},{20,28},{9,1},{13,5},{17,25},{21,29},{10,2},{... | collective-permute-start | bytes 1351688 | tf_op jit(solution)/shard_map/ppermute | solution.py:351
  79.2 37.1 %collective-permute-start.21 = (bf16[160,1408]{1,0:T(8,128)(2,1)S(1)}, bf16[160,1408]{1,0:T(8,128)(2,1)S(1)}, u32[]{:S(2)}, u32[]{:S(2)}) collective-permute-start(bf16[160,1408]{1,0:T(8,128)(2,1)S(1)} %collective-permute-done.20.refs_3_), channel_id=1, source_target_pairs={{8,0},{12,4},{16,24},{20,28},{9,1},{13,5},{17,25},{21,29},{10,2},{... | collective-permute-start | bytes 1351688 | tf_op jit(solution)/shard_map/ppermute | solution.py:350
  80.5 30.4 %collective-permute-start.31 = (bf16[96,1408]{1,0:T(8,128)(2,1)S(1)}, bf16[96,1408]{1,0:T(8,128)(2,1)S(1)}, u32[]{:S(2)}, u32[]{:S(2)}) collective-permute-start(bf16[96,1408]{1,0:T(8,128)(2,1)S(1)} %collective-permute-done.30.refs_2_), channel_id=1, source_target_pairs={{8,0},{12,4},{16,24},{20,28},{9,1},{13,5},{17,25},{21,29},{10,2},{... | collective-permute-start | bytes 811016 | tf_op jit(solution)/shard_map/ppermute | solution.py:351
  81.8 34.4 %collective-permute-start.23 = (bf16[96,1408]{1,0:T(8,128)(2,1)S(1)}, bf16[96,1408]{1,0:T(8,128)(2,1)S(1)}, u32[]{:S(2)}, u32[]{:S(2)}) collective-permute-start(bf16[96,1408]{1,0:T(8,128)(2,1)S(1)} %collective-permute-done.22.refs_5_), channel_id=1, source_target_pairs={{8,0},{12,4},{16,24},{20,28},{9,1},{13,5},{17,25},{21,29},{10,2},{... | collective-permute-start | bytes 811016 | tf_op jit(solution)/shard_map/ppermute | solution.py:350
  111.4 5.8 %collective-permute-start.32 = (bf16[128,256]{1,0:T(8,128)(2,1)S(1)}, bf16[128,256]{1,0:T(8,128)(2,1)S(1)}, u32[]{:S(2)}, u32[]{:S(2)}) collective-permute-start(bf16[128,256]{1,0:T(8,128)(2,1)S(1)} %get-tuple-element.28), channel_id=1, source_target_pairs={{0,1},{1,0},{2,3},{3,2},{4,5},{5,4},{6,7},{7,6},{8,9},{9,8},{10,11... | collective-permute-start | bytes 196616 | tf_op jit(solution)/shard_map/ppermute | solution.py:327
  117.1 1.5 %collective-permute-start.24 = (bf16[128,768]{1,0:T(8,128)(2,1)S(1)}, bf16[128,768]{1,0:T(8,128)(2,1)S(1)}, u32[]{:S(2)}, u32[]{:S(2)}) collective-permute-start(bf16[128,768]{1,0:T(8,128)(2,1)S(1)} %get-tuple-element.26), channel_id=1, source_target_pairs={{0,1},{1,0},{2,3},{3,2},{4,5},{5,4},{6,7},{7,6},{8,9},{9,8},{10,11... | collective-permute-start | bytes 589832 | tf_op jit(solution)/shard_map/ppermute | solution.py:327
  118.7 11.9 %collective-permute-start.25 = (bf16[32,768]{1,0:T(8,128)(2,1)S(1)}, bf16[32,768]{1,0:T(8,128)(2,1)S(1)}, u32[]{:S(2)}, u32[]{:S(2)}) collective-permute-start(bf16[32,768]{1,0:T(8,128)(2,1)S(1)} %get-tuple-element.67), channel_id=1, source_target_pairs={{0,2},{1,3},{2,0},{3,1},{4,6},{5,7},{6,4},{7,5},{8,10},{9,11},{10,... | collective-permute-start | bytes 147464 | tf_op jit(solution)/shard_map/ppermute | solution.py:327
  120.2 10.4 %collective-permute-start.26 = (bf16[32,768]{1,0:T(8,128)(2,1)S(1)}, bf16[32,768]{1,0:T(8,128)(2,1)S(1)}, u32[]{:S(2)}, u32[]{:S(2)}) collective-permute-start(bf16[32,768]{1,0:T(8,128)(2,1)S(1)} %get-tuple-element.66), channel_id=1, source_target_pairs={{0,4},{4,0},{8,12},{12,8},{16,20},{20,16},{24,28},{28,24},{1,5},{5... | collective-permute-start | bytes 147464 | tf_op jit(solution)/shard_map/ppermute | solution.py:327
  121.7 8.9 %collective-permute-start.27 = (bf16[32,768]{1,0:T(8,128)(2,1)S(1)}, bf16[32,768]{1,0:T(8,128)(2,1)S(1)}, u32[]{:S(2)}, u32[]{:S(2)}) collective-permute-start(bf16[32,768]{1,0:T(8,128)(2,1)S(1)} %get-tuple-element.65), channel_id=1, source_target_pairs={{0,6},{1,7},{2,4},{3,5},{4,2},{5,3},{6,0},{7,1},{8,14},{9,15},{10,... | collective-permute-start | bytes 147464 | tf_op jit(solution)/shard_map/ppermute | solution.py:335
  122.2 3.7 %collective-permute-start.33 = (bf16[32,256]{1,0:T(8,128)(2,1)S(1)}, bf16[32,256]{1,0:T(8,128)(2,1)S(1)}, u32[]{:S(2)}, u32[]{:S(2)}) collective-permute-start(bf16[32,256]{1,0:T(8,128)(2,1)S(1)} %get-tuple-element.75), channel_id=1, source_target_pairs={{0,2},{1,3},{2,0},{3,1},{4,6},{5,7},{6,4},{7,5},{8,10},{9,11},{10,... | collective-permute-start | bytes 49160 | tf_op jit(solution)/shard_map/ppermute | solution.py:327
  123.7 4.7 %collective-permute-start.34 = (bf16[32,256]{1,0:T(8,128)(2,1)S(1)}, bf16[32,256]{1,0:T(8,128)(2,1)S(1)}, u32[]{:S(2)}, u32[]{:S(2)}) collective-permute-start(bf16[32,256]{1,0:T(8,128)(2,1)S(1)} %get-tuple-element.74), channel_id=1, source_target_pairs={{0,4},{4,0},{8,12},{12,8},{16,20},{20,16},{24,28},{28,24},{1,5},{5... | collective-permute-start | bytes 49160 | tf_op jit(solution)/shard_map/ppermute | solution.py:327
  126.0 4.6 %collective-permute-start.35 = (bf16[32,256]{1,0:T(8,128)(2,1)S(1)}, bf16[32,256]{1,0:T(8,128)(2,1)S(1)}, u32[]{:S(2)}, u32[]{:S(2)}) collective-permute-start(bf16[32,256]{1,0:T(8,128)(2,1)S(1)} %get-tuple-element.73), channel_id=1, source_target_pairs={{0,6},{1,7},{2,4},{3,5},{4,2},{5,3},{6,0},{7,1},{8,14},{9,15},{10,... | collective-permute-start | bytes 49160 | tf_op jit(solution)/shard_map/ppermute | solution.py:335

commit v5 on v4

--- a/solution.py
+++ b/solution.py
@@ -166,8 +166,10 @@
     for index, ref in enumerate(queries):
         k_ref[index * rows : (index + 1) * rows] = ref[:, lanes : 2 * lanes]
         v_ref[index * rows : (index + 1) * rows] = ref[:, 2 * lanes :]
-    for index, ref in enumerate((ab_ref, cd_ref)):
-        at = slice((4 + 2 * index) * rows, (6 + 2 * index) * rows)
+    start = len(queries) * rows
+    for ref in (ab_ref, cd_ref):
+        at = slice(start, start + ref.shape[0])
+        start += ref.shape[0]
         k_ref[at] = ref[:, :lanes]
         v_ref[at] = ref[:, lanes:]
     lane = lax.broadcasted_iota(jnp.int32, (rows, lanes), 1)
@@ -416,8 +418,10 @@
         ],
     )
     first, second, third = three(dealt[1], dealt[2], dealt[3])
-    early = swap(jnp.concatenate([dealt[0][:, head_lanes:], first[:, head_lanes:]], 0), "sp", side)
-    late = swap(jnp.concatenate([second[:, head_lanes:], third[:, head_lanes:]], 0), "sp", side)
+    early = swap(dealt[0][:, head_lanes:], "sp", side)
+    late = swap(
+        jnp.concatenate([block[:, head_lanes:] for block in (first, second, third)], 0), "sp", side
+    )
     attended = kernel(
         attention_body,
         jax.ShapeDtypeStruct((planes, tokens, value_size), bf16),

time: 132 us -> 138 us (1.045)
  waiting for transfers between devices: 69.1 us -> 76.9 us
    ppermute x25, waiting for transfers between devices: 38.6 us -> 47.2 us  [swap(): return lax.ppermute(array, axis, [(i, i ^ distance) for i in range(count)])]
  transfers between devices with their start and end apart: 36 -> 36, of which waited for: 16 -> 15; matrix products, arithmetic and copies ran while one was open for 1% -> 1% of each run, Pallas kernels for 8% -> 8%
where the time goes in v5:
time: 138 us
  waiting for transfers between devices  76.9 us (56%)
  starting transfers between devices  44.9 us (33%)
  Pallas kernels  13.3 us (10%)
    ppermute x25, waiting for transfers between devices, swap(): return lax.ppermute(array, axis, [(i, i ^ distance) for i in range(count)])  47.2 us
    ppermute x25, starting transfers between devices, swap(): return lax.ppermute(array, axis, [(i, i ^ distance) for i in range(count)])  31.6 us
    ppermute x2, waiting for transfers between devices, along_line(): outer_two = lax.ppermute(middle_two, 'sp', outward_pairs)  21 us
    pallas_call x6, Pallas kernels, kernel(): call(*near, *(pltpu.with_memory_space_constraint(array, pltpu.HBM) for ar...  13.3 us
    ppermute x3, starting transfers between devices, swap_both(): return lax.ppermute(array, ('sp', 'tp'), pairs)  5.43 us
    ppermute x2, waiting for transfers between devices, along_line(): outer_one = lax.ppermute(middle_one, 'sp', outward_pairs)  4.79 us
    ppermute x3, waiting for transfers between devices, swap_both(): return lax.ppermute(array, ('sp', 'tp'), pairs)  3.9 us
  transfers between devices with their start and end apart: 36, of which 15 were waited for; matrix products, arithmetic and copies ran while one was open for 1% of the time, Pallas kernels for 8%

profile of v5, /device:TPU:0, one launch (start us, length us, event | category | flops | bytes accessed | tf_op | source)
XLA Modules:
  0.0 138.1 jit_solution(1703149798486882749)
XLA Ops:
  0.0 1.3 shard_map.127
  1.4 5.1 %collective-permute-start.2 = (bf16[128,384]{1,0:T(8,128)(2,1)S(1)}, bf16[128,384]{1,0:T(8,128)(2,1)S(1)}, u32[]{:S(2)}, u32[]{:S(2)}) collective-permute-start(bf16[128,384]{1,0:T(8,128)(2,1)S(1)} %get-tuple-element.45), channel_id=1, source_target_pairs={{0,24},{4,28},{8,16},{12,20},{16,8},{20,12},{24,0},{28,4},{1,25},{... | collective-permute-start | bytes 294920 | tf_op jit(solution)/shard_map/ppermute | solution.py:329
  6.5 0.0 collective-permute-start.1
  6.5 0.6 collective-permute-start
  7.2 3.1 %collective-permute-done.2.d_ref = bf16[128,384]{1,0:T(8,128)(2,1)S(1)} collective-permute-done((bf16[128,384]{1,0:T(8,128)(2,1)S(1)}, bf16[128,384]{1,0:T(8,128)(2,1)S(1)}, u32[]{:S(2)}, u32[]{:S(2)}) %collective-permute-start.2) | collective-permute-done | bytes 98336 | tf_op jit(solution)/shard_map/ppermute | solution.py:329
  10.2 4.6 %collective-permute-done.1.c_ref = bf16[128,384]{1,0:T(8,128)(2,1)S(1)} collective-permute-done((bf16[128,384]{1,0:T(8,128)(2,1)S(1)}, bf16[128,384]{1,0:T(8,128)(2,1)S(1)}, u32[]{:S(2)}, u32[]{:S(2)}) %collective-permute-start.1) | collective-permute-done | bytes 98336 | tf_op jit(solution)/shard_map/ppermute | solution.py:329
  14.8 0.0 collective-permute-done.b_ref
  14.8 1.6 %collective-permute-start.4 = (bf16[384,256]{1,0:T(8,128)(2,1)S(1)}, bf16[384,256]{1,0:T(8,128)(2,1)S(1)}, u32[]{:S(2)}, u32[]{:S(2)}) collective-permute-start(bf16[384,256]{1,0:T(8,128)(2,1)S(1)} %pad_maximum_fusion.1), channel_id=1, source_target_pairs={{0,4},{4,0},{8,12},{12,8},{16,20},{20,16},{24,28},{28,24},{1,5},{5... | collective-permute-start | bytes 589832 | tf_op jit(solution)/shard_map/ppermute | solution.py:329
  16.4 0.5 collective-permute-start.8
  16.9 1.5 %collective-permute-start.3 = (bf16[128,256]{1,0:T(8,128)(2,1)S(1)}, bf16[128,256]{1,0:T(8,128)(2,1)S(1)}, u32[]{:S(2)}, u32[]{:S(2)}) collective-permute-start(bf16[128,256]{1,0:T(8,128)(2,1)S(1)} %slice.156), channel_id=1, source_target_pairs={{0,4},{4,0},{8,12},{12,8},{16,20},{20,16},{24,28},{28,24},{1,5},{5... | collective-permute-start | bytes 196616 | tf_op jit(solution)/shard_map/ppermute | solution.py:329
  18.4 9.5 %collective-permute-done.3.ab_ref = bf16[128,256]{1,0:T(8,128)(2,1)S(1)} collective-permute-done((bf16[128,256]{1,0:T(8,128)(2,1)S(1)}, bf16[128,256]{1,0:T(8,128)(2,1)S(1)}, u32[]{:S(2)}, u32[]{:S(2)}) %collective-permute-start.3) | collective-permute-done | bytes 65568 | tf_op jit(solution)/shard_map/ppermute | solution.py:329
  27.9 0.0 collective-permute-done.4.cd_ref
  27.9 3.2 %shard_map.128.a_ref = bf16[4,128,128]{2,1,0:T(8,128)(2,1)S(1)} custom-call(f32[2,128]{1,0:T(2,128)S(1)} %get-tuple-element.21.extra_ref, bf16[128,384]{1,0:T(8,128)(2,1)S(1)} %get-tuple-element.48.a_ref, bf16[128,384]{1,0:T(8,128)(2,1)S(1)} %collective-permute-done.b_ref, bf16[128,384]{1,0:T(8,128)(2,1)S(1)} %collective-permute-done.1.c_ref, ...), custom_call_target="tpu_custom_call" | custom-call | tf_op jit(solution)/shard_map/pallas_call | solution.py:298
  31.1 0.4 collective-permute-start.5
  31.5 2.3 %collective-permute-start.6 = (bf16[4,128,128]{2,1,0:T(8,128)(2,1)S(1)}, bf16[4,128,128]{2,1,0:T(8,128)(2,1)S(1)}, u32[]{:S(2)}, u32[]{:S(2)}) collective-permute-start(bf16[4,128,128]{2,1,0:T(8,128)(2,1)S(1)} %shard_map.128.a_ref), channel_id=1, source_target_pairs={{0,16},{4,20},{8,24},{12,28},{16,0},{20,4},{24,8},{28,12},{1,17},{... | collective-permute-start | bytes 393224 | tf_op jit(solution)/shard_map/ppermute | solution.py:329
  33.8 1.7 %collective-permute-start.7 = (bf16[4,128,128]{2,1,0:T(8,128)(2,1)S(1)}, bf16[4,128,128]{2,1,0:T(8,128)(2,1)S(1)}, u32[]{:S(2)}, u32[]{:S(2)}) collective-permute-start(bf16[4,128,128]{2,1,0:T(8,128)(2,1)S(1)} %shard_map.128.a_ref), channel_id=1, source_target_pairs={{0,24},{4,28},{8,16},{12,20},{16,8},{20,12},{24,0},{28,4},{1,25},{... | collective-permute-start | bytes 393224 | tf_op jit(solution)/shard_map/ppermute | solution.py:329
  35.5 1.3 collective-permute-done.5.b_ref
  36.8 6.1 %collective-permute-done.6.c_ref = bf16[4,128,128]{2,1,0:T(8,128)(2,1)S(1)} collective-permute-done((bf16[4,128,128]{2,1,0:T(8,128)(2,1)S(1)}, bf16[4,128,128]{2,1,0:T(8,128)(2,1)S(1)}, u32[]{:S(2)}, u32[]{:S(2)}) %collective-permute-start.6) | collective-permute-done | bytes 131104 | tf_op jit(solution)/shard_map/ppermute | solution.py:329
  42.9 1.5 %shard_map.129 = (f32[256,512]{1,0:T(8,128)S(1)}, bf16[256,512]{1,0:T(8,128)(2,1)S(1)}) custom-call(bf16[4,128,128]{2,1,0:T(8,128)(2,1)S(1)} %shard_map.128.a_ref, bf16[4,128,128]{2,1,0:T(8,128)(2,1)S(1)} %collective-permute-done.5.b_ref, bf16[4,128,128]{2,1,0:T(8,128)(2,1)S(1)} %collective-permute-done.6.c_ref, ...), custom_call_target="tpu_custom_call" | custom-call | tf_op jit(solution)/shard_map/pallas_call | solution.py:298
  44.4 0.1 collective-permute-start.9
  44.5 1.1 slice.140
  45.6 2.0 %collective-permute-start.18 = (bf16[160,1408]{1,0:T(8,128)(2,1)S(1)}, bf16[160,1408]{1,0:T(8,128)(2,1)S(1)}, u32[]{:S(2)}, u32[]{:S(2)}) collective-permute-start(bf16[160,1408]{1,0:T(8,128)(2,1)S(1)} %slice.140), channel_id=1, source_target_pairs={{0,8},{4,12},{8,0},{12,4},{16,24},{20,28},{24,16},{28,20},{1,9},{5... | collective-permute-start | bytes 1351688 | tf_op jit(solution)/shard_map/ppermute | solution.py:329
  47.6 0.1 convert_add_fusion
  47.7 1.6 %collective-permute-start.10 = (bf16[128,512]{1,0:T(8,128)(2,1)S(1)}, bf16[128,512]{1,0:T(8,128)(2,1)S(1)}, u32[]{:S(2)}, u32[]{:S(2)}) collective-permute-start(bf16[128,512]{1,0:T(8,128)(2,1)S(1)} %slice.221), channel_id=1, source_target_pairs={{0,2},{1,3},{2,0},{3,1},{4,6},{5,7},{6,4},{7,5},{8,10},{9,11},{10,... | collective-permute-start | bytes 393224 | tf_op jit(solution)/shard_map/ppermute | solution.py:329
  49.3 0.5 collective-permute-start.19
  49.8 9.1 %collective-permute-done.18.refs_1_ = bf16[160,1408]{1,0:T(8,128)(2,1)S(1)} collective-permute-done((bf16[160,1408]{1,0:T(8,128)(2,1)S(1)}, bf16[160,1408]{1,0:T(8,128)(2,1)S(1)}, u32[]{:S(2)}, u32[]{:S(2)}) %collective-permute-start.18) | collective-permute-done | bytes 450592 | tf_op jit(solution)/shard_map/ppermute | solution.py:329
  58.9 0.7 collective-permute-start.28
  59.6 4.7 %collective-permute-start.12 = (bf16[32,512]{1,0:T(8,128)(2,1)S(1)}, bf16[32,512]{1,0:T(8,128)(2,1)S(1)}, u32[]{:S(2)}, u32[]{:S(2)}) collective-permute-start(bf16[32,512]{1,0:T(8,128)(2,1)S(1)} %get-tuple-element.69), channel_id=1, source_target_pairs={{0,16},{4,20},{8,24},{12,28},{16,0},{20,4},{24,8},{28,12},{1,17},{... | collective-permute-start | bytes 98312 | tf_op jit(solution)/shard_map/ppermute | solution.py:329
  64.3 1.6 %collective-permute-start.11 = (bf16[32,512]{1,0:T(8,128)(2,1)S(1)}, bf16[32,512]{1,0:T(8,128)(2,1)S(1)}, u32[]{:S(2)}, u32[]{:S(2)}) collective-permute-start(bf16[32,512]{1,0:T(8,128)(2,1)S(1)} %get-tuple-element.70), channel_id=1, source_target_pairs={{0,24},{4,28},{8,16},{12,20},{16,8},{20,12},{24,0},{28,4},{1,25},{... | collective-permute-start | bytes 98312 | tf_op jit(solution)/shard_map/ppermute | solution.py:329
  66.0 10.1 %collective-permute-done.12 = bf16[32,512]{1,0:T(8,128)(2,1)S(1)} collective-permute-done((bf16[32,512]{1,0:T(8,128)(2,1)S(1)}, bf16[32,512]{1,0:T(8,128)(2,1)S(1)}, u32[]{:S(2)}, u32[]{:S(2)}) %collective-permute-start.12) | collective-permute-done | bytes 32800 | tf_op jit(solution)/shard_map/ppermute | solution.py:329
  76.2 0.2 fusion
  76.4 0.1 fusion.2
  76.5 2.5 %collective-permute-start.16 = (bf16[32,2048]{1,0:T(8,128)(2,1)S(1)}, bf16[32,2048]{1,0:T(8,128)(2,1)S(1)}, u32[]{:S(2)}, u32[]{:S(2)}) collective-permute-start(bf16[32,2048]{1,0:T(8,128)(2,1)S(1)} %fusion.2), channel_id=1, source_target_pairs={{0,6},{1,7},{2,4},{3,5},{4,2},{5,3},{6,0},{7,1},{8,14},{9,15},{10,... | collective-permute-start | bytes 393224 | tf_op jit(solution)/shard_map/ppermute | solution.py:337
  79.0 0.5 collective-permute-start.15
  79.5 0.5 collective-permute-start.14
  80.0 0.7 collective-permute-start.20
  80.7 1.7 %collective-permute-done.16 = bf16[32,2048]{1,0:T(8,128)(2,1)S(1)} collective-permute-done((bf16[32,2048]{1,0:T(8,128)(2,1)S(1)}, bf16[32,2048]{1,0:T(8,128)(2,1)S(1)}, u32[]{:S(2)}, u32[]{:S(2)}) %collective-permute-start.16) | collective-permute-done | bytes 131104 | tf_op jit(solution)/shard_map/ppermute | solution.py:337
  82.4 0.7 collective-permute-start.30
  83.1 0.9 collective-permute-done.15
  83.9 0.5 collective-permute-done.14
  84.5 0.1 collective-permute-start.17
  84.6 0.7 collective-permute-start.22
  85.3 1.3 collective-permute-start.29
  86.6 1.3 collective-permute-start.21
  87.9 1.3 collective-permute-start.31
  89.2 1.3 collective-permute-start.23
  90.5 6.0 %shard_map.130.hidden_ref = bf16[256,1408]{1,0:T(8,128)(2,1)S(1)} custom-call(bf16[128,2048]{1,0:T(8,128)(2,1)S(1)} %pad_maximum_fusion.here_ref, bf16[128,2048]{1,0:T(8,128)(2,1)S(1)} %collective-permute-done.17.there_ref, bf16[2048,1408]{1,0:T(8,128)(2,1)} %gate_ref.1, bf16[2048,1408]{1,0:T(8,128)(2,1)} %up_ref.1), custom_call_target="tpu_custom_call" | custom-call | tf_op jit(solution)/shard_map/pallas_call | solution.py:298
  96.6 21.0 %collective-permute-done.31.refs_3_ = bf16[96,1408]{1,0:T(8,128)(2,1)S(1)} collective-permute-done((bf16[96,1408]{1,0:T(8,128)(2,1)S(1)}, bf16[96,1408]{1,0:T(8,128)(2,1)S(1)}, u32[]{:S(2)}, u32[]{:S(2)}) %collective-permute-start.31) | collective-permute-done | bytes 270368 | tf_op jit(solution)/shard_map/ppermute | solution.py:353
  117.6 0.4 shard_map.132
  118.0 0.1 collective-permute-start.32
  118.1 4.8 %collective-permute-done.23.refs_6_ = bf16[96,1408]{1,0:T(8,128)(2,1)S(1)} collective-permute-done((bf16[96,1408]{1,0:T(8,128)(2,1)S(1)}, bf16[96,1408]{1,0:T(8,128)(2,1)S(1)}, u32[]{:S(2)}, u32[]{:S(2)}) %collective-permute-start.23) | collective-permute-done | bytes 270368 | tf_op jit(solution)/shard_map/ppermute | solution.py:352
  122.9 0.8 shard_map.131
  123.7 0.1 collective-permute-start.24
  123.8 1.4 %collective-permute-done.24 = bf16[128,768]{1,0:T(8,128)(2,1)S(1)} collective-permute-done((bf16[128,768]{1,0:T(8,128)(2,1)S(1)}, bf16[128,768]{1,0:T(8,128)(2,1)S(1)}, u32[]{:S(2)}, u32[]{:S(2)}) %collective-permute-start.24) | collective-permute-done | bytes 196640 | tf_op jit(solution)/shard_map/ppermute | solution.py:329
  125.2 0.1 fusion.18
  125.3 1.6 %collective-permute-start.25 = (bf16[32,768]{1,0:T(8,128)(2,1)S(1)}, bf16[32,768]{1,0:T(8,128)(2,1)S(1)}, u32[]{:S(2)}, u32[]{:S(2)}) collective-permute-start(bf16[32,768]{1,0:T(8,128)(2,1)S(1)} %get-tuple-element.67), channel_id=1, source_target_pairs={{0,2},{1,3},{2,0},{3,1},{4,6},{5,7},{6,4},{7,5},{8,10},{9,11},{10,... | collective-permute-start | bytes 147464 | tf_op jit(solution)/shard_map/ppermute | solution.py:329
  126.9 1.5 %collective-permute-start.26 = (bf16[32,768]{1,0:T(8,128)(2,1)S(1)}, bf16[32,768]{1,0:T(8,128)(2,1)S(1)}, u32[]{:S(2)}, u32[]{:S(2)}) collective-permute-start(bf16[32,768]{1,0:T(8,128)(2,1)S(1)} %get-tuple-element.66), channel_id=1, source_target_pairs={{0,4},{4,0},{8,12},{12,8},{16,20},{20,16},{24,28},{28,24},{1,5},{5... | collective-permute-start | bytes 147464 | tf_op jit(solution)/shard_map/ppermute | solution.py:329
  128.4 0.5 collective-permute-start.27
  128.9 1.5 %collective-permute-start.33 = (bf16[32,256]{1,0:T(8,128)(2,1)S(1)}, bf16[32,256]{1,0:T(8,128)(2,1)S(1)}, u32[]{:S(2)}, u32[]{:S(2)}) collective-permute-start(bf16[32,256]{1,0:T(8,128)(2,1)S(1)} %get-tuple-element.75), channel_id=1, source_target_pairs={{0,2},{1,3},{2,0},{3,1},{4,6},{5,7},{6,4},{7,5},{8,10},{9,11},{10,... | collective-permute-start | bytes 49160 | tf_op jit(solution)/shard_map/ppermute | solution.py:329
  130.4 1.5 %collective-permute-start.34 = (bf16[32,256]{1,0:T(8,128)(2,1)S(1)}, bf16[32,256]{1,0:T(8,128)(2,1)S(1)}, u32[]{:S(2)}, u32[]{:S(2)}) collective-permute-start(bf16[32,256]{1,0:T(8,128)(2,1)S(1)} %get-tuple-element.74), channel_id=1, source_target_pairs={{0,4},{4,0},{8,12},{12,8},{16,20},{20,16},{24,28},{28,24},{1,5},{5... | collective-permute-start | bytes 49160 | tf_op jit(solution)/shard_map/ppermute | solution.py:329
  131.8 0.8 collective-permute-done.33
  132.6 2.4 %collective-permute-start.35 = (bf16[32,256]{1,0:T(8,128)(2,1)S(1)}, bf16[32,256]{1,0:T(8,128)(2,1)S(1)}, u32[]{:S(2)}, u32[]{:S(2)}) collective-permute-start(bf16[32,256]{1,0:T(8,128)(2,1)S(1)} %get-tuple-element.73), channel_id=1, source_target_pairs={{0,6},{1,7},{2,4},{3,5},{4,2},{5,3},{6,0},{7,1},{8,14},{9,15},{10,... | collective-permute-start | bytes 49160 | tf_op jit(solution)/shard_map/ppermute | solution.py:337
  135.0 2.2 %collective-permute-done.35 = bf16[32,256]{1,0:T(8,128)(2,1)S(1)} collective-permute-done((bf16[32,256]{1,0:T(8,128)(2,1)S(1)}, bf16[32,256]{1,0:T(8,128)(2,1)S(1)}, u32[]{:S(2)}, u32[]{:S(2)}) %collective-permute-start.35) | collective-permute-done | bytes 16416 | tf_op jit(solution)/shard_map/ppermute | solution.py:337
  137.4 0.7 fusion.3
  (57 shorter events, 0.5 us)
Async XLA Ops:
  0.0 49.3 %copy-start = (bf16[256,1408]{1,0:T(8,128)(2,1)S(1)}, bf16[256,1408]{1,0:T(8,128)(2,1)}, u32[]{:S(2)}) copy-start(bf16[256,1408]{1,0:T(8,128)(2,1)} %refs_0_.3) | copy-start | bytes 2162692
  0.0 76.2 %copy-start.1 = (bf16[32,2048]{1,0:T(8,128)(2,1)S(1)}, bf16[32,2048]{1,0:T(8,128)(2,1)}, u32[]{:S(2)}) copy-start(bf16[32,2048]{1,0:T(8,128)(2,1)} %param.13) | copy-start | bytes 393220
  0.0 76.3 %copy-start.2 = (f32[2048]{0:T(1024)S(1)}, f32[2048]{0:T(1024)}, u32[]{:S(2)}) copy-start(f32[2048]{0:T(1024)} %param.22) | copy-start | bytes 24580
  1.4 8.8 %collective-permute-start.2 = (bf16[128,384]{1,0:T(8,128)(2,1)S(1)}, bf16[128,384]{1,0:T(8,128)(2,1)S(1)}, u32[]{:S(2)}, u32[]{:S(2)}) collective-permute-start(bf16[128,384]{1,0:T(8,128)(2,1)S(1)} %get-tuple-element.45), channel_id=1, source_target_pairs={{0,24},{4,28},{8,16},{12,20},{16,8},{20,12},{24,0},{28,4},{1,25},{... | collective-permute-start | bytes 294920 | tf_op jit(solution)/shard_map/ppermute | solution.py:329
  6.5 8.3 %collective-permute-start.1 = (bf16[128,384]{1,0:T(8,128)(2,1)S(1)}, bf16[128,384]{1,0:T(8,128)(2,1)S(1)}, u32[]{:S(2)}, u32[]{:S(2)}) collective-permute-start(bf16[128,384]{1,0:T(8,128)(2,1)S(1)} %get-tuple-element.46), channel_id=1, source_target_pairs={{0,16},{4,20},{8,24},{12,28},{16,0},{20,4},{24,8},{28,12},{1,17},{... | collective-permute-start | bytes 294920 | tf_op jit(solution)/shard_map/ppermute | solution.py:329
  6.5 8.3 %collective-permute-start = (bf16[128,384]{1,0:T(8,128)(2,1)S(1)}, bf16[128,384]{1,0:T(8,128)(2,1)S(1)}, u32[]{:S(2)}, u32[]{:S(2)}) collective-permute-start(bf16[128,384]{1,0:T(8,128)(2,1)S(1)} %get-tuple-element.47), channel_id=1, source_target_pairs={{0,8},{4,12},{8,0},{12,4},{16,24},{20,28},{24,16},{28,20},{1,9},{5... | collective-permute-start | bytes 294920 | tf_op jit(solution)/shard_map/ppermute | solution.py:329
  14.8 13.1 %collective-permute-start.4 = (bf16[384,256]{1,0:T(8,128)(2,1)S(1)}, bf16[384,256]{1,0:T(8,128)(2,1)S(1)}, u32[]{:S(2)}, u32[]{:S(2)}) collective-permute-start(bf16[384,256]{1,0:T(8,128)(2,1)S(1)} %pad_maximum_fusion.1), channel_id=1, source_target_pairs={{0,4},{4,0},{8,12},{12,8},{16,20},{20,16},{24,28},{28,24},{1,5},{5... | collective-permute-start | bytes 589832 | tf_op jit(solution)/shard_map/ppermute | solution.py:329
  16.4 19.1 %collective-permute-start.8 = (bf16[256,512]{1,0:T(8,128)(2,1)}, bf16[256,512]{1,0:T(8,128)(2,1)S(1)}, u32[]{:S(2)}, u32[]{:S(2)}) collective-permute-start(bf16[256,512]{1,0:T(8,128)(2,1)} %source.1), channel_id=1, source_target_pairs={{0,4},{4,0},{8,12},{12,8},{16,20},{20,16},{24,28},{28,24},{1,5},{5... | collective-permute-start | bytes 786440 | tf_op jit(solution)/shard_map/ppermute | solution.py:329
  16.9 11.0 %collective-permute-start.3 = (bf16[128,256]{1,0:T(8,128)(2,1)S(1)}, bf16[128,256]{1,0:T(8,128)(2,1)S(1)}, u32[]{:S(2)}, u32[]{:S(2)}) collective-permute-start(bf16[128,256]{1,0:T(8,128)(2,1)S(1)} %slice.156), channel_id=1, source_target_pairs={{0,4},{4,0},{8,12},{12,8},{16,20},{20,16},{24,28},{28,24},{1,5},{5... | collective-permute-start | bytes 196616 | tf_op jit(solution)/shard_map/ppermute | solution.py:329
  31.1 5.7 %collective-permute-start.5 = (bf16[4,128,128]{2,1,0:T(8,128)(2,1)S(1)}, bf16[4,128,128]{2,1,0:T(8,128)(2,1)S(1)}, u32[]{:S(2)}, u32[]{:S(2)}) collective-permute-start(bf16[4,128,128]{2,1,0:T(8,128)(2,1)S(1)} %shard_map.128.a_ref), channel_id=1, source_target_pairs={{0,8},{4,12},{8,0},{12,4},{16,24},{20,28},{24,16},{28,20},{1,9},{5... | collective-permute-start | bytes 393224 | tf_op jit(solution)/shard_map/ppermute | solution.py:329
  31.5 11.4 %collective-permute-start.6 = (bf16[4,128,128]{2,1,0:T(8,128)(2,1)S(1)}, bf16[4,128,128]{2,1,0:T(8,128)(2,1)S(1)}, u32[]{:S(2)}, u32[]{:S(2)}) collective-permute-start(bf16[4,128,128]{2,1,0:T(8,128)(2,1)S(1)} %shard_map.128.a_ref), channel_id=1, source_target_pairs={{0,16},{4,20},{8,24},{12,28},{16,0},{20,4},{24,8},{28,12},{1,17},{... | collective-permute-start | bytes 393224 | tf_op jit(solution)/shard_map/ppermute | solution.py:329
  33.8 9.1 %collective-permute-start.7 = (bf16[4,128,128]{2,1,0:T(8,128)(2,1)S(1)}, bf16[4,128,128]{2,1,0:T(8,128)(2,1)S(1)}, u32[]{:S(2)}, u32[]{:S(2)}) collective-permute-start(bf16[4,128,128]{2,1,0:T(8,128)(2,1)S(1)} %shard_map.128.a_ref), channel_id=1, source_target_pairs={{0,24},{4,28},{8,16},{12,20},{16,8},{20,12},{24,0},{28,4},{1,25},{... | collective-permute-start | bytes 393224 | tf_op jit(solution)/shard_map/ppermute | solution.py:329
  44.4 3.2 %collective-permute-start.9 = (bf16[256,512]{1,0:T(8,128)(2,1)S(1)}, bf16[256,512]{1,0:T(8,128)(2,1)S(1)}, u32[]{:S(2)}, u32[]{:S(2)}) collective-permute-start(bf16[256,512]{1,0:T(8,128)(2,1)S(1)} %get-tuple-element.24), channel_id=1, source_target_pairs={{0,1},{1,0},{2,3},{3,2},{4,5},{5,4},{6,7},{7,6},{8,9},{9,8},{10,11... | collective-permute-start | bytes 786440 | tf_op jit(solution)/shard_map/ppermute | solution.py:329
  45.6 13.3 %collective-permute-start.18 = (bf16[160,1408]{1,0:T(8,128)(2,1)S(1)}, bf16[160,1408]{1,0:T(8,128)(2,1)S(1)}, u32[]{:S(2)}, u32[]{:S(2)}) collective-permute-start(bf16[160,1408]{1,0:T(8,128)(2,1)S(1)} %slice.140), channel_id=1, source_target_pairs={{0,8},{4,12},{8,0},{12,4},{16,24},{20,28},{24,16},{28,20},{1,9},{5... | collective-permute-start | bytes 1351688 | tf_op jit(solution)/shard_map/ppermute | solution.py:329
  47.7 11.8 %collective-permute-start.10 = (bf16[128,512]{1,0:T(8,128)(2,1)S(1)}, bf16[128,512]{1,0:T(8,128)(2,1)S(1)}, u32[]{:S(2)}, u32[]{:S(2)}) collective-permute-start(bf16[128,512]{1,0:T(8,128)(2,1)S(1)} %slice.221), channel_id=1, source_target_pairs={{0,2},{1,3},{2,0},{3,1},{4,6},{5,7},{6,4},{7,5},{8,10},{9,11},{10,... | collective-permute-start | bytes 393224 | tf_op jit(solution)/shard_map/ppermute | solution.py:329
  49.3 30.7 %collective-permute-start.19 = (bf16[96,1408]{1,0:T(8,128)(2,1)S(1)}, bf16[96,1408]{1,0:T(8,128)(2,1)S(1)}, u32[]{:S(2)}, u32[]{:S(2)}) collective-permute-start(bf16[96,1408]{1,0:T(8,128)(2,1)S(1)} %slice.141), channel_id=1, source_target_pairs={{0,8},{4,12},{8,0},{12,4},{16,24},{20,28},{24,16},{28,20},{1,9},{5... | collective-permute-start | bytes 811016 | tf_op jit(solution)/shard_map/ppermute | solution.py:329
  58.9 26.4 %collective-permute-start.28 = (bf16[160,1408]{1,0:T(8,128)(2,1)S(1)}, bf16[160,1408]{1,0:T(8,128)(2,1)S(1)}, u32[]{:S(2)}, u32[]{:S(2)}) collective-permute-start(bf16[160,1408]{1,0:T(8,128)(2,1)S(1)} %collective-permute-done.18.refs_1_), channel_id=1, source_target_pairs={{8,16},{12,20},{16,8},{20,12},{9,17},{13,21},{17,9},{21,13},{10,18... | collective-permute-start | bytes 1351688 | tf_op jit(solution)/shard_map/ppermute | solution.py:351
  59.6 16.4 %collective-permute-start.12 = (bf16[32,512]{1,0:T(8,128)(2,1)S(1)}, bf16[32,512]{1,0:T(8,128)(2,1)S(1)}, u32[]{:S(2)}, u32[]{:S(2)}) collective-permute-start(bf16[32,512]{1,0:T(8,128)(2,1)S(1)} %get-tuple-element.69), channel_id=1, source_target_pairs={{0,16},{4,20},{8,24},{12,28},{16,0},{20,4},{24,8},{28,12},{1,17},{... | collective-permute-start | bytes 98312 | tf_op jit(solution)/shard_map/ppermute | solution.py:329
  64.3 11.7 %collective-permute-start.11 = (bf16[32,512]{1,0:T(8,128)(2,1)S(1)}, bf16[32,512]{1,0:T(8,128)(2,1)S(1)}, u32[]{:S(2)}, u32[]{:S(2)}) collective-permute-start(bf16[32,512]{1,0:T(8,128)(2,1)S(1)} %get-tuple-element.70), channel_id=1, source_target_pairs={{0,24},{4,28},{8,16},{12,20},{16,8},{20,12},{24,0},{28,4},{1,25},{... | collective-permute-start | bytes 98312 | tf_op jit(solution)/shard_map/ppermute | solution.py:329
  66.0 10.1 %collective-permute-start.13 = (bf16[32,512]{1,0:T(8,128)(2,1)S(1)}, bf16[32,512]{1,0:T(8,128)(2,1)S(1)}, u32[]{:S(2)}, u32[]{:S(2)}) collective-permute-start(bf16[32,512]{1,0:T(8,128)(2,1)S(1)} %get-tuple-element.68), channel_id=1, source_target_pairs={{0,8},{4,12},{8,0},{12,4},{16,24},{20,28},{24,16},{28,20},{1,9},{5... | collective-permute-start | bytes 98312 | tf_op jit(solution)/shard_map/ppermute | solution.py:329
  76.5 5.9 %collective-permute-start.16 = (bf16[32,2048]{1,0:T(8,128)(2,1)S(1)}, bf16[32,2048]{1,0:T(8,128)(2,1)S(1)}, u32[]{:S(2)}, u32[]{:S(2)}) collective-permute-start(bf16[32,2048]{1,0:T(8,128)(2,1)S(1)} %fusion.2), channel_id=1, source_target_pairs={{0,6},{1,7},{2,4},{3,5},{4,2},{5,3},{6,0},{7,1},{8,14},{9,15},{10,... | collective-permute-start | bytes 393224 | tf_op jit(solution)/shard_map/ppermute | solution.py:337
  79.0 5.0 %collective-permute-start.15 = (bf16[32,2048]{1,0:T(8,128)(2,1)S(1)}, bf16[32,2048]{1,0:T(8,128)(2,1)S(1)}, u32[]{:S(2)}, u32[]{:S(2)}) collective-permute-start(bf16[32,2048]{1,0:T(8,128)(2,1)S(1)} %fusion.2), channel_id=1, source_target_pairs={{0,4},{4,0},{8,12},{12,8},{16,20},{20,16},{24,28},{28,24},{1,5},{5... | collective-permute-start | bytes 393224 | tf_op jit(solution)/shard_map/ppermute | solution.py:329
  79.5 5.0 %collective-permute-start.14 = (bf16[32,2048]{1,0:T(8,128)(2,1)S(1)}, bf16[32,2048]{1,0:T(8,128)(2,1)S(1)}, u32[]{:S(2)}, u32[]{:S(2)}) collective-permute-start(bf16[32,2048]{1,0:T(8,128)(2,1)S(1)} %fusion.2), channel_id=1, source_target_pairs={{0,2},{1,3},{2,0},{3,1},{4,6},{5,7},{6,4},{7,5},{8,10},{9,11},{10,... | collective-permute-start | bytes 393224 | tf_op jit(solution)/shard_map/ppermute | solution.py:329
  80.0 6.6 %collective-permute-start.20 = (bf16[160,1408]{1,0:T(8,128)(2,1)S(1)}, bf16[160,1408]{1,0:T(8,128)(2,1)S(1)}, u32[]{:S(2)}, u32[]{:S(2)}) collective-permute-start(bf16[160,1408]{1,0:T(8,128)(2,1)S(1)} %slice.140), channel_id=1, source_target_pairs={{8,16},{12,20},{16,8},{20,12},{9,17},{13,21},{17,9},{21,13},{10,18... | collective-permute-start | bytes 1351688 | tf_op jit(solution)/shard_map/ppermute | solution.py:350
  82.4 5.5 %collective-permute-start.30 = (bf16[96,1408]{1,0:T(8,128)(2,1)S(1)}, bf16[96,1408]{1,0:T(8,128)(2,1)S(1)}, u32[]{:S(2)}, u32[]{:S(2)}) collective-permute-start(bf16[96,1408]{1,0:T(8,128)(2,1)S(1)} %collective-permute-done.19.refs_2_), channel_id=1, source_target_pairs={{8,16},{12,20},{16,8},{20,12},{9,17},{13,21},{17,9},{21,13},{10,18... | collective-permute-start | bytes 811016 | tf_op jit(solution)/shard_map/ppermute | solution.py:351
  84.5 6.0 %collective-permute-start.17 = (bf16[128,2048]{1,0:T(8,128)(2,1)S(1)}, bf16[128,2048]{1,0:T(8,128)(2,1)S(1)}, u32[]{:S(2)}, u32[]{:S(2)}) collective-permute-start(bf16[128,2048]{1,0:T(8,128)(2,1)S(1)} %pad_maximum_fusion.here_ref), channel_id=1, source_target_pairs={{0,1},{1,0},{2,3},{3,2},{4,5},{5,4},{6,7},{7,6},{8,9},{9,8},{10,11... | collective-permute-start | bytes 1572872 | tf_op jit(solution)/shard_map/ppermute | solution.py:329
  84.6 4.6 %collective-permute-start.22 = (bf16[96,1408]{1,0:T(8,128)(2,1)S(1)}, bf16[96,1408]{1,0:T(8,128)(2,1)S(1)}, u32[]{:S(2)}, u32[]{:S(2)}) collective-permute-start(bf16[96,1408]{1,0:T(8,128)(2,1)S(1)} %slice.141), channel_id=1, source_target_pairs={{8,16},{12,20},{16,8},{20,12},{9,17},{13,21},{17,9},{21,13},{10,18... | collective-permute-start | bytes 811016 | tf_op jit(solution)/shard_map/ppermute | solution.py:350
  85.3 32.3 %collective-permute-start.29 = (bf16[160,1408]{1,0:T(8,128)(2,1)S(1)}, bf16[160,1408]{1,0:T(8,128)(2,1)S(1)}, u32[]{:S(2)}, u32[]{:S(2)}) collective-permute-start(bf16[160,1408]{1,0:T(8,128)(2,1)S(1)} %collective-permute-done.28.refs_0_), channel_id=1, source_target_pairs={{8,0},{12,4},{16,24},{20,28},{9,1},{13,5},{17,25},{21,29},{10,2},{... | collective-permute-start | bytes 1351688 | tf_op jit(solution)/shard_map/ppermute | solution.py:353
  86.6 36.3 %collective-permute-start.21 = (bf16[160,1408]{1,0:T(8,128)(2,1)S(1)}, bf16[160,1408]{1,0:T(8,128)(2,1)S(1)}, u32[]{:S(2)}, u32[]{:S(2)}) collective-permute-start(bf16[160,1408]{1,0:T(8,128)(2,1)S(1)} %collective-permute-done.20.refs_3_), channel_id=1, source_target_pairs={{8,0},{12,4},{16,24},{20,28},{9,1},{13,5},{17,25},{21,29},{10,2},{... | collective-permute-start | bytes 1351688 | tf_op jit(solution)/shard_map/ppermute | solution.py:352
  87.9 29.7 %collective-permute-start.31 = (bf16[96,1408]{1,0:T(8,128)(2,1)S(1)}, bf16[96,1408]{1,0:T(8,128)(2,1)S(1)}, u32[]{:S(2)}, u32[]{:S(2)}) collective-permute-start(bf16[96,1408]{1,0:T(8,128)(2,1)S(1)} %collective-permute-done.30.refs_2_), channel_id=1, source_target_pairs={{8,0},{12,4},{16,24},{20,28},{9,1},{13,5},{17,25},{21,29},{10,2},{... | collective-permute-start | bytes 811016 | tf_op jit(solution)/shard_map/ppermute | solution.py:353
  89.2 33.7 %collective-permute-start.23 = (bf16[96,1408]{1,0:T(8,128)(2,1)S(1)}, bf16[96,1408]{1,0:T(8,128)(2,1)S(1)}, u32[]{:S(2)}, u32[]{:S(2)}) collective-permute-start(bf16[96,1408]{1,0:T(8,128)(2,1)S(1)} %collective-permute-done.22.refs_5_), channel_id=1, source_target_pairs={{8,0},{12,4},{16,24},{20,28},{9,1},{13,5},{17,25},{21,29},{10,2},{... | collective-permute-start | bytes 811016 | tf_op jit(solution)/shard_map/ppermute | solution.py:352
  118.0 5.8 %collective-permute-start.32 = (bf16[128,256]{1,0:T(8,128)(2,1)S(1)}, bf16[128,256]{1,0:T(8,128)(2,1)S(1)}, u32[]{:S(2)}, u32[]{:S(2)}) collective-permute-start(bf16[128,256]{1,0:T(8,128)(2,1)S(1)} %get-tuple-element.28), channel_id=1, source_target_pairs={{0,1},{1,0},{2,3},{3,2},{4,5},{5,4},{6,7},{7,6},{8,9},{9,8},{10,11... | collective-permute-start | bytes 196616 | tf_op jit(solution)/shard_map/ppermute | solution.py:329
  123.7 1.5 %collective-permute-start.24 = (bf16[128,768]{1,0:T(8,128)(2,1)S(1)}, bf16[128,768]{1,0:T(8,128)(2,1)S(1)}, u32[]{:S(2)}, u32[]{:S(2)}) collective-permute-start(bf16[128,768]{1,0:T(8,128)(2,1)S(1)} %get-tuple-element.26), channel_id=1, source_target_pairs={{0,1},{1,0},{2,3},{3,2},{4,5},{5,4},{6,7},{7,6},{8,9},{9,8},{10,11... | collective-permute-start | bytes 589832 | tf_op jit(solution)/shard_map/ppermute | solution.py:329
  125.3 11.9 %collective-permute-start.25 = (bf16[32,768]{1,0:T(8,128)(2,1)S(1)}, bf16[32,768]{1,0:T(8,128)(2,1)S(1)}, u32[]{:S(2)}, u32[]{:S(2)}) collective-permute-start(bf16[32,768]{1,0:T(8,128)(2,1)S(1)} %get-tuple-element.67), channel_id=1, source_target_pairs={{0,2},{1,3},{2,0},{3,1},{4,6},{5,7},{6,4},{7,5},{8,10},{9,11},{10,... | collective-permute-start | bytes 147464 | tf_op jit(solution)/shard_map/ppermute | solution.py:329
  126.9 10.4 %collective-permute-start.26 = (bf16[32,768]{1,0:T(8,128)(2,1)S(1)}, bf16[32,768]{1,0:T(8,128)(2,1)S(1)}, u32[]{:S(2)}, u32[]{:S(2)}) collective-permute-start(bf16[32,768]{1,0:T(8,128)(2,1)S(1)} %get-tuple-element.66), channel_id=1, source_target_pairs={{0,4},{4,0},{8,12},{12,8},{16,20},{20,16},{24,28},{28,24},{1,5},{5... | collective-permute-start | bytes 147464 | tf_op jit(solution)/shard_map/ppermute | solution.py:329
  128.4 8.9 %collective-permute-start.27 = (bf16[32,768]{1,0:T(8,128)(2,1)S(1)}, bf16[32,768]{1,0:T(8,128)(2,1)S(1)}, u32[]{:S(2)}, u32[]{:S(2)}) collective-permute-start(bf16[32,768]{1,0:T(8,128)(2,1)S(1)} %get-tuple-element.65), channel_id=1, source_target_pairs={{0,6},{1,7},{2,4},{3,5},{4,2},{5,3},{6,0},{7,1},{8,14},{9,15},{10,... | collective-permute-start | bytes 147464 | tf_op jit(solution)/shard_map/ppermute | solution.py:337
  128.9 3.7 %collective-permute-start.33 = (bf16[32,256]{1,0:T(8,128)(2,1)S(1)}, bf16[32,256]{1,0:T(8,128)(2,1)S(1)}, u32[]{:S(2)}, u32[]{:S(2)}) collective-permute-start(bf16[32,256]{1,0:T(8,128)(2,1)S(1)} %get-tuple-element.75), channel_id=1, source_target_pairs={{0,2},{1,3},{2,0},{3,1},{4,6},{5,7},{6,4},{7,5},{8,10},{9,11},{10,... | collective-permute-start | bytes 49160 | tf_op jit(solution)/shard_map/ppermute | solution.py:329
  130.4 4.7 %collective-permute-start.34 = (bf16[32,256]{1,0:T(8,128)(2,1)S(1)}, bf16[32,256]{1,0:T(8,128)(2,1)S(1)}, u32[]{:S(2)}, u32[]{:S(2)}) collective-permute-start(bf16[32,256]{1,0:T(8,128)(2,1)S(1)} %get-tuple-element.74), channel_id=1, source_target_pairs={{0,4},{4,0},{8,12},{12,8},{16,20},{20,16},{24,28},{28,24},{1,5},{5... | collective-permute-start | bytes 49160 | tf_op jit(solution)/shard_map/ppermute | solution.py:329
  132.6 4.6 %collective-permute-start.35 = (bf16[32,256]{1,0:T(8,128)(2,1)S(1)}, bf16[32,256]{1,0:T(8,128)(2,1)S(1)}, u32[]{:S(2)}, u32[]{:S(2)}) collective-permute-start(bf16[32,256]{1,0:T(8,128)(2,1)S(1)} %get-tuple-element.73), channel_id=1, source_target_pairs={{0,6},{1,7},{2,4},{3,5},{4,2},{5,3},{6,0},{7,1},{8,14},{9,15},{10,... | collective-permute-start | bytes 49160 | tf_op jit(solution)/shard_map/ppermute | solution.py:337
